TPU v7x, 32 devices: a whole 2x2x4 slice. The times are simulated.
32 devices in a mesh: sp: 4 (over z), dp: 8 (over y, x, core).
Axes of the slice: x: 2, y: 2, z: 4, core: 2. Of those that a mesh axis runs over, the one named last changes fastest.
Arguments:
- value_half: bfloat16 [8, 1536, 2048], P('dp', 'sp'), may hold values from -6 to 6
- gate_half: bfloat16 [8, 1536, 2048], P('dp', 'sp'), may hold values from -9 to 9
- conv_taps: bfloat16 [31, 2048], replicated, may hold values from -1 to 1
- norm_gain: float32 [2048], replicated, may hold values from 0.1 to 1.9
- norm_shift: float32 [2048], replicated, may hold values from -3 to 3
- out_weight: bfloat16 [2048, 2048], P('dp', 'sp'), may hold values from -0.125 to 0.125
Outputs:
- module_out: bfloat16 [8, 1536, 2048], P('dp', 'sp')
All inputs are finite; a program needn't handle non-finite values.
Results may differ from a plain program's by a relative error of at most 0.0064.
Values may be sent and summed in bfloat16 or wider, within the bound.
No kernel may reach another device: no remote copies, remote signals or barrier semaphores. Data moves between devices by JAX's collectives and lax.ppermute only.
A program may use at most 64 MiB of HBM per device.

v0:
```python
import jax
import jax.numpy as jnp
from jax import lax
from jax.sharding import PartitionSpec as P

EPSILON = 1e-06


def passed_along(value, axis, steps):
    count = lax.axis_size(axis)
    initial, last = (max(0, -steps), min(count, count - steps))
    return lax.ppermute(value, axis, [(source, source + steps) for source in range(initial, last)])


def causal_mix(padded, conv_taps, length):
    tap_count = conv_taps.shape[0]
    running = jnp.zeros((length, padded.shape[1]), jnp.float32)
    for tap_index in range(tap_count):
        running = running + padded[tap_index : tap_index + length].astype(jnp.float32) * conv_taps[
            tap_index
        ].astype(jnp.float32)
    return running.astype(jnp.bfloat16)


def per_device(value_half, gate_half, conv_taps, norm_gain, norm_shift, out_weight):
    tap_count = conv_taps.shape[0]
    tok_rows = value_half.shape[1]
    gated = (
        value_half[0].astype(jnp.float32) * jax.nn.sigmoid(gate_half[0].astype(jnp.float32))
    ).astype(jnp.bfloat16)
    tail_rows = gated[tok_rows - (tap_count - 1) :]
    history = passed_along(tail_rows, "sp", 1)
    padded = jnp.concatenate([history, gated], 0)
    convolved = causal_mix(padded, conv_taps, tok_rows)
    widened = convolved.astype(jnp.float32)
    mean_row = jnp.mean(widened, axis=-1, keepdims=True)
    centered = widened - mean_row
    variance = jnp.mean(centered * centered, axis=-1, keepdims=True)
    normed = centered * lax.rsqrt(variance + EPSILON) * norm_gain + norm_shift
    activated = jax.nn.silu(normed).astype(jnp.bfloat16)
    row_block = lax.all_gather(out_weight, "sp", axis=1, tiled=True)
    projected = jnp.dot(
        activated,
        lax.all_gather(row_block, "dp", axis=0, tiled=True),
        preferred_element_type=jnp.float32,
    )
    return projected.astype(jnp.bfloat16)[None]


def solution(mesh):
    placed = (P("dp", "sp", None), P("dp", "sp", None), P(), P(), P(), P("dp", "sp"))
    return jax.shard_map(
        per_device, mesh=mesh, in_specs=placed, out_specs=P("dp", "sp", None), check_vma=False
    )
```

profile of v0, /device:TPU:0, one launch (start us, length us, event | category | flops | bytes accessed | tf_op | source)
XLA Modules:
  0.0 110.5 jit_solution(4330929815768049006)
XLA Ops:
  6.5 0.0 copy-start
  6.5 0.0 all-gather.3.cloned.1.call-start
  6.5 0.7 all-gather.3.cloned.1.call-update
  7.3 0.0 all-gather.5.cloned.1.call-start
  7.3 32.3 %all-gather.3.cloned.1.call-done = bf16[256,2048]{1,0:T(8,128)(2,1)} async-done(((bf16[256,512]{1,0:T(8,128)(2,1)}), bf16[256,2048]{1,0:T(8,128)(2,1)}) %all-gather.3.cloned.1.call-update) | async-done | bytes 1048592 | tf_op jit(solution)/shard_map/all_gather | solution.py:41
  39.6 0.0 all-gather.5.cloned.1.call-update
  39.7 2.8 %multiply_convert_fusion = bf16[1,384,2048]{2,1,0:T(8,128)(2,1)S(1)} fusion(bf16[1,384,2048]{2,1,0:T(8,128)(2,1)} %param.6, bf16[1,384,2048]{2,1,0:T(8,128)(2,1)} %param.7), kind=kLoop, calls=%fused_computation.42 | loop fusion | flops 5505024 | bytes 4718592 | tf_op jit(solution)/shard_map/convert_element_type | solution.py:30
  42.5 0.0 copy-start.1
  42.5 0.0 copy-start.2
  42.5 3.4 %collective-permute-start = (bf16[30,2048]{1,0:T(8,128)(2,1)S(1)}, bf16[30,2048]{1,0:T(8,128)(2,1)S(1)}, u32[]{:S(2)}, u32[]{:S(2)}) collective-permute-start(bf16[30,2048]{1,0:T(8,128)(2,1)S(1)} %slice_bitcast_fusion), channel_id=1, source_target_pairs={{0,8},{8,16},{16,24},{1,9},{9,17},{17,25},{2,10},{10,18},{18,26},{... | collective-permute-start | bytes 368648 | tf_op jit(solution)/shard_map/ppermute | solution.py:12
  45.9 0.0 copy-done
  45.9 0.1 slice_convert_fusion.30
  46.0 0.1 slice_convert_fusion.29
  46.1 2.3 %collective-permute-done = bf16[30,2048]{1,0:T(8,128)(2,1)S(1)} collective-permute-done((bf16[30,2048]{1,0:T(8,128)(2,1)S(1)}, bf16[30,2048]{1,0:T(8,128)(2,1)S(1)}, u32[]{:S(2)}, u32[]{:S(2)}) %collective-permute-start) | collective-permute-done | bytes 122912 | tf_op jit(solution)/shard_map/ppermute | solution.py:12
  48.4 14.3 %convert_reduce_fusion = (f32[384]{0:T(512)S(1)}, bf16[384,2048]{1,0:T(8,128)(2,1)S(1)}) fusion(f32[2048]{0:T(1024)S(1)} %bitcast.67, bf16[384,2048]{1,0:T(8,128)(2,1)S(1)} %bitcast.37, f32[2048]{0:T(1024)S(1)} %bitcast.68, bf16[30,2048]{1,0:T(8,128)(2,1)S(1)} %collective-permute-done, f32[2048]{0:T(1024)S(1)} %bitcast.39, f32[2048]{0:T(1024)S(1)} %bitcast.40, ...), kind=kLoop, calls=%fused_computation.30 | loop fusion | flops 145489536 | bytes 3524096 | tf_op jit(solution)/shard_map/reduce_sum | solution.py:36
  62.7 0.6 fusion.2
  63.2 31.9 %all-gather.5.cloned.1.call-done = bf16[2048,2048]{1,0:T(8,128)(2,1)} async-done(((bf16[256,2048]{1,0:T(8,128)(2,1)}), bf16[2048,2048]{1,0:T(8,128)(2,1)}) %all-gather.5.cloned.1.call-update) | async-done | bytes 8388624 | tf_op jit(solution)/shard_map/all_gather | solution.py:44
  95.2 0.0 copy-done.1
  95.2 0.0 copy-done.2
  95.2 8.5 %fusion.11 = bf16[1,384,2048]{2,1,0:T(8,128)(2,1)} fusion(bf16[2048,2048]{1,0:T(8,128)(2,1)} %all-gather.5.cloned.1.call-done, bf16[384,2048]{1,0:T(8,128)(2,1)S(1)} %get-tuple-element.6, f32[2048]{0:T(1024)S(1)} %copy-done.1, f32[2048]{0:T(1024)S(1)} %copy-done.2, f32[384]{0:T(512)S(1)} %add_rsqrt_fusion, f32[384]{0:T(512)S(1)} %broadcast_multiply_fusion), kind=kOutput, calls=%fused_computation.45 | convolution fusion | flops 3229876224 | bytes 11553792 | tf_op jit(solution)/shard_map/dot_general | solution.py:42
  (3 shorter events, 0.0 us)
Async XLA Ops:
  6.5 39.4 %copy-start = (bf16[31,2048]{1,0:T(8,128)(2,1)S(1)}, bf16[31,2048]{1,0:T(8,128)(2,1)}, u32[]{:S(2)}) copy-start(bf16[31,2048]{1,0:T(8,128)(2,1)} %param.8) | copy-start | bytes 380932
  6.5 33.1 %all-gather.3.cloned.1.call-start = ((), (), s32[]{:S(2)}) async-start(), calls=%async_computation | async-start | bytes 1310720 | tf_op jit(solution)/shard_map/all_gather | solution.py:41
  7.3 87.9 %all-gather.5.cloned.1.call-start = ((), (), s32[]{:S(2)}) async-start(), calls=%async_computation.1 | async-start | bytes 9437184 | tf_op jit(solution)/shard_map/all_gather | solution.py:44
  42.5 52.7 %copy-start.1 = (f32[2048]{0:T(1024)S(1)}, f32[2048]{0:T(1024)}, u32[]{:S(2)}) copy-start(f32[2048]{0:T(1024)} %param.10) | copy-start | bytes 24580
  42.5 52.7 %copy-start.2 = (f32[2048]{0:T(1024)S(1)}, f32[2048]{0:T(1024)}, u32[]{:S(2)}) copy-start(f32[2048]{0:T(1024)} %param.9) | copy-start | bytes 24580
  42.5 5.9 %collective-permute-start = (bf16[30,2048]{1,0:T(8,128)(2,1)S(1)}, bf16[30,2048]{1,0:T(8,128)(2,1)S(1)}, u32[]{:S(2)}, u32[]{:S(2)}) collective-permute-start(bf16[30,2048]{1,0:T(8,128)(2,1)S(1)} %slice_bitcast_fusion), channel_id=1, source_target_pairs={{0,8},{8,16},{16,24},{1,9},{9,17},{17,25},{2,10},{10,18},{18,26},{... | collective-permute-start | bytes 368648 | tf_op jit(solution)/shard_map/ppermute | solution.py:12
Sparse Core Ops, SparseCore 0:
  8.9 30.6 all-gather.2
  41.5 53.6 all-gather.4
where the time goes:
time: 111 us
  waiting for transfers between devices  67.3 us (61%)
  other arithmetic  17.8 us (16%)
  between operations  13.5 us (12%)
  matrix products  8.49 us (8%)
  starting transfers between devices  3.4 us (3%)
    all_gather x1, waiting for transfers between devices, per_device(): row_block = lax.all_gather(out_weight, 'sp', axis=1, tiled=True)  32.3 us
    all_gather x1, waiting for transfers between devices, per_device(): lax.all_gather(row_block, 'dp', axis=0, tiled=True)  31.9 us
    reduce_sum x1, other arithmetic, per_device(): mean_row = jnp.mean(widened, axis=-1, keepdims=True)  14.3 us
    dot_general x1, matrix products, per_device(): jnp.dot(activated, lax.all_gather(row_block, 'dp', axis=0, tiled=True), p...  8.49 us
    ppermute x1, starting transfers between devices, passed_along(): lax.ppermute(value, axis, [(source, source + steps) for source in range(i...  3.36 us
    convert_element_type x1, other arithmetic, per_device(): gated = (value_half[0].astype(jnp.float32) * jax.nn.sigmoid(gate_half[0]....  2.79 us
    ppermute x1, waiting for transfers between devices, passed_along(): lax.ppermute(value, axis, [(source, source + steps) for source in range(i...  2.29 us
  transfers between devices with their start and end apart: 3, of which 3 were waited for; matrix products, arithmetic and copies ran while one was open for 16% of the time, Pallas kernels for 0%

commit v1 on v0

v1 whole, which is shorter than its diff:
```python
import functools

import jax
import jax.numpy as jnp
from jax import lax
from jax.experimental import pallas as pl
from jax.experimental.pallas import tpu as pltpu
from jax.sharding import PartitionSpec as P


EPSILON = 1e-06
LANES = 128


def swapped(value, axis, mask_of):
    count = lax.axis_size(axis)
    return lax.ppermute(value, axis, [(index, index ^ mask_of(index)) for index in range(count)])


def named(value, axis, even, odd):
    return swapped(value, axis, lambda index: odd if index & 1 else even)


def passed_along(value, axis, steps):
    count = lax.axis_size(axis)
    initial, last = (max(0, -steps), min(count, count - steps))
    return lax.ppermute(value, axis, [(source, source + steps) for source in range(initial, last)])


def plane_gather(piece, axis):
    count = lax.axis_size(axis)
    masks = [1 << bit for bit in range(1, (count - 1).bit_length())]
    held = piece[None]
    for even, odd in zip(masks, masks[::-1]):
        other = swapped(held, axis, lambda index: odd if index & 1 else even)
        held = jnp.concatenate([held, other], 0)
    return jnp.concatenate([held, swapped(held, axis, lambda index: 1)], 0)


def slot_offsets(count):
    masks = [1 << bit for bit in range(1, (count - 1).bit_length())]
    halves = []
    for order in (masks, masks[::-1]):
        held = [0]
        for mask in order:
            held = held + [offset ^ mask for offset in held]
        halves.append(held)
    return [halves[parity] + [offset ^ 1 for offset in halves[1 - parity]] for parity in range(2)]


def general(value_half, gate_half, conv_taps, norm_gain, norm_shift, out_weight):
    tap_count, tok_rows = (conv_taps.shape[0], value_half.shape[1])
    layers, blocks = (lax.axis_size("sp"), lax.axis_size("dp"))
    here, place = (lax.axis_index("sp"), lax.axis_index("dp"))
    depth, width = out_weight.shape
    gathered = [
        plane_gather(swapped(out_weight, "sp", lambda index: step) if step else out_weight, "dp")
        for step in range(layers)
    ]
    gated = (
        value_half[0].astype(jnp.float32) * jax.nn.sigmoid(gate_half[0].astype(jnp.float32))
    ).astype(jnp.bfloat16)
    history = passed_along(gated[tok_rows - (tap_count - 1) :], "sp", 1)
    padded = jnp.concatenate([history, gated], 0)
    running = jnp.zeros(gated.shape, jnp.float32)
    for tap_index in range(tap_count):
        running = running + padded[tap_index : tap_index + tok_rows].astype(jnp.float32) * conv_taps[
            tap_index
        ].astype(jnp.float32)
    widened = running.astype(jnp.bfloat16).astype(jnp.float32)
    centered = widened - jnp.mean(widened, axis=-1, keepdims=True)
    variance = jnp.mean(centered * centered, axis=-1, keepdims=True)
    normed = centered * lax.rsqrt(variance + EPSILON) * norm_gain + norm_shift
    activated = jax.nn.silu(normed).astype(jnp.bfloat16)
    even, odd = slot_offsets(blocks)
    offsets = jnp.where(place % 2 == 0, jnp.array(even), jnp.array(odd))
    ordered = jnp.concatenate(
        [
            lax.dynamic_slice_in_dim(activated, (place ^ offsets[slot]) * depth, depth, 1)
            for slot in range(blocks)
        ],
        1,
    )
    out = jnp.zeros((tok_rows, layers * width), jnp.bfloat16)
    for step in range(layers):
        part = jnp.dot(
            ordered,
            gathered[step].reshape(blocks * depth, width),
            preferred_element_type=jnp.float32,
        ).astype(jnp.bfloat16)
        out = lax.dynamic_update_slice_in_dim(out, part, (here ^ step) * width, 1)
    return out[None]


GATHERED = ((0, 2, 4, 6), (0, 4, 2, 6))
SWAPS = (((0, 1, 2, 3),), ((0, 1, 2, 3),), ((0, 1, 2, 3),), ((0, 1, 2), (3,)))


def logistic_times(value, argument):
    return value / (1.0 + jnp.exp(-argument))


def tail_kernel(value_ref, gate_ref, out_ref):
    rows = out_ref.shape[0]
    span = pl.ds(value_ref.shape[1] - rows, rows)
    value = value_ref[0, span].astype(jnp.float32)
    gate = gate_ref[0, span].astype(jnp.float32)
    out_ref[...] = logistic_times(value, gate).astype(jnp.bfloat16)


def stack_kernel(*refs):
    for index, ref in enumerate(refs[:-1]):
        refs[-1][index] = ref[...]


def mix_kernel(first_row, rows, pad, tap_count, depth, *refs):
    (value_ref, gate_ref, taps_ref, gain_ref, shift_ref) = refs[:5]
    history_ref = refs[5] if first_row == 0 else None
    (out_ref, mixed, summed, wide_taps) = refs[-4:]
    channels = value_ref.shape[-1]
    groups = channels // LANES
    lead = 0 if history_ref is not None else pad

    for group in range(groups):
        columns = pl.ds(group * LANES, LANES)
        wide_taps[group, :tap_count] = taps_ref[:, columns].astype(jnp.float32)
        if history_ref is not None:
            live = lax.axis_index("sp") > 0
            mixed[group, :pad] = jnp.where(live, history_ref[:, columns].astype(jnp.float32), 0.0)

    gate_rows = 32

    @pl.loop(0, (rows + lead) // gate_rows)
    def _(block):
        base = pl.multiple_of(block * gate_rows, gate_rows)
        for group in range(groups):
            columns = pl.ds(group * LANES, LANES)
            span = pl.ds(base + (first_row - lead), gate_rows)
            value = value_ref[0, span, columns].astype(jnp.float32)
            gate = gate_ref[0, span, columns].astype(jnp.float32)
            mixed[group, pl.ds(base + (pad - lead), gate_rows)] = logistic_times(value, gate)

    offset = pad - (tap_count - 1)
    step_rows = next(count for count in (64, 32) if rows % count == 0)
    tiles = step_rows // 8

    @pl.loop(0, groups)
    def _(group):
        taps = [
            jnp.broadcast_to(wide_taps[group, pl.ds(tap, 1)], (8, LANES)) for tap in range(tap_count)
        ]

        @pl.loop(0, rows // step_rows)
        def _(block):
            base = pl.multiple_of(block * step_rows, step_rows)
            totals = [None] * tiles
            for shift in range(8 * (tiles - 1) + tap_count):
                piece = mixed[group, pl.ds(base + offset + shift, 8)]
                for tile in range(tiles):
                    tap = shift - 8 * tile
                    if 0 <= tap < tap_count:
                        term = piece * taps[tap]
                        totals[tile] = term if totals[tile] is None else totals[tile] + term
                        if tap == tap_count - 1:
                            summed[group, pl.ds(base + 8 * tile, 8)] = totals[tile]

    place = lax.axis_index("dp")
    even = GATHERED[0] + tuple(offset ^ 1 for offset in GATHERED[1])
    odd = GATHERED[1] + tuple(offset ^ 1 for offset in GATHERED[0])
    per_slot = depth // LANES
    norm_rows = 16

    @pl.loop(0, rows // norm_rows)
    def _(block):
        span = pl.ds(pl.multiple_of(block * norm_rows, norm_rows), norm_rows)
        total = summed[0, span]
        for group in range(1, groups):
            total = total + summed[group, span]
        mean = jnp.sum(total, axis=-1, keepdims=True) / channels
        square = None
        for group in range(groups):
            apart = summed[group, span] - mean
            square = apart * apart if square is None else square + apart * apart
        variance = jnp.sum(square, axis=-1, keepdims=True) / channels
        scale = lax.rsqrt(variance + EPSILON)
        for slot in range(len(even)):
            owner = place ^ jnp.where(place % 2 == 0, even[slot], odd[slot])
            for part in range(per_slot):
                group = owner * per_slot + part
                normed = (summed[group, span] - mean) * scale * gain_ref[group] + shift_ref[group]
                active = logistic_times(normed, normed)
                out_ref[slot, span, pl.ds(part * LANES, LANES)] = active.astype(jnp.bfloat16)


def projected(acts, weights):
    total, slot = (None, 0)
    for weight in weights:
        for index in range(weight.shape[0]):
            left = jnp.concatenate([act[slot] for act in acts], 0)
            term = jnp.dot(left, weight[index], preferred_element_type=jnp.float32)
            total = term if total is None else total + term
            slot += 1
    return total.astype(jnp.bfloat16)


def project_kernel(chunks, *refs):
    refs[-1][...] = projected(refs[:chunks], refs[chunks:-1])


def last_kernel(chunks, layers, *refs):
    done = refs[: layers - 1]
    acts, weights = (refs[layers - 1 : layers - 1 + chunks], refs[layers - 1 + chunks : -3])
    out_ref, buf, sem = refs[-3:]
    width = buf.shape[1]
    here = lax.axis_index("sp")
    copies = []
    for step in range(layers):
        if step == layers - 1:
            buf[...] = projected(acts, weights)
        column = pl.ds(pl.multiple_of((here ^ step) * width, width), width)
        copy = pltpu.make_async_copy(
            buf if step == layers - 1 else done[step], out_ref.at[0, :, column], sem.at[step]
        )
        copy.start()
        copies.append(copy)
    for copy in copies:
        copy.wait()


VMEM = pl.BlockSpec(memory_space=pltpu.VMEM)
ANY = pl.BlockSpec(memory_space=pl.ANY)


def kernel_call(body, operands, shape, scratch=(), out_spec=VMEM, flops=0, mib=8):
    return pl.pallas_call(
        body,
        out_shape=jax.ShapeDtypeStruct(shape, jnp.bfloat16),
        in_specs=[VMEM] * len(operands),
        out_specs=out_spec,
        scratch_shapes=list(scratch),
        compiler_params=pltpu.CompilerParams(vmem_limit_bytes=mib << 20),
        cost_estimate=pl.CostEstimate(flops=flops, bytes_accessed=0, transcendentals=0),
    )(*operands)


def square_plane(value_half, gate_half, conv_taps, norm_gain, norm_shift, out_weight):
    tap_count = conv_taps.shape[0]
    tok_rows, channels = value_half.shape[1:]
    layers = lax.axis_size("sp")
    depth, width = out_weight.shape
    pad = -(-(tap_count - 1) // 32) * 32
    chunks = next(count for count in (3, 2, 4, 1) if tok_rows % (32 * count) == 0)
    rows = tok_rows // chunks
    groups = channels // LANES

    tail = kernel_call(tail_kernel, (value_half, gate_half), (pad, channels), mib=4)
    history = lax.ppermute(
        tail, "sp", [(source, (source + 1) % layers) for source in range(layers)]
    )

    gathered = []
    for step in range(layers):
        piece = named(out_weight, "sp", step, step) if step else out_weight
        first = named(piece, "dp", 2, 4)
        second = named(piece, "dp", 4, 2)
        forwarded = named(first, "dp", 4, 2)
        pieces = (piece, first, second, forwarded)
        partner = []
        for members in SWAPS[step]:
            sent = pieces[members[0]][None]
            if len(members) > 1:
                sent = kernel_call(
                    stack_kernel,
                    [pieces[member] for member in members],
                    (len(members), depth, width),
                    mib=4,
                )
            partner.append(named(sent, "dp", 1, 1))
        gathered.append([part[None] for part in pieces] + partner)

    gain, shift = (norm_gain.reshape(groups, 1, LANES), norm_shift.reshape(groups, 1, LANES))
    acts = []
    for chunk in range(chunks):
        first_row = chunk * rows
        operands = [value_half, gate_half, conv_taps, gain, shift]
        if chunk == 0:
            operands.append(history)
        acts.append(
            kernel_call(
                functools.partial(mix_kernel, first_row, rows, pad, tap_count, depth),
                operands,
                (channels // depth, rows, depth),
                (
                    pltpu.VMEM((groups, rows + pad, LANES), jnp.float32),
                    pltpu.VMEM((groups, rows, LANES), jnp.float32),
                    pltpu.VMEM((groups, -(-tap_count // 8) * 8, LANES), jnp.float32),
                ),
                flops=2 * tap_count * rows * channels,
            )
        )

    flops = 2 * tok_rows * channels * width
    done = []
    for step in range(layers - 1):
        done.append(
            kernel_call(
                functools.partial(project_kernel, chunks),
                acts + gathered[step],
                (tok_rows, width),
                flops=flops,
            )
        )
    return kernel_call(
        functools.partial(last_kernel, chunks, layers),
        done + acts + gathered[layers - 1],
        (1, tok_rows, layers * width),
        (pltpu.VMEM((tok_rows, width), jnp.bfloat16), pltpu.SemaphoreType.DMA((layers,))),
        out_spec=ANY,
        flops=flops,
    )


def solution(mesh):
    placed = (P("dp", "sp", None), P("dp", "sp", None), P(), P(), P(), P("dp", "sp"))
    plain = mesh.shape["dp"] != 8 or mesh.shape["sp"] != 4

    def per_device(*operands):
        if plain:
            return general(*operands)
        return square_plane(*operands)

    return jax.shard_map(
        per_device, mesh=mesh, in_specs=placed, out_specs=P("dp", "sp", None), check_vma=False
    )
```

time: 111 us -> 84.3 us (0.76)
  waiting for transfers between devices: 67.3 us -> 36.3 us
  starting transfers between devices: 3.4 us -> 25.9 us
  Pallas kernels: 0 us -> 20.6 us
  other arithmetic: 17.8 us -> 0 us
  between operations: 13.5 us -> 0.24 us
  matrix products: 8.49 us -> 0 us
    all_gather x2 -> x0, waiting for transfers between devices: 64.3 us -> none  [the longest x1 32.3 us: per_device(): row_block = lax.all_gather(out_weight, 'sp', axis=1, tiled=True)]
    ppermute x1 -> x21, waiting for transfers between devices: 2.29 us -> 36.3 us  [the longest x20 29.9 us: swapped(): lax.ppermute(value, axis, [(index, index ^ mask_of(index)) for index in r...]
    ppermute x1 -> x21, starting transfers between devices: 3.36 us -> 25.9 us  [the longest x20 24.7 us: swapped(): lax.ppermute(value, axis, [(index, index ^ mask_of(index)) for index in r...]
    pallas_call x0 -> x12, Pallas kernels: none -> 20.6 us  [kernel_call(): pl.pallas_call(body, out_shape=jax.ShapeDtypeStruct(shape, jnp.bfloat16),...]
    reduce_sum x2 -> x0, other arithmetic: 14.8 us -> none  [the longest x1 14.3 us: per_device(): mean_row = jnp.mean(widened, axis=-1, keepdims=True)]
    dot_general x1 -> x0, matrix products: 8.49 us -> none  [per_device(): jnp.dot(activated, lax.all_gather(row_block, 'dp', axis=0, tiled=True), p...]
    convert_element_type x1 -> x0, other arithmetic: 2.79 us -> none  [per_device(): gated = (value_half[0].astype(jnp.float32) * jax.nn.sigmoid(gate_half[0]....]
  transfers between devices with their start and end apart: 3 -> 21, of which waited for: 3 -> 8; matrix products, arithmetic and copies ran while one was open for 16% -> 0% of each run, Pallas kernels for 0% -> 22%
where the time goes in v1:
time: 84.3 us; the launch traced here: 84.1 us
  waiting for transfers between devices  36.3 us (43%)
  starting transfers between devices  25.9 us (31%)
  Pallas kernels  20.6 us (24%)
  local copies, waits for them, and re-layouts  1.02 us (1%)
    ppermute x20, waiting for transfers between devices, swapped(): lax.ppermute(value, axis, [(index, index ^ mask_of(index)) for index in r...  29.9 us
    ppermute x20, starting transfers between devices, swapped(): lax.ppermute(value, axis, [(index, index ^ mask_of(index)) for index in r...  24.7 us
    pallas_call x12, Pallas kernels, kernel_call(): pl.pallas_call(body, out_shape=jax.ShapeDtypeStruct(shape, jnp.bfloat16),...  20.6 us
    ppermute x1, waiting for transfers between devices, square_plane(): lax.ppermute(tail, 'sp', [(source, (source + 1) % layers) for source in r...  6.44 us
  transfers between devices with their start and end apart: 21, of which 8 were waited for; matrix products, arithmetic and copies ran while one was open for 0% of the time, Pallas kernels for 22%

profile of v1, /device:TPU:0, one launch (start us, length us, event | category | flops | bytes accessed | tf_op | source)
XLA Modules:
  0.0 84.1 jit_solution(13222984460498708200)
XLA Ops:
  0.0 3.1 %collective-permute-start.5 = (bf16[256,512]{1,0:T(8,128)(2,1)}, bf16[256,512]{1,0:T(8,128)(2,1)S(1)}, u32[]{:S(2)}, u32[]{:S(2)}) collective-permute-start(bf16[256,512]{1,0:T(8,128)(2,1)} %refs_0_.7), channel_id=1, source_target_pairs={{0,8},{8,0},{16,24},{24,16},{1,9},{9,1},{17,25},{25,17},{2,10},{10... | collective-permute-start | bytes 786440 | tf_op jit(solution)/shard_map/ppermute | solution.py:17
  3.1 2.6 %collective-permute-start.10 = (bf16[256,512]{1,0:T(8,128)(2,1)}, bf16[256,512]{1,0:T(8,128)(2,1)S(1)}, u32[]{:S(2)}, u32[]{:S(2)}) collective-permute-start(bf16[256,512]{1,0:T(8,128)(2,1)} %refs_0_.7), channel_id=1, source_target_pairs={{0,16},{8,24},{16,0},{24,8},{1,17},{9,25},{17,1},{25,9},{2,18},{10... | collective-permute-start | bytes 786440 | tf_op jit(solution)/shard_map/ppermute | solution.py:17
  5.6 1.5 %collective-permute-start.1 = (bf16[256,512]{1,0:T(8,128)(2,1)}, bf16[256,512]{1,0:T(8,128)(2,1)S(1)}, u32[]{:S(2)}, u32[]{:S(2)}) collective-permute-start(bf16[256,512]{1,0:T(8,128)(2,1)} %refs_0_.7), channel_id=1, source_target_pairs={{0,2},{1,5},{2,0},{3,7},{4,6},{5,1},{6,4},{7,3},{8,10},{9,13},{10,... | collective-permute-start | bytes 786440 | tf_op jit(solution)/shard_map/ppermute | solution.py:17
  7.1 7.9 %collective-permute-done.5.refs_0_ = bf16[256,512]{1,0:T(8,128)(2,1)S(1)} collective-permute-done((bf16[256,512]{1,0:T(8,128)(2,1)}, bf16[256,512]{1,0:T(8,128)(2,1)S(1)}, u32[]{:S(2)}, u32[]{:S(2)}) %collective-permute-start.5) | collective-permute-done | bytes 262176 | tf_op jit(solution)/shard_map/ppermute | solution.py:17
  15.1 1.7 %collective-permute-start.6 = (bf16[256,512]{1,0:T(8,128)(2,1)S(1)}, bf16[256,512]{1,0:T(8,128)(2,1)S(1)}, u32[]{:S(2)}, u32[]{:S(2)}) collective-permute-start(bf16[256,512]{1,0:T(8,128)(2,1)S(1)} %collective-permute-done.5.refs_0_), channel_id=1, source_target_pairs={{0,2},{1,5},{2,0},{3,7},{4,6},{5,1},{6,4},{7,3},{8,10},{9,13},{10,... | collective-permute-start | bytes 786440 | tf_op jit(solution)/shard_map/ppermute | solution.py:17
  16.7 1.5 %collective-permute-start.2 = (bf16[256,512]{1,0:T(8,128)(2,1)}, bf16[256,512]{1,0:T(8,128)(2,1)S(1)}, u32[]{:S(2)}, u32[]{:S(2)}) collective-permute-start(bf16[256,512]{1,0:T(8,128)(2,1)} %refs_0_.7), channel_id=1, source_target_pairs={{0,4},{1,3},{2,6},{3,1},{4,0},{5,7},{6,2},{7,5},{8,12},{9,11},{10,... | collective-permute-start | bytes 786440 | tf_op jit(solution)/shard_map/ppermute | solution.py:17
  18.2 0.9 %collective-permute-start.11 = (bf16[256,512]{1,0:T(8,128)(2,1)S(1)}, bf16[256,512]{1,0:T(8,128)(2,1)S(1)}, u32[]{:S(2)}, u32[]{:S(2)}) collective-permute-start(bf16[256,512]{1,0:T(8,128)(2,1)S(1)} %collective-permute-done.10.refs_0_), channel_id=1, source_target_pairs={{0,2},{1,5},{2,0},{3,7},{4,6},{5,1},{6,4},{7,3},{8,10},{9,13},{10,... | collective-permute-start | bytes 786440 | tf_op jit(solution)/shard_map/ppermute | solution.py:17
  19.1 1.5 %collective-permute-start.3 = (bf16[256,512]{1,0:T(8,128)(2,1)S(1)}, bf16[256,512]{1,0:T(8,128)(2,1)S(1)}, u32[]{:S(2)}, u32[]{:S(2)}) collective-permute-start(bf16[256,512]{1,0:T(8,128)(2,1)S(1)} %collective-permute-done.1.refs_1_), channel_id=1, source_target_pairs={{0,4},{1,3},{2,6},{3,1},{4,0},{5,7},{6,2},{7,5},{8,12},{9,11},{10,... | collective-permute-start | bytes 786440 | tf_op jit(solution)/shard_map/ppermute | solution.py:17
  21.1 3.1 %collective-permute-done.6.refs_1_ = bf16[256,512]{1,0:T(8,128)(2,1)S(1)} collective-permute-done((bf16[256,512]{1,0:T(8,128)(2,1)S(1)}, bf16[256,512]{1,0:T(8,128)(2,1)S(1)}, u32[]{:S(2)}, u32[]{:S(2)}) %collective-permute-start.6) | collective-permute-done | bytes 262176 | tf_op jit(solution)/shard_map/ppermute | solution.py:17
  24.2 1.7 %collective-permute-start.8 = (bf16[256,512]{1,0:T(8,128)(2,1)S(1)}, bf16[256,512]{1,0:T(8,128)(2,1)S(1)}, u32[]{:S(2)}, u32[]{:S(2)}) collective-permute-start(bf16[256,512]{1,0:T(8,128)(2,1)S(1)} %collective-permute-done.6.refs_1_), channel_id=1, source_target_pairs={{0,4},{1,3},{2,6},{3,1},{4,0},{5,7},{6,2},{7,5},{8,12},{9,11},{10,... | collective-permute-start | bytes 786440 | tf_op jit(solution)/shard_map/ppermute | solution.py:17
  25.9 0.8 collective-permute-start.12
  26.7 3.1 %collective-permute-done.11.refs_1_ = bf16[256,512]{1,0:T(8,128)(2,1)S(1)} collective-permute-done((bf16[256,512]{1,0:T(8,128)(2,1)S(1)}, bf16[256,512]{1,0:T(8,128)(2,1)S(1)}, u32[]{:S(2)}, u32[]{:S(2)}) %collective-permute-start.11) | collective-permute-done | bytes 262176 | tf_op jit(solution)/shard_map/ppermute | solution.py:17
  29.9 1.7 %collective-permute-start.13 = (bf16[256,512]{1,0:T(8,128)(2,1)S(1)}, bf16[256,512]{1,0:T(8,128)(2,1)S(1)}, u32[]{:S(2)}, u32[]{:S(2)}) collective-permute-start(bf16[256,512]{1,0:T(8,128)(2,1)S(1)} %collective-permute-done.11.refs_1_), channel_id=1, source_target_pairs={{0,4},{1,3},{2,6},{3,1},{4,0},{5,7},{6,2},{7,5},{8,12},{9,11},{10,... | collective-permute-start | bytes 786440 | tf_op jit(solution)/shard_map/ppermute | solution.py:17
  31.5 2.5 %collective-permute-start.15 = (bf16[256,512]{1,0:T(8,128)(2,1)}, bf16[256,512]{1,0:T(8,128)(2,1)S(1)}, u32[]{:S(2)}, u32[]{:S(2)}) collective-permute-start(bf16[256,512]{1,0:T(8,128)(2,1)} %refs_0_.7), channel_id=1, source_target_pairs={{0,24},{8,16},{16,8},{24,0},{1,25},{9,17},{17,9},{25,1},{2,26},{10... | collective-permute-start | bytes 786440 | tf_op jit(solution)/shard_map/ppermute | solution.py:17
  34.0 1.0 %copy-done.3 = bf16[256,512]{1,0:T(8,128)(2,1)S(1)} copy-done((bf16[256,512]{1,0:T(8,128)(2,1)S(1)}, bf16[256,512]{1,0:T(8,128)(2,1)}, u32[]{:S(2)}) %copy-start.3) | copy-done | bytes 262168
  35.3 0.5 collective-permute-start.9
  35.8 0.7 collective-permute-done.12.refs_2_
  36.6 2.8 %collective-permute-done.13.refs_3_ = bf16[256,512]{1,0:T(8,128)(2,1)S(1)} collective-permute-done((bf16[256,512]{1,0:T(8,128)(2,1)S(1)}, bf16[256,512]{1,0:T(8,128)(2,1)S(1)}, u32[]{:S(2)}, u32[]{:S(2)}) %collective-permute-start.13) | collective-permute-done | bytes 262176 | tf_op jit(solution)/shard_map/ppermute | solution.py:17
  39.4 1.2 %collective-permute-start.14 = (bf16[4,256,512]{2,1,0:T(8,128)(2,1)S(1)}, bf16[4,256,512]{2,1,0:T(8,128)(2,1)S(1)}, u32[]{:S(2)}, u32[]{:S(2)}) collective-permute-start(bf16[4,256,512]{2,1,0:T(8,128)(2,1)S(1)} %shard_map.72), channel_id=1, source_target_pairs={{0,1},{1,0},{2,3},{3,2},{4,5},{5,4},{6,7},{7,6},{8,9},{9,8},{10,11... | collective-permute-start | bytes 3145736 | tf_op jit(solution)/shard_map/ppermute | solution.py:17
  40.7 1.5 %collective-permute-start.16 = (bf16[256,512]{1,0:T(8,128)(2,1)S(1)}, bf16[256,512]{1,0:T(8,128)(2,1)S(1)}, u32[]{:S(2)}, u32[]{:S(2)}) collective-permute-start(bf16[256,512]{1,0:T(8,128)(2,1)S(1)} %collective-permute-done.15.refs_0_), channel_id=1, source_target_pairs={{0,2},{1,5},{2,0},{3,7},{4,6},{5,1},{6,4},{7,3},{8,10},{9,13},{10,... | collective-permute-start | bytes 786440 | tf_op jit(solution)/shard_map/ppermute | solution.py:17
  42.7 6.7 %collective-permute-done.16.refs_1_ = bf16[256,512]{1,0:T(8,128)(2,1)S(1)} collective-permute-done((bf16[256,512]{1,0:T(8,128)(2,1)S(1)}, bf16[256,512]{1,0:T(8,128)(2,1)S(1)}, u32[]{:S(2)}, u32[]{:S(2)}) %collective-permute-start.16) | collective-permute-done | bytes 262176 | tf_op jit(solution)/shard_map/ppermute | solution.py:17
  49.7 1.3 %collective-permute-start = (bf16[32,2048]{1,0:T(8,128)(2,1)S(1)}, bf16[32,2048]{1,0:T(8,128)(2,1)S(1)}, u32[]{:S(2)}, u32[]{:S(2)}) collective-permute-start(bf16[32,2048]{1,0:T(8,128)(2,1)S(1)} %shard_map.64), channel_id=1, source_target_pairs={{0,8},{8,16},{16,24},{24,0},{1,9},{9,17},{17,25},{25,1},{2,10},{10... | collective-permute-start | bytes 393224 | tf_op jit(solution)/shard_map/ppermute | solution.py:257
  50.9 6.4 %collective-permute-done.refs_5_ = bf16[32,2048]{1,0:T(8,128)(2,1)S(1)} collective-permute-done((bf16[32,2048]{1,0:T(8,128)(2,1)S(1)}, bf16[32,2048]{1,0:T(8,128)(2,1)S(1)}, u32[]{:S(2)}, u32[]{:S(2)}) %collective-permute-start) | collective-permute-done | bytes 131104 | tf_op jit(solution)/shard_map/ppermute | solution.py:257
  57.4 0.9 %collective-permute-start.18 = (bf16[256,512]{1,0:T(8,128)(2,1)S(1)}, bf16[256,512]{1,0:T(8,128)(2,1)S(1)}, u32[]{:S(2)}, u32[]{:S(2)}) collective-permute-start(bf16[256,512]{1,0:T(8,128)(2,1)S(1)} %collective-permute-done.16.refs_1_), channel_id=1, source_target_pairs={{0,4},{1,3},{2,6},{3,1},{4,0},{5,7},{6,2},{7,5},{8,12},{9,11},{10,... | collective-permute-start | bytes 786440 | tf_op jit(solution)/shard_map/ppermute | solution.py:17
  58.2 5.5 %collective-permute-done.18 = bf16[256,512]{1,0:T(8,128)(2,1)S(1)} collective-permute-done((bf16[256,512]{1,0:T(8,128)(2,1)S(1)}, bf16[256,512]{1,0:T(8,128)(2,1)S(1)}, u32[]{:S(2)}, u32[]{:S(2)}) %collective-permute-start.18) | collective-permute-done | bytes 262176 | tf_op jit(solution)/shard_map/ppermute | solution.py:17
  63.8 5.2 %shard_map.66.refs_1_.refs_4_ = bf16[8,128,256]{2,1,0:T(8,128)(2,1)S(1)} custom-call(bf16[1,384,2048]{2,1,0:T(8,128)(2,1)S(1)} %copy-done, bf16[1,384,2048]{2,1,0:T(8,128)(2,1)S(1)} %copy-done.1, bf16[31,2048]{1,0:T(8,128)(2,1)S(1)} %copy-done.2, f32[16,1,128]{2,1,0:T(1,128)S(1)} %bitcast.35, f32[16,1,128]{2,1,0:T(1,128)S(1)} %bitcast.38), custom_call_target="tpu_custom_call" | custom-call | flops 16252928 | tf_op jit(solution)/shard_map/pallas_call | solution.py:235
  68.9 5.2 %shard_map.67.refs_2_.refs_5_ = bf16[8,128,256]{2,1,0:T(8,128)(2,1)S(1)} custom-call(bf16[1,384,2048]{2,1,0:T(8,128)(2,1)S(1)} %copy-done, bf16[1,384,2048]{2,1,0:T(8,128)(2,1)S(1)} %copy-done.1, bf16[31,2048]{1,0:T(8,128)(2,1)S(1)} %copy-done.2, f32[16,1,128]{2,1,0:T(1,128)S(1)} %bitcast.36, f32[16,1,128]{2,1,0:T(1,128)S(1)} %bitcast.39), custom_call_target="tpu_custom_call" | custom-call | flops 16252928 | tf_op jit(solution)/shard_map/pallas_call | solution.py:235
  74.1 5.1 %shard_map.65.refs_0_.refs_3_ = bf16[8,128,256]{2,1,0:T(8,128)(2,1)S(1)} custom-call(bf16[1,384,2048]{2,1,0:T(8,128)(2,1)S(1)} %copy-done, bf16[1,384,2048]{2,1,0:T(8,128)(2,1)S(1)} %copy-done.1, bf16[31,2048]{1,0:T(8,128)(2,1)S(1)} %copy-done.2, f32[16,1,128]{2,1,0:T(1,128)S(1)} %bitcast.37, f32[16,1,128]{2,1,0:T(1,128)S(1)} %bitcast.40, ...), custom_call_target="tpu_custom_call" | custom-call | flops 16252928 | tf_op jit(solution)/shard_map/pallas_call | solution.py:235
  79.2 1.0 %shard_map.69.refs_0_ = bf16[384,512]{1,0:T(8,128)(2,1)S(1)} custom-call(bf16[8,128,256]{2,1,0:T(8,128)(2,1)S(1)} %shard_map.65.refs_0_.refs_3_, bf16[8,128,256]{2,1,0:T(8,128)(2,1)S(1)} %shard_map.66.refs_1_.refs_4_, bf16[8,128,256]{2,1,0:T(8,128)(2,1)S(1)} %shard_map.67.refs_2_.refs_5_, bf16[1,256,512]{2,1,0:T(8,128)(2,1)S(1)} %bitcast.21, ...), custom_call_target="tpu_custom_call" | custom-call | flops 805306368 | tf_op jit(solution)/shard_map/pallas_call | solution.py:235
  80.2 1.0 %shard_map.71.refs_1_ = bf16[384,512]{1,0:T(8,128)(2,1)S(1)} custom-call(bf16[8,128,256]{2,1,0:T(8,128)(2,1)S(1)} %shard_map.65.refs_0_.refs_3_, bf16[8,128,256]{2,1,0:T(8,128)(2,1)S(1)} %shard_map.66.refs_1_.refs_4_, bf16[8,128,256]{2,1,0:T(8,128)(2,1)S(1)} %shard_map.67.refs_2_.refs_5_, bf16[1,256,512]{2,1,0:T(8,128)(2,1)S(1)} %bitcast.23, ...), custom_call_target="tpu_custom_call" | custom-call | flops 805306368 | tf_op jit(solution)/shard_map/pallas_call | solution.py:235
  81.2 1.0 %shard_map.73.refs_2_ = bf16[384,512]{1,0:T(8,128)(2,1)S(1)} custom-call(bf16[8,128,256]{2,1,0:T(8,128)(2,1)S(1)} %shard_map.65.refs_0_.refs_3_, bf16[8,128,256]{2,1,0:T(8,128)(2,1)S(1)} %shard_map.66.refs_1_.refs_4_, bf16[8,128,256]{2,1,0:T(8,128)(2,1)S(1)} %shard_map.67.refs_2_.refs_5_, bf16[1,256,512]{2,1,0:T(8,128)(2,1)S(1)} %bitcast.22, ...), custom_call_target="tpu_custom_call" | custom-call | flops 805306368 | tf_op jit(solution)/shard_map/pallas_call | solution.py:235
  82.2 1.9 %shard_map.75 = bf16[1,384,2048]{2,1,0:T(8,128)(2,1)} custom-call(bf16[384,512]{1,0:T(8,128)(2,1)S(1)} %shard_map.69.refs_0_, bf16[384,512]{1,0:T(8,128)(2,1)S(1)} %shard_map.71.refs_1_, bf16[384,512]{1,0:T(8,128)(2,1)S(1)} %shard_map.73.refs_2_, bf16[8,128,256]{2,1,0:T(8,128)(2,1)S(1)} %shard_map.65.refs_0_.refs_3_, ...), custom_call_target="tpu_custom_call" | custom-call | flops 805306368 | tf_op jit(solution)/shard_map/pallas_call | solution.py:235
  (36 shorter events, 1.6 us)
Async XLA Ops:
  0.0 15.1 %collective-permute-start.5 = (bf16[256,512]{1,0:T(8,128)(2,1)}, bf16[256,512]{1,0:T(8,128)(2,1)S(1)}, u32[]{:S(2)}, u32[]{:S(2)}) collective-permute-start(bf16[256,512]{1,0:T(8,128)(2,1)} %refs_0_.7), channel_id=1, source_target_pairs={{0,8},{8,0},{16,24},{24,16},{1,9},{9,1},{17,25},{25,17},{2,10},{10... | collective-permute-start | bytes 786440 | tf_op jit(solution)/shard_map/ppermute | solution.py:17
  3.1 15.2 %collective-permute-start.10 = (bf16[256,512]{1,0:T(8,128)(2,1)}, bf16[256,512]{1,0:T(8,128)(2,1)S(1)}, u32[]{:S(2)}, u32[]{:S(2)}) collective-permute-start(bf16[256,512]{1,0:T(8,128)(2,1)} %refs_0_.7), channel_id=1, source_target_pairs={{0,16},{8,24},{16,0},{24,8},{1,17},{9,25},{17,1},{25,9},{2,18},{10... | collective-permute-start | bytes 786440 | tf_op jit(solution)/shard_map/ppermute | solution.py:17
  5.6 13.5 %collective-permute-start.1 = (bf16[256,512]{1,0:T(8,128)(2,1)}, bf16[256,512]{1,0:T(8,128)(2,1)S(1)}, u32[]{:S(2)}, u32[]{:S(2)}) collective-permute-start(bf16[256,512]{1,0:T(8,128)(2,1)} %refs_0_.7), channel_id=1, source_target_pairs={{0,2},{1,5},{2,0},{3,7},{4,6},{5,1},{6,4},{7,3},{8,10},{9,13},{10,... | collective-permute-start | bytes 786440 | tf_op jit(solution)/shard_map/ppermute | solution.py:17
  15.1 9.2 %collective-permute-start.6 = (bf16[256,512]{1,0:T(8,128)(2,1)S(1)}, bf16[256,512]{1,0:T(8,128)(2,1)S(1)}, u32[]{:S(2)}, u32[]{:S(2)}) collective-permute-start(bf16[256,512]{1,0:T(8,128)(2,1)S(1)} %collective-permute-done.5.refs_0_), channel_id=1, source_target_pairs={{0,2},{1,5},{2,0},{3,7},{4,6},{5,1},{6,4},{7,3},{8,10},{9,13},{10,... | collective-permute-start | bytes 786440 | tf_op jit(solution)/shard_map/ppermute | solution.py:17
  16.7 9.2 %collective-permute-start.2 = (bf16[256,512]{1,0:T(8,128)(2,1)}, bf16[256,512]{1,0:T(8,128)(2,1)S(1)}, u32[]{:S(2)}, u32[]{:S(2)}) collective-permute-start(bf16[256,512]{1,0:T(8,128)(2,1)} %refs_0_.7), channel_id=1, source_target_pairs={{0,4},{1,3},{2,6},{3,1},{4,0},{5,7},{6,2},{7,5},{8,12},{9,11},{10,... | collective-permute-start | bytes 786440 | tf_op jit(solution)/shard_map/ppermute | solution.py:17
  18.2 11.6 %collective-permute-start.11 = (bf16[256,512]{1,0:T(8,128)(2,1)S(1)}, bf16[256,512]{1,0:T(8,128)(2,1)S(1)}, u32[]{:S(2)}, u32[]{:S(2)}) collective-permute-start(bf16[256,512]{1,0:T(8,128)(2,1)S(1)} %collective-permute-done.10.refs_0_), channel_id=1, source_target_pairs={{0,2},{1,5},{2,0},{3,7},{4,6},{5,1},{6,4},{7,3},{8,10},{9,13},{10,... | collective-permute-start | bytes 786440 | tf_op jit(solution)/shard_map/ppermute | solution.py:17
  19.1 12.4 %collective-permute-start.3 = (bf16[256,512]{1,0:T(8,128)(2,1)S(1)}, bf16[256,512]{1,0:T(8,128)(2,1)S(1)}, u32[]{:S(2)}, u32[]{:S(2)}) collective-permute-start(bf16[256,512]{1,0:T(8,128)(2,1)S(1)} %collective-permute-done.1.refs_1_), channel_id=1, source_target_pairs={{0,4},{1,3},{2,6},{3,1},{4,0},{5,7},{6,2},{7,5},{8,12},{9,11},{10,... | collective-permute-start | bytes 786440 | tf_op jit(solution)/shard_map/ppermute | solution.py:17
  20.6 14.5 %collective-permute-start.7 = (bf16[256,512]{1,0:T(8,128)(2,1)S(1)}, bf16[256,512]{1,0:T(8,128)(2,1)S(1)}, u32[]{:S(2)}, u32[]{:S(2)}) collective-permute-start(bf16[256,512]{1,0:T(8,128)(2,1)S(1)} %collective-permute-done.5.refs_0_), channel_id=1, source_target_pairs={{0,4},{1,3},{2,6},{3,1},{4,0},{5,7},{6,2},{7,5},{8,12},{9,11},{10,... | collective-permute-start | bytes 786440 | tf_op jit(solution)/shard_map/ppermute | solution.py:17
  24.2 10.9 %collective-permute-start.8 = (bf16[256,512]{1,0:T(8,128)(2,1)S(1)}, bf16[256,512]{1,0:T(8,128)(2,1)S(1)}, u32[]{:S(2)}, u32[]{:S(2)}) collective-permute-start(bf16[256,512]{1,0:T(8,128)(2,1)S(1)} %collective-permute-done.6.refs_1_), channel_id=1, source_target_pairs={{0,4},{1,3},{2,6},{3,1},{4,0},{5,7},{6,2},{7,5},{8,12},{9,11},{10,... | collective-permute-start | bytes 786440 | tf_op jit(solution)/shard_map/ppermute | solution.py:17
  25.9 10.6 %collective-permute-start.12 = (bf16[256,512]{1,0:T(8,128)(2,1)S(1)}, bf16[256,512]{1,0:T(8,128)(2,1)S(1)}, u32[]{:S(2)}, u32[]{:S(2)}) collective-permute-start(bf16[256,512]{1,0:T(8,128)(2,1)S(1)} %collective-permute-done.10.refs_0_), channel_id=1, source_target_pairs={{0,4},{1,3},{2,6},{3,1},{4,0},{5,7},{6,2},{7,5},{8,12},{9,11},{10,... | collective-permute-start | bytes 786440 | tf_op jit(solution)/shard_map/ppermute | solution.py:17
  29.9 9.5 %collective-permute-start.13 = (bf16[256,512]{1,0:T(8,128)(2,1)S(1)}, bf16[256,512]{1,0:T(8,128)(2,1)S(1)}, u32[]{:S(2)}, u32[]{:S(2)}) collective-permute-start(bf16[256,512]{1,0:T(8,128)(2,1)S(1)} %collective-permute-done.11.refs_1_), channel_id=1, source_target_pairs={{0,4},{1,3},{2,6},{3,1},{4,0},{5,7},{6,2},{7,5},{8,12},{9,11},{10,... | collective-permute-start | bytes 786440 | tf_op jit(solution)/shard_map/ppermute | solution.py:17
  31.5 9.1 %collective-permute-start.15 = (bf16[256,512]{1,0:T(8,128)(2,1)}, bf16[256,512]{1,0:T(8,128)(2,1)S(1)}, u32[]{:S(2)}, u32[]{:S(2)}) collective-permute-start(bf16[256,512]{1,0:T(8,128)(2,1)} %refs_0_.7), channel_id=1, source_target_pairs={{0,24},{8,16},{16,8},{24,0},{1,25},{9,17},{17,9},{25,1},{2,26},{10... | collective-permute-start | bytes 786440 | tf_op jit(solution)/shard_map/ppermute | solution.py:17
  34.0 1.0 %copy-start.3 = (bf16[256,512]{1,0:T(8,128)(2,1)S(1)}, bf16[256,512]{1,0:T(8,128)(2,1)}, u32[]{:S(2)}) copy-start(bf16[256,512]{1,0:T(8,128)(2,1)} %refs_0_.7) | copy-start | bytes 786436
  35.1 44.1 %collective-permute-start.4 = (bf16[4,256,512]{2,1,0:T(8,128)(2,1)S(1)}, bf16[4,256,512]{2,1,0:T(8,128)(2,1)S(1)}, u32[]{:S(2)}, u32[]{:S(2)}) collective-permute-start(bf16[4,256,512]{2,1,0:T(8,128)(2,1)S(1)} %shard_map.68), channel_id=1, source_target_pairs={{0,1},{1,0},{2,3},{3,2},{4,5},{5,4},{6,7},{7,6},{8,9},{9,8},{10,11... | collective-permute-start | bytes 3145736 | tf_op jit(solution)/shard_map/ppermute | solution.py:17
  35.3 14.3 %copy-start = (bf16[1,384,2048]{2,1,0:T(8,128)(2,1)S(1)}, bf16[1,384,2048]{2,1,0:T(8,128)(2,1)}, u32[]{:S(2)}) copy-start(bf16[1,384,2048]{2,1,0:T(8,128)(2,1)} %refs_0_.6) | copy-start | bytes 4718596
  35.3 14.3 %copy-start.1 = (bf16[1,384,2048]{2,1,0:T(8,128)(2,1)S(1)}, bf16[1,384,2048]{2,1,0:T(8,128)(2,1)}, u32[]{:S(2)}) copy-start(bf16[1,384,2048]{2,1,0:T(8,128)(2,1)} %refs_1_.5) | copy-start | bytes 4718596
  35.3 44.9 %collective-permute-start.9 = (bf16[4,256,512]{2,1,0:T(8,128)(2,1)S(1)}, bf16[4,256,512]{2,1,0:T(8,128)(2,1)S(1)}, u32[]{:S(2)}, u32[]{:S(2)}) collective-permute-start(bf16[4,256,512]{2,1,0:T(8,128)(2,1)S(1)} %shard_map.70), channel_id=1, source_target_pairs={{0,1},{1,0},{2,3},{3,2},{4,5},{5,4},{6,7},{7,6},{8,9},{9,8},{10,11... | collective-permute-start | bytes 3145736 | tf_op jit(solution)/shard_map/ppermute | solution.py:17
  39.4 41.7 %collective-permute-start.14 = (bf16[4,256,512]{2,1,0:T(8,128)(2,1)S(1)}, bf16[4,256,512]{2,1,0:T(8,128)(2,1)S(1)}, u32[]{:S(2)}, u32[]{:S(2)}) collective-permute-start(bf16[4,256,512]{2,1,0:T(8,128)(2,1)S(1)} %shard_map.72), channel_id=1, source_target_pairs={{0,1},{1,0},{2,3},{3,2},{4,5},{5,4},{6,7},{7,6},{8,9},{9,8},{10,11... | collective-permute-start | bytes 3145736 | tf_op jit(solution)/shard_map/ppermute | solution.py:17
  40.7 8.7 %collective-permute-start.16 = (bf16[256,512]{1,0:T(8,128)(2,1)S(1)}, bf16[256,512]{1,0:T(8,128)(2,1)S(1)}, u32[]{:S(2)}, u32[]{:S(2)}) collective-permute-start(bf16[256,512]{1,0:T(8,128)(2,1)S(1)} %collective-permute-done.15.refs_0_), channel_id=1, source_target_pairs={{0,2},{1,5},{2,0},{3,7},{4,6},{5,1},{6,4},{7,3},{8,10},{9,13},{10,... | collective-permute-start | bytes 786440 | tf_op jit(solution)/shard_map/ppermute | solution.py:17
  42.2 7.2 %collective-permute-start.17 = (bf16[256,512]{1,0:T(8,128)(2,1)S(1)}, bf16[256,512]{1,0:T(8,128)(2,1)S(1)}, u32[]{:S(2)}, u32[]{:S(2)}) collective-permute-start(bf16[256,512]{1,0:T(8,128)(2,1)S(1)} %collective-permute-done.15.refs_0_), channel_id=1, source_target_pairs={{0,4},{1,3},{2,6},{3,1},{4,0},{5,7},{6,2},{7,5},{8,12},{9,11},{10,... | collective-permute-start | bytes 786440 | tf_op jit(solution)/shard_map/ppermute | solution.py:17
  49.4 14.3 %copy-start.2 = (bf16[31,2048]{1,0:T(8,128)(2,1)S(1)}, bf16[31,2048]{1,0:T(8,128)(2,1)}, u32[]{:S(2)}) copy-start(bf16[31,2048]{1,0:T(8,128)(2,1)} %refs_2_.5) | copy-start | bytes 380932
  49.4 14.3 %copy-start.5 = (f32[2048]{0:T(1024)S(1)}, f32[2048]{0:T(1024)}, u32[]{:S(2)}) copy-start(f32[2048]{0:T(1024)} %param.9) | copy-start | bytes 24580
  49.5 14.3 %copy-start.6 = (f32[2048]{0:T(1024)S(1)}, f32[2048]{0:T(1024)}, u32[]{:S(2)}) copy-start(f32[2048]{0:T(1024)} %param.10) | copy-start | bytes 24580
  49.5 32.7 %collective-permute-start.19 = (bf16[3,256,512]{2,1,0:T(8,128)(2,1)S(1)}, bf16[3,256,512]{2,1,0:T(8,128)(2,1)S(1)}, u32[]{:S(2)}, u32[]{:S(2)}) collective-permute-start(bf16[3,256,512]{2,1,0:T(8,128)(2,1)S(1)} %shard_map.74), channel_id=1, source_target_pairs={{0,1},{1,0},{2,3},{3,2},{4,5},{5,4},{6,7},{7,6},{8,9},{9,8},{10,11... | collective-permute-start | bytes 2359304 | tf_op jit(solution)/shard_map/ppermute | solution.py:17
  49.7 7.7 %collective-permute-start = (bf16[32,2048]{1,0:T(8,128)(2,1)S(1)}, bf16[32,2048]{1,0:T(8,128)(2,1)S(1)}, u32[]{:S(2)}, u32[]{:S(2)}) collective-permute-start(bf16[32,2048]{1,0:T(8,128)(2,1)S(1)} %shard_map.64), channel_id=1, source_target_pairs={{0,8},{8,16},{16,24},{24,0},{1,9},{9,17},{17,25},{25,1},{2,10},{10... | collective-permute-start | bytes 393224 | tf_op jit(solution)/shard_map/ppermute | solution.py:257
  57.4 6.4 %collective-permute-start.18 = (bf16[256,512]{1,0:T(8,128)(2,1)S(1)}, bf16[256,512]{1,0:T(8,128)(2,1)S(1)}, u32[]{:S(2)}, u32[]{:S(2)}) collective-permute-start(bf16[256,512]{1,0:T(8,128)(2,1)S(1)} %collective-permute-done.16.refs_1_), channel_id=1, source_target_pairs={{0,4},{1,3},{2,6},{3,1},{4,0},{5,7},{6,2},{7,5},{8,12},{9,11},{10,... | collective-permute-start | bytes 786440 | tf_op jit(solution)/shard_map/ppermute | solution.py:17
  63.8 18.4 %collective-permute-start.20 = (bf16[1,256,512]{2,1,0:T(8,128)(2,1)S(1)}, bf16[1,256,512]{2,1,0:T(8,128)(2,1)S(1)}, u32[]{:S(2)}, u32[]{:S(2)}) collective-permute-start(bf16[1,256,512]{2,1,0:T(8,128)(2,1)S(1)} %bitcast.33), channel_id=1, source_target_pairs={{0,1},{1,0},{2,3},{3,2},{4,5},{5,4},{6,7},{7,6},{8,9},{9,8},{10,11... | collective-permute-start | bytes 786440 | tf_op jit(solution)/shard_map/ppermute | solution.py:17
  74.1 5.1 %copy-start.4 = (bf16[256,512]{1,0:T(8,128)(2,1)S(1)}, bf16[256,512]{1,0:T(8,128)(2,1)}, u32[]{:S(2)}) copy-start(bf16[256,512]{1,0:T(8,128)(2,1)} %refs_0_.7) | copy-start | bytes 786436

commit v2 on v1

v2 whole, which is shorter than its diff:
```python
import functools

import jax
import jax.numpy as jnp
from jax import lax
from jax.experimental import pallas as pl
from jax.experimental.pallas import tpu as pltpu
from jax.sharding import PartitionSpec as P


EPSILON = 1e-06
LANES = 128


def swapped(value, axis, mask_of):
    count = lax.axis_size(axis)
    return lax.ppermute(value, axis, [(index, index ^ mask_of(index)) for index in range(count)])


def named(value, axis, even, odd):
    return swapped(value, axis, lambda index: odd if index & 1 else even)


def passed_along(value, axis, steps):
    count = lax.axis_size(axis)
    initial, last = (max(0, -steps), min(count, count - steps))
    return lax.ppermute(value, axis, [(source, source + steps) for source in range(initial, last)])


def plane_gather(piece, axis):
    count = lax.axis_size(axis)
    masks = [1 << bit for bit in range(1, (count - 1).bit_length())]
    held = piece[None]
    for even, odd in zip(masks, masks[::-1]):
        other = swapped(held, axis, lambda index: odd if index & 1 else even)
        held = jnp.concatenate([held, other], 0)
    return jnp.concatenate([held, swapped(held, axis, lambda index: 1)], 0)


def slot_offsets(count):
    masks = [1 << bit for bit in range(1, (count - 1).bit_length())]
    halves = []
    for order in (masks, masks[::-1]):
        held = [0]
        for mask in order:
            held = held + [offset ^ mask for offset in held]
        halves.append(held)
    return [halves[parity] + [offset ^ 1 for offset in halves[1 - parity]] for parity in range(2)]


def general(value_half, gate_half, conv_taps, norm_gain, norm_shift, out_weight):
    tap_count, tok_rows = (conv_taps.shape[0], value_half.shape[1])
    layers, blocks = (lax.axis_size("sp"), lax.axis_size("dp"))
    here, place = (lax.axis_index("sp"), lax.axis_index("dp"))
    depth, width = out_weight.shape
    gathered = [
        plane_gather(swapped(out_weight, "sp", lambda index: step) if step else out_weight, "dp")
        for step in range(layers)
    ]
    gated = (
        value_half[0].astype(jnp.float32) * jax.nn.sigmoid(gate_half[0].astype(jnp.float32))
    ).astype(jnp.bfloat16)
    history = passed_along(gated[tok_rows - (tap_count - 1) :], "sp", 1)
    padded = jnp.concatenate([history, gated], 0)
    running = jnp.zeros(gated.shape, jnp.float32)
    for tap_index in range(tap_count):
        running = running + padded[tap_index : tap_index + tok_rows].astype(jnp.float32) * conv_taps[
            tap_index
        ].astype(jnp.float32)
    widened = running.astype(jnp.bfloat16).astype(jnp.float32)
    centered = widened - jnp.mean(widened, axis=-1, keepdims=True)
    variance = jnp.mean(centered * centered, axis=-1, keepdims=True)
    normed = centered * lax.rsqrt(variance + EPSILON) * norm_gain + norm_shift
    activated = jax.nn.silu(normed).astype(jnp.bfloat16)
    even, odd = slot_offsets(blocks)
    offsets = jnp.where(place % 2 == 0, jnp.array(even), jnp.array(odd))
    ordered = jnp.concatenate(
        [
            lax.dynamic_slice_in_dim(activated, (place ^ offsets[slot]) * depth, depth, 1)
            for slot in range(blocks)
        ],
        1,
    )
    out = jnp.zeros((tok_rows, layers * width), jnp.bfloat16)
    for step in range(layers):
        part = jnp.dot(
            ordered,
            gathered[step].reshape(blocks * depth, width),
            preferred_element_type=jnp.float32,
        ).astype(jnp.bfloat16)
        out = lax.dynamic_update_slice_in_dim(out, part, (here ^ step) * width, 1)
    return out[None]


GATHERED = ((0, 2, 4, 6), (0, 4, 2, 6))


def logistic_times(value, argument):
    return value / (1.0 + jnp.exp(-argument))


def blank_kernel(out_ref):
    out_ref[...] = jnp.zeros_like(out_ref)


def gate_kernel(pad, tap_count, *refs):
    (value_ref, gate_ref, taps_ref) = refs[:3]
    (mixed, tail_ref, wide_taps) = refs[-3:]
    (rows, channels) = value_ref.shape[1:]
    groups = channels // LANES
    gate_rows = 32

    @pl.loop(0, rows // gate_rows)
    def _(block):
        span = pl.ds(pl.multiple_of(block * gate_rows, gate_rows), gate_rows)
        for group in range(groups):
            columns = pl.ds(group * LANES, LANES)
            value = value_ref[0, span, columns].astype(jnp.float32)
            gate = gate_ref[0, span, columns].astype(jnp.float32)
            gated = logistic_times(value, gate).astype(jnp.bfloat16)
            mixed[group, span] = gated.astype(jnp.float32)

    for group in range(groups):
        columns = pl.ds(group * LANES, LANES)
        tail_ref[:, columns] = mixed[group, pl.ds(rows - pad, pad)].astype(jnp.bfloat16)
    for group in range(groups):
        wide_taps[group, :tap_count] = taps_ref[:, pl.ds(group * LANES, LANES)].astype(jnp.float32)


def stack_kernel(*refs):
    for index, ref in enumerate(refs[:-1]):
        refs[-1][index] = ref[...]


def mix_kernel(first_row, rows, pad, tap_count, depth, *refs):
    (mixed, wide_taps, gain_ref, shift_ref) = refs[:4]
    if first_row == 0:
        (history_ref, out_ref, summed, total, scale_ref, shown) = refs[4:]
    else:
        (out_ref, summed, total, scale_ref) = refs[4:]
        shown = mixed
    groups = mixed.shape[0]
    channels = groups * LANES
    if first_row == 0:
        live = lax.axis_index("sp") > 0
        for group in range(groups):
            columns = pl.ds(group * LANES, LANES)
            shown[group, :pad] = jnp.where(live, history_ref[:, columns].astype(jnp.float32), 0.0)
            shown[group, pl.ds(pad, rows)] = mixed[group, :rows]
    offset = (pad if first_row == 0 else first_row) - (tap_count - 1)
    tiles = rows // 8
    total[...] = jnp.zeros_like(total)

    @pl.loop(0, groups)
    def _(group):
        taps = [
            jnp.broadcast_to(wide_taps[group, pl.ds(tap, 1)], (8, LANES)) for tap in range(tap_count)
        ]
        totals = [None] * tiles
        for shift in range(8 * (tiles - 1) + tap_count):
            piece = shown[group, pl.ds(offset + shift, 8)]
            for tile in range(tiles):
                tap = shift - 8 * tile
                if 0 <= tap < tap_count:
                    term = piece * taps[tap]
                    totals[tile] = term if totals[tile] is None else totals[tile] + term
                    if tap == tap_count - 1:
                        rounded = totals[tile].astype(jnp.bfloat16).astype(jnp.float32)
                        summed[group, pl.ds(8 * tile, 8)] = rounded
                        total[pl.ds(8 * tile, 8)] += rounded

    mean = jnp.sum(total[...], axis=-1, keepdims=True) / channels
    total[...] = jnp.broadcast_to(mean, total.shape)
    norm_rows = 16

    @pl.loop(0, rows // norm_rows)
    def _(block):
        span = pl.ds(pl.multiple_of(block * norm_rows, norm_rows), norm_rows)
        square = None
        for group in range(groups):
            apart = summed[group, span] - total[span]
            square = apart * apart if square is None else square + apart * apart
        scale_ref[span] = square

    variance = jnp.sum(scale_ref[...], axis=-1, keepdims=True) / channels
    scale_ref[...] = jnp.broadcast_to(lax.rsqrt(variance + EPSILON), scale_ref.shape)

    place = lax.axis_index("dp")
    even = GATHERED[0] + tuple(offset ^ 1 for offset in GATHERED[1])
    odd = GATHERED[1] + tuple(offset ^ 1 for offset in GATHERED[0])
    per_slot = depth // LANES

    @pl.loop(0, rows // norm_rows)
    def _(block):
        span = pl.ds(pl.multiple_of(block * norm_rows, norm_rows), norm_rows)
        for slot in range(len(even)):
            owner = place ^ jnp.where(place % 2 == 0, even[slot], odd[slot])
            for part in range(per_slot):
                group = owner * per_slot + part
                normed = (summed[group, span] - total[span]) * scale_ref[span]
                normed = normed * gain_ref[group] + shift_ref[group]
                active = logistic_times(normed, normed)
                out_ref[slot, span, pl.ds(part * LANES, LANES)] = active.astype(jnp.bfloat16)


def projected(acts, weights, slots):
    total = None
    for weight, places in zip(weights, slots, strict=True):
        for index, slot in enumerate(places):
            left = jnp.concatenate([act[slot] for act in acts], 0)
            term = jnp.dot(left, weight[index], preferred_element_type=jnp.float32)
            total = term if total is None else total + term
    return total


def project_kernel(chunks, slots, *refs):
    refs[-1][...] = projected(refs[:chunks], refs[chunks:-1], slots).astype(refs[-1].dtype)


def last_kernel(chunks, slots, *refs):
    (begun, done) = (refs[0], refs[1:4])
    (acts, weights) = (refs[4 : 4 + chunks], refs[4 + chunks : -3])
    (out_ref, buf, sem) = refs[-3:]
    width = buf.shape[1]
    (here, parity) = (lax.axis_index("sp"), lax.axis_index("dp") % 2)
    copies = []
    for index, step in enumerate((0, 1 + parity, 2 - parity, 3)):
        if index == len(done):
            buf[...] = (begun[...] + projected(acts, weights, slots)).astype(buf.dtype)
        column = pl.ds(pl.multiple_of((here ^ step) * width, width), width)
        source = buf if index == len(done) else done[index]
        copy = pltpu.make_async_copy(source, out_ref.at[0, :, column], sem.at[index])
        copy.start()
        copies.append(copy)
    for copy in copies:
        copy.wait()


VMEM = pl.BlockSpec(memory_space=pltpu.VMEM)
ANY = pl.BlockSpec(memory_space=pl.ANY)


HBM = pl.BlockSpec(memory_space=pltpu.HBM)


def kernel_call(body, operands, outs, scratch=(), out_spec=VMEM, flops=0, mib=8, hbm=0):
    outs = [jax.ShapeDtypeStruct(out, jnp.bfloat16) if isinstance(out, tuple) else out for out in outs]
    results = pl.pallas_call(
        body,
        out_shape=outs,
        in_specs=[HBM] * hbm + [VMEM] * (len(operands) - hbm),
        out_specs=[out_spec] * len(outs),
        scratch_shapes=list(scratch),
        compiler_params=pltpu.CompilerParams(vmem_limit_bytes=mib << 20),
        cost_estimate=pl.CostEstimate(flops=flops, bytes_accessed=0, transcendentals=0),
    )(*operands)
    return results if len(outs) > 1 else results[0]


def square_plane(value_half, gate_half, conv_taps, norm_gain, norm_shift, out_weight):
    tap_count = conv_taps.shape[0]
    tok_rows, channels = value_half.shape[1:]
    layers = lax.axis_size("sp")
    depth, width = out_weight.shape
    pad = -(-(tap_count - 1) // 32) * 32
    rows = next(count for count in (64, 64, 32) if tok_rows % count == 0)
    chunks = tok_rows // rows
    groups = channels // LANES

    gain, shift = (norm_gain.reshape(groups, 1, LANES), norm_shift.reshape(groups, 1, LANES))
    blank = kernel_call(blank_kernel, (), [(16, LANES)], flops=1 << 36)
    mixed, tail, taps = kernel_call(
        functools.partial(gate_kernel, pad, tap_count),
        (value_half, gate_half, conv_taps, blank),
        (
            jax.ShapeDtypeStruct((groups, tok_rows, LANES), jnp.float32),
            (pad, channels),
            jax.ShapeDtypeStruct((groups, -(-tap_count // 8) * 8, LANES), jnp.float32),
        ),
        flops=40 * tok_rows * channels,
        mib=8,
    )
    history = lax.ppermute(
        tail, "sp", [(source, (source + 1) % layers) for source in range(layers)]
    )

    def both(pieces):
        stacked = kernel_call(stack_kernel, pieces, [(len(pieces), depth, width)], mib=4)
        return named(stacked, "dp", 1, 1)

    singles = []
    for step in (0, 3):
        if step:
            piece = named(out_weight, "sp", 3, 3)
            partner = named(piece, "dp", 1, 1)
        else:
            piece = out_weight
            partner = own_partner = named(out_weight, "dp", 1, 1)
        first = named(piece, "dp", 2, 4)
        second = named(piece, "dp", 4, 2)
        forwarded = named(first, "dp", 4, 2)
        singles.append((piece, first, second, forwarded, partner))

    chip = kernel_call(stack_kernel, (out_weight, own_partner), [(2, depth, width)], mib=4)
    blocks = lax.axis_size("dp")
    route = [
        (z * blocks + d, (z ^ (2 if d % 2 else 1)) * blocks + d)
        for z in range(layers)
        for d in range(blocks)
    ]
    arrived = lax.ppermute(chip, ("sp", "dp"), route)
    first = named(arrived, "dp", 2, 4)
    second = named(arrived, "dp", 4, 2)
    forwarded = named(first, "dp", 4, 2)
    pairs = (arrived, first, second, forwarded)
    pairs_other = [named(pair, "dp", 1, 1) for pair in pairs]

    acts = []
    for chunk in range(chunks):
        operands = [mixed, taps, gain, shift]
        scratch = [
            pltpu.VMEM((groups, rows, LANES), jnp.float32),
            pltpu.VMEM((rows, LANES), jnp.float32),
            pltpu.VMEM((rows, LANES), jnp.float32),
        ]
        if chunk == 0:
            operands.append(history)
            scratch.append(pltpu.VMEM((groups, rows + pad, LANES), jnp.float32))
        acts.append(
            kernel_call(
                functools.partial(mix_kernel, chunk * rows, rows, pad, tap_count, depth),
                operands,
                [(channels // depth, rows, depth)],
                scratch,
                flops=2 * tap_count * rows * channels,
            )
        )

    def project(weights, slots, dtype=jnp.bfloat16):
        weights = [weight if weight.ndim == 3 else weight[None] for weight in weights]
        return kernel_call(
            functools.partial(project_kernel, chunks, slots),
            acts + weights,
            [jax.ShapeDtypeStruct((tok_rows, width), dtype)],
            flops=2 * tok_rows * depth * width * sum(len(places) for places in slots),
        )

    (piece, first, second, forwarded, partner) = singles[0]
    swapped_0 = both((first, second, forwarded))
    done = [
        project(
            (piece, first, second, forwarded, partner, swapped_0),
            ((0,), (1,), (2,), (3,), (4,), (5, 6, 7)),
        ),
        project(pairs, ((0, 4), (1, 6), (2, 5), (3, 7))),
        project(pairs_other, ((4, 0), (5, 2), (6, 1), (7, 3))),
    ]
    (piece, first, second, forwarded, partner) = singles[1]
    swapped_3 = both((first, second))
    begun = project(
        (piece, first, second, partner, swapped_3), ((0,), (1,), (2,), (4,), (5, 6)), jnp.float32
    )
    last = named(forwarded, "dp", 1, 1)
    return kernel_call(
        functools.partial(last_kernel, chunks, ((3,), (7,))),
        [begun] + done + acts + [forwarded[None], last[None]],
        [(1, tok_rows, layers * width)],
        (pltpu.VMEM((tok_rows, width), jnp.bfloat16), pltpu.SemaphoreType.DMA((layers,))),
        out_spec=ANY,
        flops=4 * tok_rows * depth * width,
    )


def solution(mesh):
    placed = (P("dp", "sp", None), P("dp", "sp", None), P(), P(), P(), P("dp", "sp"))
    plain = mesh.shape["dp"] != 8 or mesh.shape["sp"] != 4

    def per_device(*operands):
        if plain:
            return general(*operands)
        return square_plane(*operands)

    return jax.shard_map(
        per_device, mesh=mesh, in_specs=placed, out_specs=P("dp", "sp", None), check_vma=False
    )
```

time: 84.3 us -> 78.6 us (0.932)
  starting transfers between devices: 25.9 us -> 20.8 us
  local copies, waits for them, and re-layouts: 1.02 us -> 0.03 us
  waiting for transfers between devices: 36.3 us -> 37.2 us
    ppermute x20 -> x19, waiting for transfers between devices: 29.9 us -> 37.2 us  [swapped(): lax.ppermute(value, axis, [(index, index ^ mask_of(index)) for index in r...]
    ppermute x20 -> x19, starting transfers between devices: 24.7 us -> 17.8 us  [swapped(): lax.ppermute(value, axis, [(index, index ^ mask_of(index)) for index in r...]
    ppermute x1, waiting for transfers between devices: 6.44 us -> 0.01 us  [square_plane(): lax.ppermute(tail, 'sp', [(source, (source + 1) % layers) for source in r...]
    ppermute x0 -> x1, starting transfers between devices: none -> 3 us  [square_plane(): arrived = lax.ppermute(chip, ('sp', 'dp'), route)]
    ppermute x1, starting transfers between devices: 1.29 us -> 0.01 us  [square_plane(): lax.ppermute(tail, 'sp', [(source, (source + 1) % layers) for source in r...]
    unnamed x14 -> x10, local copies, waits for them, and re-layouts: 1.02 us -> 0.03 us
    pallas_call x12 -> x16, Pallas kernels: 20.6 us -> 20.1 us  [kernel_call(): pl.pallas_call(body, out_shape=outs, in_specs=[HBM] * hbm + [VMEM] * (len...]
  transfers between devices with their start and end apart: 21 -> 21, of which waited for: 8 -> 6; matrix products, arithmetic and copies ran while one was open for 0% -> 0% of each run, Pallas kernels for 22% -> 23%
where the time goes in v2:
time: 78.6 us; the launch traced here: 78.4 us
  waiting for transfers between devices  37.2 us (47%)
  starting transfers between devices  20.8 us (26%)
  Pallas kernels  20.1 us (26%)
    ppermute x19, waiting for transfers between devices, swapped(): lax.ppermute(value, axis, [(index, index ^ mask_of(index)) for index in r...  37.2 us
    pallas_call x16, Pallas kernels, kernel_call(): pl.pallas_call(body, out_shape=outs, in_specs=[HBM] * hbm + [VMEM] * (len...  20.1 us
    ppermute x19, starting transfers between devices, swapped(): lax.ppermute(value, axis, [(index, index ^ mask_of(index)) for index in r...  17.8 us
    ppermute x1, starting transfers between devices, square_plane(): arrived = lax.ppermute(chip, ('sp', 'dp'), route)  3 us
  transfers between devices with their start and end apart: 21, of which 6 were waited for; matrix products, arithmetic and copies ran while one was open for 0% of the time, Pallas kernels for 23%

profile of v2, /device:TPU:0, one launch (start us, length us, event | category | flops | bytes accessed | tf_op | source)
XLA Modules:
  0.0 78.4 jit_solution(15490510735130771795)
XLA Ops:
  0.5 1.4 %collective-permute-done.9.refs_1_ = bf16[256,512]{1,0:T(8,128)(2,1)S(1)} collective-permute-done((bf16[256,512]{1,0:T(8,128)(2,1)}, bf16[256,512]{1,0:T(8,128)(2,1)S(1)}, u32[]{:S(2)}, u32[]{:S(2)}) %collective-permute-start.9) | collective-permute-done | bytes 262176 | tf_op jit(solution)/shard_map/ppermute | solution.py:17
  1.9 1.0 %shard_map.76 = bf16[2,256,512]{2,1,0:T(8,128)(2,1)S(1)} custom-call(bf16[256,512]{1,0:T(8,128)(2,1)} %refs_0_.3, bf16[256,512]{1,0:T(8,128)(2,1)S(1)} %collective-permute-done.9.refs_1_), custom_call_target="tpu_custom_call" | custom-call | tf_op jit(solution)/shard_map/pallas_call | solution.py:248
  2.9 3.0 %collective-permute-start.11 = (bf16[2,256,512]{2,1,0:T(8,128)(2,1)S(1)}, bf16[2,256,512]{2,1,0:T(8,128)(2,1)S(1)}, u32[]{:S(2)}, u32[]{:S(2)}) collective-permute-start(bf16[2,256,512]{2,1,0:T(8,128)(2,1)S(1)} %shard_map.76), channel_id=1, source_target_pairs={{0,8},{1,17},{2,10},{3,19},{4,12},{5,21},{6,14},{7,23},{8,0},{9,25... | collective-permute-start | bytes 1572872 | tf_op jit(solution)/shard_map/ppermute | solution.py:311
  5.9 2.5 %collective-permute-start.1 = (bf16[256,512]{1,0:T(8,128)(2,1)}, bf16[256,512]{1,0:T(8,128)(2,1)S(1)}, u32[]{:S(2)}, u32[]{:S(2)}) collective-permute-start(bf16[256,512]{1,0:T(8,128)(2,1)} %refs_0_.3), channel_id=1, source_target_pairs={{0,24},{8,16},{16,8},{24,0},{1,25},{9,17},{17,9},{25,1},{2,26},{10... | collective-permute-start | bytes 786440 | tf_op jit(solution)/shard_map/ppermute | solution.py:17
  8.4 1.5 %collective-permute-start.6 = (bf16[256,512]{1,0:T(8,128)(2,1)}, bf16[256,512]{1,0:T(8,128)(2,1)S(1)}, u32[]{:S(2)}, u32[]{:S(2)}) collective-permute-start(bf16[256,512]{1,0:T(8,128)(2,1)} %refs_0_.3), channel_id=1, source_target_pairs={{0,2},{1,5},{2,0},{3,7},{4,6},{5,1},{6,4},{7,3},{8,10},{9,13},{10,... | collective-permute-start | bytes 786440 | tf_op jit(solution)/shard_map/ppermute | solution.py:17
  9.9 1.5 %collective-permute-start.7 = (bf16[256,512]{1,0:T(8,128)(2,1)}, bf16[256,512]{1,0:T(8,128)(2,1)S(1)}, u32[]{:S(2)}, u32[]{:S(2)}) collective-permute-start(bf16[256,512]{1,0:T(8,128)(2,1)} %refs_0_.3), channel_id=1, source_target_pairs={{0,4},{1,3},{2,6},{3,1},{4,0},{5,7},{6,2},{7,5},{8,12},{9,11},{10,... | collective-permute-start | bytes 786440 | tf_op jit(solution)/shard_map/ppermute | solution.py:17
  11.4 14.5 %collective-permute-done.1 = bf16[256,512]{1,0:T(8,128)(2,1)S(1)} collective-permute-done((bf16[256,512]{1,0:T(8,128)(2,1)}, bf16[256,512]{1,0:T(8,128)(2,1)S(1)}, u32[]{:S(2)}, u32[]{:S(2)}) %collective-permute-start.1) | collective-permute-done | bytes 262176 | tf_op jit(solution)/shard_map/ppermute | solution.py:17
  25.8 1.5 %collective-permute-start.2 = (bf16[256,512]{1,0:T(8,128)(2,1)S(1)}, bf16[256,512]{1,0:T(8,128)(2,1)S(1)}, u32[]{:S(2)}, u32[]{:S(2)}) collective-permute-start(bf16[256,512]{1,0:T(8,128)(2,1)S(1)} %collective-permute-done.1), channel_id=1, source_target_pairs={{0,2},{1,5},{2,0},{3,7},{4,6},{5,1},{6,4},{7,3},{8,10},{9,13},{10,... | collective-permute-start | bytes 786440 | tf_op jit(solution)/shard_map/ppermute | solution.py:17
  27.3 1.5 %collective-permute-start.3 = (bf16[256,512]{1,0:T(8,128)(2,1)S(1)}, bf16[256,512]{1,0:T(8,128)(2,1)S(1)}, u32[]{:S(2)}, u32[]{:S(2)}) collective-permute-start(bf16[256,512]{1,0:T(8,128)(2,1)S(1)} %collective-permute-done.1), channel_id=1, source_target_pairs={{0,4},{1,3},{2,6},{3,1},{4,0},{5,7},{6,2},{7,5},{8,12},{9,11},{10,... | collective-permute-start | bytes 786440 | tf_op jit(solution)/shard_map/ppermute | solution.py:17
  28.8 0.5 collective-permute-start.8
  29.4 0.5 collective-permute-start.12
  29.9 1.2 %shard_map.65 = (f32[16,384,128]{2,1,0:T(8,128)S(1)}, bf16[32,2048]{1,0:T(8,128)(2,1)S(1)}, f32[16,32,128]{2,1,0:T(8,128)S(1)}) custom-call(bf16[1,384,2048]{2,1,0:T(8,128)(2,1)S(1)} %copy-done, bf16[1,384,2048]{2,1,0:T(8,128)(2,1)S(1)} %copy-done.1, bf16[31,2048]{1,0:T(8,128)(2,1)S(1)} %copy-done.4, bf16[16,128]{1,0:T(8,128)(2,1)S(1)} %shard_map.64.refs_3_), custom_call_target="tpu_custom_call" | custom-call | flops 31457280 | tf_op jit(solution)/shard_map/pallas_call | solution.py:248
  31.1 3.9 %collective-permute-done.2.refs_0_ = bf16[256,512]{1,0:T(8,128)(2,1)S(1)} collective-permute-done((bf16[256,512]{1,0:T(8,128)(2,1)S(1)}, bf16[256,512]{1,0:T(8,128)(2,1)S(1)}, u32[]{:S(2)}, u32[]{:S(2)}) %collective-permute-start.2) | collective-permute-done | bytes 262176 | tf_op jit(solution)/shard_map/ppermute | solution.py:17
  35.0 1.5 %collective-permute-done.3.refs_1_ = bf16[256,512]{1,0:T(8,128)(2,1)S(1)} collective-permute-done((bf16[256,512]{1,0:T(8,128)(2,1)S(1)}, bf16[256,512]{1,0:T(8,128)(2,1)S(1)}, u32[]{:S(2)}, u32[]{:S(2)}) %collective-permute-start.3) | collective-permute-done | bytes 262176 | tf_op jit(solution)/shard_map/ppermute | solution.py:17
  36.5 2.9 %collective-permute-start.4 = (bf16[256,512]{1,0:T(8,128)(2,1)S(1)}, bf16[256,512]{1,0:T(8,128)(2,1)S(1)}, u32[]{:S(2)}, u32[]{:S(2)}) collective-permute-start(bf16[256,512]{1,0:T(8,128)(2,1)S(1)} %collective-permute-done.1), channel_id=1, source_target_pairs={{0,1},{1,0},{2,3},{3,2},{4,5},{5,4},{6,7},{7,6},{8,9},{9,8},{10,11... | collective-permute-start | bytes 786440 | tf_op jit(solution)/shard_map/ppermute | solution.py:17
  39.5 2.1 %collective-permute-done.8.refs_2_ = bf16[256,512]{1,0:T(8,128)(2,1)S(1)} collective-permute-done((bf16[256,512]{1,0:T(8,128)(2,1)S(1)}, bf16[256,512]{1,0:T(8,128)(2,1)S(1)}, u32[]{:S(2)}, u32[]{:S(2)}) %collective-permute-start.8) | collective-permute-done | bytes 262176 | tf_op jit(solution)/shard_map/ppermute | solution.py:17
  41.6 1.5 %collective-permute-start.13 = (bf16[2,256,512]{2,1,0:T(8,128)(2,1)S(1)}, bf16[2,256,512]{2,1,0:T(8,128)(2,1)S(1)}, u32[]{:S(2)}, u32[]{:S(2)}) collective-permute-start(bf16[2,256,512]{2,1,0:T(8,128)(2,1)S(1)} %collective-permute-done.11.refs_6_), channel_id=1, source_target_pairs={{0,4},{1,3},{2,6},{3,1},{4,0},{5,7},{6,2},{7,5},{8,12},{9,11},{10,... | collective-permute-start | bytes 1572872 | tf_op jit(solution)/shard_map/ppermute | solution.py:17
  43.2 0.5 collective-permute-start.14
  43.8 1.6 %collective-permute-start.19 = (bf16[256,512]{1,0:T(8,128)(2,1)S(1)}, bf16[256,512]{1,0:T(8,128)(2,1)S(1)}, u32[]{:S(2)}, u32[]{:S(2)}) collective-permute-start(bf16[256,512]{1,0:T(8,128)(2,1)S(1)} %collective-permute-done.2.refs_0_), channel_id=1, source_target_pairs={{0,4},{1,3},{2,6},{3,1},{4,0},{5,7},{6,2},{7,5},{8,12},{9,11},{10,... | collective-permute-start | bytes 786440 | tf_op jit(solution)/shard_map/ppermute | solution.py:17
  45.4 13.8 %collective-permute-done.19 = bf16[256,512]{1,0:T(8,128)(2,1)S(1)} collective-permute-done((bf16[256,512]{1,0:T(8,128)(2,1)S(1)}, bf16[256,512]{1,0:T(8,128)(2,1)S(1)}, u32[]{:S(2)}, u32[]{:S(2)}) %collective-permute-start.19) | collective-permute-done | bytes 262176 | tf_op jit(solution)/shard_map/ppermute | solution.py:17
  59.3 0.5 collective-permute-start.16
  60.3 2.0 %shard_map.67.refs_1_.refs_5_ = bf16[8,64,256]{2,1,0:T(8,128)(2,1)S(1)} custom-call(f32[16,384,128]{2,1,0:T(8,128)S(1)} %get-tuple-element.8.refs_0_, f32[16,32,128]{2,1,0:T(8,128)S(1)} %get-tuple-element.9.refs_1_, f32[16,1,128]{2,1,0:T(1,128)S(1)} %bitcast.19, f32[16,1,128]{2,1,0:T(1,128)S(1)} %bitcast.25), custom_call_target="tpu_custom_call" | custom-call | flops 8126464 | tf_op jit(solution)/shard_map/pallas_call | solution.py:248
  62.3 2.0 %shard_map.68.refs_2_.refs_6_ = bf16[8,64,256]{2,1,0:T(8,128)(2,1)S(1)} custom-call(f32[16,384,128]{2,1,0:T(8,128)S(1)} %get-tuple-element.8.refs_0_, f32[16,32,128]{2,1,0:T(8,128)S(1)} %get-tuple-element.9.refs_1_, f32[16,1,128]{2,1,0:T(1,128)S(1)} %bitcast.20, f32[16,1,128]{2,1,0:T(1,128)S(1)} %bitcast.26), custom_call_target="tpu_custom_call" | custom-call | flops 8126464 | tf_op jit(solution)/shard_map/pallas_call | solution.py:248
  64.2 2.0 %shard_map.69.refs_3_.refs_7_ = bf16[8,64,256]{2,1,0:T(8,128)(2,1)S(1)} custom-call(f32[16,384,128]{2,1,0:T(8,128)S(1)} %get-tuple-element.8.refs_0_, f32[16,32,128]{2,1,0:T(8,128)S(1)} %get-tuple-element.9.refs_1_, f32[16,1,128]{2,1,0:T(1,128)S(1)} %bitcast.21, f32[16,1,128]{2,1,0:T(1,128)S(1)} %bitcast.27), custom_call_target="tpu_custom_call" | custom-call | flops 8126464 | tf_op jit(solution)/shard_map/pallas_call | solution.py:248
  66.2 2.0 %shard_map.70.refs_4_.refs_8_ = bf16[8,64,256]{2,1,0:T(8,128)(2,1)S(1)} custom-call(f32[16,384,128]{2,1,0:T(8,128)S(1)} %get-tuple-element.8.refs_0_, f32[16,32,128]{2,1,0:T(8,128)S(1)} %get-tuple-element.9.refs_1_, f32[16,1,128]{2,1,0:T(1,128)S(1)} %bitcast.22, f32[16,1,128]{2,1,0:T(1,128)S(1)} %bitcast.28), custom_call_target="tpu_custom_call" | custom-call | flops 8126464 | tf_op jit(solution)/shard_map/pallas_call | solution.py:248
  68.2 2.0 %shard_map.71.refs_5_.refs_9_ = bf16[8,64,256]{2,1,0:T(8,128)(2,1)S(1)} custom-call(f32[16,384,128]{2,1,0:T(8,128)S(1)} %get-tuple-element.8.refs_0_, f32[16,32,128]{2,1,0:T(8,128)S(1)} %get-tuple-element.9.refs_1_, f32[16,1,128]{2,1,0:T(1,128)S(1)} %bitcast.23, f32[16,1,128]{2,1,0:T(1,128)S(1)} %bitcast.29), custom_call_target="tpu_custom_call" | custom-call | flops 8126464 | tf_op jit(solution)/shard_map/pallas_call | solution.py:248
  70.1 2.1 %shard_map.66.refs_0_.refs_4_ = bf16[8,64,256]{2,1,0:T(8,128)(2,1)S(1)} custom-call(f32[16,384,128]{2,1,0:T(8,128)S(1)} %get-tuple-element.8.refs_0_, f32[16,32,128]{2,1,0:T(8,128)S(1)} %get-tuple-element.9.refs_1_, f32[16,1,128]{2,1,0:T(1,128)S(1)} %bitcast.24, f32[16,1,128]{2,1,0:T(1,128)S(1)} %bitcast.30, bf16[32,2048]{1,0:T(8,128)(2,1)S(1)} %collective-permute-done.refs_4_), custom_call_target="tpu_custom_call" | custom-call | flops 8126464 | tf_op jit(solution)/shard_map/pallas_call | solution.py:248
  72.4 0.8 shard_map.73.refs_0_
  73.2 1.9 %shard_map.75.refs_1_ = bf16[384,512]{1,0:T(8,128)(2,1)S(1)} custom-call(bf16[8,64,256]{2,1,0:T(8,128)(2,1)S(1)} %shard_map.66.refs_0_.refs_4_, bf16[8,64,256]{2,1,0:T(8,128)(2,1)S(1)} %shard_map.67.refs_1_.refs_5_, bf16[8,64,256]{2,1,0:T(8,128)(2,1)S(1)} %shard_map.68.refs_2_.refs_6_, bf16[8,64,256]{2,1,0:T(8,128)(2,1)S(1)} %shard_map.69.refs_3_.refs_7_, ...), custom_call_target="tpu_custom_call" | custom-call | flops 805306368 | tf_op jit(solution)/shard_map/pallas_call | solution.py:248
  75.1 1.0 %shard_map.77.refs_2_ = bf16[384,512]{1,0:T(8,128)(2,1)S(1)} custom-call(bf16[8,64,256]{2,1,0:T(8,128)(2,1)S(1)} %shard_map.66.refs_0_.refs_4_, bf16[8,64,256]{2,1,0:T(8,128)(2,1)S(1)} %shard_map.67.refs_1_.refs_5_, bf16[8,64,256]{2,1,0:T(8,128)(2,1)S(1)} %shard_map.68.refs_2_.refs_6_, bf16[8,64,256]{2,1,0:T(8,128)(2,1)S(1)} %shard_map.69.refs_3_.refs_7_, ...), custom_call_target="tpu_custom_call" | custom-call | flops 805306368 | tf_op jit(solution)/shard_map/pallas_call | solution.py:248
  76.1 1.0 %shard_map.78.refs_3_ = bf16[384,512]{1,0:T(8,128)(2,1)S(1)} custom-call(bf16[8,64,256]{2,1,0:T(8,128)(2,1)S(1)} %shard_map.66.refs_0_.refs_4_, bf16[8,64,256]{2,1,0:T(8,128)(2,1)S(1)} %shard_map.67.refs_1_.refs_5_, bf16[8,64,256]{2,1,0:T(8,128)(2,1)S(1)} %shard_map.68.refs_2_.refs_6_, bf16[8,64,256]{2,1,0:T(8,128)(2,1)S(1)} %shard_map.69.refs_3_.refs_7_, ...), custom_call_target="tpu_custom_call" | custom-call | flops 805306368 | tf_op jit(solution)/shard_map/pallas_call | solution.py:248
  77.1 1.3 %shard_map.79 = bf16[1,384,2048]{2,1,0:T(8,128)(2,1)} custom-call(f32[384,512]{1,0:T(8,128)S(1)} %shard_map.73.refs_0_, bf16[384,512]{1,0:T(8,128)(2,1)S(1)} %shard_map.75.refs_1_, bf16[384,512]{1,0:T(8,128)(2,1)S(1)} %shard_map.77.refs_2_, bf16[384,512]{1,0:T(8,128)(2,1)S(1)} %shard_map.78.refs_3_, bf16[8,64,256]{2,1,0:T(8,128)(2,1)S(1)} %shard_map.66.refs_0_.refs_4_, ...), custom_call_target="tpu_custom_call" | custom-call | flops 201326592 | tf_op jit(solution)/shard_map/pallas_call | solution.py:248
  (36 shorter events, 1.4 us)
Async XLA Ops:
  0.0 1.9 %collective-permute-start.9 = (bf16[256,512]{1,0:T(8,128)(2,1)}, bf16[256,512]{1,0:T(8,128)(2,1)S(1)}, u32[]{:S(2)}, u32[]{:S(2)}) collective-permute-start(bf16[256,512]{1,0:T(8,128)(2,1)} %refs_0_.3), channel_id=1, source_target_pairs={{0,1},{1,0},{2,3},{3,2},{4,5},{5,4},{6,7},{7,6},{8,9},{9,8},{10,11... | collective-permute-start | bytes 786440 | tf_op jit(solution)/shard_map/ppermute | solution.py:17
  2.9 27.0 %copy-start = (bf16[1,384,2048]{2,1,0:T(8,128)(2,1)S(1)}, bf16[1,384,2048]{2,1,0:T(8,128)(2,1)}, u32[]{:S(2)}) copy-start(bf16[1,384,2048]{2,1,0:T(8,128)(2,1)} %refs_0_.2) | copy-start | bytes 4718596
  2.9 27.0 %copy-start.1 = (bf16[1,384,2048]{2,1,0:T(8,128)(2,1)S(1)}, bf16[1,384,2048]{2,1,0:T(8,128)(2,1)}, u32[]{:S(2)}) copy-start(bf16[1,384,2048]{2,1,0:T(8,128)(2,1)} %refs_1_.1) | copy-start | bytes 4718596
  2.9 27.0 %copy-start.4 = (bf16[31,2048]{1,0:T(8,128)(2,1)S(1)}, bf16[31,2048]{1,0:T(8,128)(2,1)}, u32[]{:S(2)}) copy-start(bf16[31,2048]{1,0:T(8,128)(2,1)} %refs_2_.1) | copy-start | bytes 380932
  2.9 26.5 %collective-permute-start.11 = (bf16[2,256,512]{2,1,0:T(8,128)(2,1)S(1)}, bf16[2,256,512]{2,1,0:T(8,128)(2,1)S(1)}, u32[]{:S(2)}, u32[]{:S(2)}) collective-permute-start(bf16[2,256,512]{2,1,0:T(8,128)(2,1)S(1)} %shard_map.76), channel_id=1, source_target_pairs={{0,8},{1,17},{2,10},{3,19},{4,12},{5,21},{6,14},{7,23},{8,0},{9,25... | collective-permute-start | bytes 1572872 | tf_op jit(solution)/shard_map/ppermute | solution.py:311
  5.9 19.9 %collective-permute-start.1 = (bf16[256,512]{1,0:T(8,128)(2,1)}, bf16[256,512]{1,0:T(8,128)(2,1)S(1)}, u32[]{:S(2)}, u32[]{:S(2)}) collective-permute-start(bf16[256,512]{1,0:T(8,128)(2,1)} %refs_0_.3), channel_id=1, source_target_pairs={{0,24},{8,16},{16,8},{24,0},{1,25},{9,17},{17,9},{25,1},{2,26},{10... | collective-permute-start | bytes 786440 | tf_op jit(solution)/shard_map/ppermute | solution.py:17
  8.4 20.5 %collective-permute-start.6 = (bf16[256,512]{1,0:T(8,128)(2,1)}, bf16[256,512]{1,0:T(8,128)(2,1)S(1)}, u32[]{:S(2)}, u32[]{:S(2)}) collective-permute-start(bf16[256,512]{1,0:T(8,128)(2,1)} %refs_0_.3), channel_id=1, source_target_pairs={{0,2},{1,5},{2,0},{3,7},{4,6},{5,1},{6,4},{7,3},{8,10},{9,13},{10,... | collective-permute-start | bytes 786440 | tf_op jit(solution)/shard_map/ppermute | solution.py:17
  9.9 29.6 %collective-permute-start.7 = (bf16[256,512]{1,0:T(8,128)(2,1)}, bf16[256,512]{1,0:T(8,128)(2,1)S(1)}, u32[]{:S(2)}, u32[]{:S(2)}) collective-permute-start(bf16[256,512]{1,0:T(8,128)(2,1)} %refs_0_.3), channel_id=1, source_target_pairs={{0,4},{1,3},{2,6},{3,1},{4,0},{5,7},{6,2},{7,5},{8,12},{9,11},{10,... | collective-permute-start | bytes 786440 | tf_op jit(solution)/shard_map/ppermute | solution.py:17
  25.8 9.2 %collective-permute-start.2 = (bf16[256,512]{1,0:T(8,128)(2,1)S(1)}, bf16[256,512]{1,0:T(8,128)(2,1)S(1)}, u32[]{:S(2)}, u32[]{:S(2)}) collective-permute-start(bf16[256,512]{1,0:T(8,128)(2,1)S(1)} %collective-permute-done.1), channel_id=1, source_target_pairs={{0,2},{1,5},{2,0},{3,7},{4,6},{5,1},{6,4},{7,3},{8,10},{9,13},{10,... | collective-permute-start | bytes 786440 | tf_op jit(solution)/shard_map/ppermute | solution.py:17
  27.3 9.2 %collective-permute-start.3 = (bf16[256,512]{1,0:T(8,128)(2,1)S(1)}, bf16[256,512]{1,0:T(8,128)(2,1)S(1)}, u32[]{:S(2)}, u32[]{:S(2)}) collective-permute-start(bf16[256,512]{1,0:T(8,128)(2,1)S(1)} %collective-permute-done.1), channel_id=1, source_target_pairs={{0,4},{1,3},{2,6},{3,1},{4,0},{5,7},{6,2},{7,5},{8,12},{9,11},{10,... | collective-permute-start | bytes 786440 | tf_op jit(solution)/shard_map/ppermute | solution.py:17
  28.8 12.8 %collective-permute-start.8 = (bf16[256,512]{1,0:T(8,128)(2,1)S(1)}, bf16[256,512]{1,0:T(8,128)(2,1)S(1)}, u32[]{:S(2)}, u32[]{:S(2)}) collective-permute-start(bf16[256,512]{1,0:T(8,128)(2,1)S(1)} %collective-permute-done.6.refs_0_), channel_id=1, source_target_pairs={{0,4},{1,3},{2,6},{3,1},{4,0},{5,7},{6,2},{7,5},{8,12},{9,11},{10,... | collective-permute-start | bytes 786440 | tf_op jit(solution)/shard_map/ppermute | solution.py:17
  29.4 13.8 %collective-permute-start.12 = (bf16[2,256,512]{2,1,0:T(8,128)(2,1)S(1)}, bf16[2,256,512]{2,1,0:T(8,128)(2,1)S(1)}, u32[]{:S(2)}, u32[]{:S(2)}) collective-permute-start(bf16[2,256,512]{2,1,0:T(8,128)(2,1)S(1)} %collective-permute-done.11.refs_6_), channel_id=1, source_target_pairs={{0,2},{1,5},{2,0},{3,7},{4,6},{5,1},{6,4},{7,3},{8,10},{9,13},{10,... | collective-permute-start | bytes 1572872 | tf_op jit(solution)/shard_map/ppermute | solution.py:17
  31.1 29.2 %copy-start.2 = (f32[2048]{0:T(1024)S(1)}, f32[2048]{0:T(1024)}, u32[]{:S(2)}) copy-start(f32[2048]{0:T(1024)} %param.9) | copy-start | bytes 24580
  31.1 29.2 %copy-start.3 = (f32[2048]{0:T(1024)S(1)}, f32[2048]{0:T(1024)}, u32[]{:S(2)}) copy-start(f32[2048]{0:T(1024)} %param.10) | copy-start | bytes 24580
  35.0 8.7 %collective-permute-start = (bf16[32,2048]{1,0:T(8,128)(2,1)S(1)}, bf16[32,2048]{1,0:T(8,128)(2,1)S(1)}, u32[]{:S(2)}, u32[]{:S(2)}) collective-permute-start(bf16[32,2048]{1,0:T(8,128)(2,1)S(1)} %get-tuple-element.10), channel_id=1, source_target_pairs={{0,8},{8,16},{16,24},{24,0},{1,9},{9,17},{17,25},{25,1},{2,10},{10... | collective-permute-start | bytes 393224 | tf_op jit(solution)/shard_map/ppermute | solution.py:283
  36.5 7.3 %collective-permute-start.4 = (bf16[256,512]{1,0:T(8,128)(2,1)S(1)}, bf16[256,512]{1,0:T(8,128)(2,1)S(1)}, u32[]{:S(2)}, u32[]{:S(2)}) collective-permute-start(bf16[256,512]{1,0:T(8,128)(2,1)S(1)} %collective-permute-done.1), channel_id=1, source_target_pairs={{0,1},{1,0},{2,3},{3,2},{4,5},{5,4},{6,7},{7,6},{8,9},{9,8},{10,11... | collective-permute-start | bytes 786440 | tf_op jit(solution)/shard_map/ppermute | solution.py:17
  39.5 19.8 %collective-permute-start.5 = (bf16[2,256,512]{2,1,0:T(8,128)(2,1)S(1)}, bf16[2,256,512]{2,1,0:T(8,128)(2,1)S(1)}, u32[]{:S(2)}, u32[]{:S(2)}) collective-permute-start(bf16[2,256,512]{2,1,0:T(8,128)(2,1)S(1)} %shard_map.72), channel_id=1, source_target_pairs={{0,1},{1,0},{2,3},{3,2},{4,5},{5,4},{6,7},{7,6},{8,9},{9,8},{10,11... | collective-permute-start | bytes 1572872 | tf_op jit(solution)/shard_map/ppermute | solution.py:17
  41.6 18.1 %collective-permute-start.13 = (bf16[2,256,512]{2,1,0:T(8,128)(2,1)S(1)}, bf16[2,256,512]{2,1,0:T(8,128)(2,1)S(1)}, u32[]{:S(2)}, u32[]{:S(2)}) collective-permute-start(bf16[2,256,512]{2,1,0:T(8,128)(2,1)S(1)} %collective-permute-done.11.refs_6_), channel_id=1, source_target_pairs={{0,4},{1,3},{2,6},{3,1},{4,0},{5,7},{6,2},{7,5},{8,12},{9,11},{10,... | collective-permute-start | bytes 1572872 | tf_op jit(solution)/shard_map/ppermute | solution.py:17
  43.2 16.7 %collective-permute-start.14 = (bf16[2,256,512]{2,1,0:T(8,128)(2,1)S(1)}, bf16[2,256,512]{2,1,0:T(8,128)(2,1)S(1)}, u32[]{:S(2)}, u32[]{:S(2)}) collective-permute-start(bf16[2,256,512]{2,1,0:T(8,128)(2,1)S(1)} %collective-permute-done.12.refs_7_), channel_id=1, source_target_pairs={{0,4},{1,3},{2,6},{3,1},{4,0},{5,7},{6,2},{7,5},{8,12},{9,11},{10,... | collective-permute-start | bytes 1572872 | tf_op jit(solution)/shard_map/ppermute | solution.py:17
  43.7 28.5 %collective-permute-start.10 = (bf16[3,256,512]{2,1,0:T(8,128)(2,1)S(1)}, bf16[3,256,512]{2,1,0:T(8,128)(2,1)S(1)}, u32[]{:S(2)}, u32[]{:S(2)}) collective-permute-start(bf16[3,256,512]{2,1,0:T(8,128)(2,1)S(1)} %shard_map.74), channel_id=1, source_target_pairs={{0,1},{1,0},{2,3},{3,2},{4,5},{5,4},{6,7},{7,6},{8,9},{9,8},{10,11... | collective-permute-start | bytes 2359304 | tf_op jit(solution)/shard_map/ppermute | solution.py:17
  43.8 15.4 %collective-permute-start.19 = (bf16[256,512]{1,0:T(8,128)(2,1)S(1)}, bf16[256,512]{1,0:T(8,128)(2,1)S(1)}, u32[]{:S(2)}, u32[]{:S(2)}) collective-permute-start(bf16[256,512]{1,0:T(8,128)(2,1)S(1)} %collective-permute-done.2.refs_0_), channel_id=1, source_target_pairs={{0,4},{1,3},{2,6},{3,1},{4,0},{5,7},{6,2},{7,5},{8,12},{9,11},{10,... | collective-permute-start | bytes 786440 | tf_op jit(solution)/shard_map/ppermute | solution.py:17
  59.2 16.8 %collective-permute-start.15 = (bf16[2,256,512]{2,1,0:T(8,128)(2,1)S(1)}, bf16[2,256,512]{2,1,0:T(8,128)(2,1)S(1)}, u32[]{:S(2)}, u32[]{:S(2)}) collective-permute-start(bf16[2,256,512]{2,1,0:T(8,128)(2,1)S(1)} %collective-permute-done.11.refs_6_), channel_id=1, source_target_pairs={{0,1},{1,0},{2,3},{3,2},{4,5},{5,4},{6,7},{7,6},{8,9},{9,8},{10,11... | collective-permute-start | bytes 1572872 | tf_op jit(solution)/shard_map/ppermute | solution.py:17
  59.3 16.8 %collective-permute-start.16 = (bf16[2,256,512]{2,1,0:T(8,128)(2,1)S(1)}, bf16[2,256,512]{2,1,0:T(8,128)(2,1)S(1)}, u32[]{:S(2)}, u32[]{:S(2)}) collective-permute-start(bf16[2,256,512]{2,1,0:T(8,128)(2,1)S(1)} %collective-permute-done.12.refs_7_), channel_id=1, source_target_pairs={{0,1},{1,0},{2,3},{3,2},{4,5},{5,4},{6,7},{7,6},{8,9},{9,8},{10,11... | collective-permute-start | bytes 1572872 | tf_op jit(solution)/shard_map/ppermute | solution.py:17
  59.8 16.3 %collective-permute-start.17 = (bf16[2,256,512]{2,1,0:T(8,128)(2,1)S(1)}, bf16[2,256,512]{2,1,0:T(8,128)(2,1)S(1)}, u32[]{:S(2)}, u32[]{:S(2)}) collective-permute-start(bf16[2,256,512]{2,1,0:T(8,128)(2,1)S(1)} %collective-permute-done.13.refs_8_), channel_id=1, source_target_pairs={{0,1},{1,0},{2,3},{3,2},{4,5},{5,4},{6,7},{7,6},{8,9},{9,8},{10,11... | collective-permute-start | bytes 1572872 | tf_op jit(solution)/shard_map/ppermute | solution.py:17
  59.8 16.3 %collective-permute-start.18 = (bf16[2,256,512]{2,1,0:T(8,128)(2,1)S(1)}, bf16[2,256,512]{2,1,0:T(8,128)(2,1)S(1)}, u32[]{:S(2)}, u32[]{:S(2)}) collective-permute-start(bf16[2,256,512]{2,1,0:T(8,128)(2,1)S(1)} %collective-permute-done.14.refs_9_), channel_id=1, source_target_pairs={{0,1},{1,0},{2,3},{3,2},{4,5},{5,4},{6,7},{7,6},{8,9},{9,8},{10,11... | collective-permute-start | bytes 1572872 | tf_op jit(solution)/shard_map/ppermute | solution.py:17
  72.3 4.8 %collective-permute-start.20 = (bf16[256,512]{1,0:T(8,128)(2,1)S(1)}, bf16[256,512]{1,0:T(8,128)(2,1)S(1)}, u32[]{:S(2)}, u32[]{:S(2)}) collective-permute-start(bf16[256,512]{1,0:T(8,128)(2,1)S(1)} %collective-permute-done.19), channel_id=1, source_target_pairs={{0,1},{1,0},{2,3},{3,2},{4,5},{5,4},{6,7},{7,6},{8,9},{9,8},{10,11... | collective-permute-start | bytes 786440 | tf_op jit(solution)/shard_map/ppermute | solution.py:17

commit v3 on v2

--- a/solution.py
+++ b/solution.py
@@ -298,7 +298,10 @@
             partner = own_partner = named(out_weight, "dp", 1, 1)
         first = named(piece, "dp", 2, 4)
         second = named(piece, "dp", 4, 2)
-        forwarded = named(first, "dp", 4, 2)
+        if step:
+            forwarded = named(singles[0][3], "sp", step, step)
+        else:
+            forwarded = named(first, "dp", 4, 2)
         singles.append((piece, first, second, forwarded, partner))
 
     chip = kernel_call(stack_kernel, (out_weight, own_partner), [(2, depth, width)], mib=4)
@@ -356,18 +359,16 @@
         project(pairs_other, ((4, 0), (5, 2), (6, 1), (7, 3))),
     ]
     (piece, first, second, forwarded, partner) = singles[1]
+    last = named(forwarded, "dp", 1, 1)
+    begun = project((piece, partner, forwarded, last), ((0,), (4,), (3,), (7,)), jnp.float32)
     swapped_3 = both((first, second))
-    begun = project(
-        (piece, first, second, partner, swapped_3), ((0,), (1,), (2,), (4,), (5, 6)), jnp.float32
-    )
-    last = named(forwarded, "dp", 1, 1)
     return kernel_call(
-        functools.partial(last_kernel, chunks, ((3,), (7,))),
-        [begun] + done + acts + [forwarded[None], last[None]],
+        functools.partial(last_kernel, chunks, ((1,), (2,), (5, 6))),
+        [begun] + done + acts + [first[None], second[None], swapped_3],
         [(1, tok_rows, layers * width)],
         (pltpu.VMEM((tok_rows, width), jnp.bfloat16), pltpu.SemaphoreType.DMA((layers,))),
         out_spec=ANY,
-        flops=4 * tok_rows * depth * width,
+        flops=8 * tok_rows * depth * width,
     )
 
 

time: 78.6 us -> 77.6 us (0.987)
  waiting for transfers between devices: 37.2 us -> 31 us
  starting transfers between devices: 20.8 us -> 26.6 us
  Pallas kernels: 20.1 us -> 18.2 us
  local copies, waits for them, and re-layouts: 0.03 us -> 1.38 us
    ppermute x19, waiting for transfers between devices: 37.2 us -> 29.5 us  [swapped(): lax.ppermute(value, axis, [(index, index ^ mask_of(index)) for index in r...]
    ppermute x1, starting transfers between devices: 0.01 us -> 5.22 us  [square_plane(): lax.ppermute(tail, 'sp', [(source, (source + 1) % layers) for source in r...]
    pallas_call x16, Pallas kernels: 20.1 us -> 18.2 us  [kernel_call(): pl.pallas_call(body, out_shape=outs, in_specs=[HBM] * hbm + [VMEM] * (len...]
    ppermute x19, starting transfers between devices: 17.8 us -> 19.5 us  [swapped(): lax.ppermute(value, axis, [(index, index ^ mask_of(index)) for index in r...]
    ppermute x1, waiting for transfers between devices: 0.01 us -> 1.44 us  [square_plane(): lax.ppermute(tail, 'sp', [(source, (source + 1) % layers) for source in r...]
    unnamed x10 -> x14, local copies, waits for them, and re-layouts: 0.03 us -> 1.38 us
    ppermute x1, starting transfers between devices: 3 us -> 1.86 us  [square_plane(): arrived = lax.ppermute(chip, ('sp', 'dp'), route)]
  transfers between devices with their start and end apart: 21 -> 21, of which waited for: 6 -> 4; matrix products, arithmetic and copies ran while one was open for 0% -> 0% of each run, Pallas kernels for 23% -> 22%
where the time goes in v3:
time: 77.6 us; the launch traced here: 77.4 us
  waiting for transfers between devices  31 us (40%)
  starting transfers between devices  26.6 us (34%)
  Pallas kernels  18.2 us (23%)
  local copies, waits for them, and re-layouts  1.38 us (2%)
    ppermute x19, waiting for transfers between devices, swapped(): lax.ppermute(value, axis, [(index, index ^ mask_of(index)) for index in r...  29.5 us
    ppermute x19, starting transfers between devices, swapped(): lax.ppermute(value, axis, [(index, index ^ mask_of(index)) for index in r...  19.5 us
    pallas_call x16, Pallas kernels, kernel_call(): pl.pallas_call(body, out_shape=outs, in_specs=[HBM] * hbm + [VMEM] * (len...  18.2 us
    ppermute x1, starting transfers between devices, square_plane(): lax.ppermute(tail, 'sp', [(source, (source + 1) % layers) for source in r...  5.22 us
    ppermute x1, starting transfers between devices, square_plane(): arrived = lax.ppermute(chip, ('sp', 'dp'), route)  1.86 us
  transfers between devices with their start and end apart: 21, of which 4 were waited for; matrix products, arithmetic and copies ran while one was open for 0% of the time, Pallas kernels for 22%

profile of v3, /device:TPU:0, one launch (start us, length us, event | category | flops | bytes accessed | tf_op | source)
XLA Modules:
  0.0 77.4 jit_solution(10707095412868881697)
XLA Ops:
  0.0 0.5 collective-permute-start.8
  0.5 2.5 %collective-permute-start.3 = (bf16[256,512]{1,0:T(8,128)(2,1)}, bf16[256,512]{1,0:T(8,128)(2,1)S(1)}, u32[]{:S(2)}, u32[]{:S(2)}) collective-permute-start(bf16[256,512]{1,0:T(8,128)(2,1)} %refs_0_.3), channel_id=1, source_target_pairs={{0,2},{1,5},{2,0},{3,7},{4,6},{5,1},{6,4},{7,3},{8,10},{9,13},{10,... | collective-permute-start | bytes 786440 | tf_op jit(solution)/shard_map/ppermute | solution.py:17
  3.0 1.0 %copy-done.2 = bf16[256,512]{1,0:T(8,128)(2,1)S(1)} copy-done((bf16[256,512]{1,0:T(8,128)(2,1)S(1)}, bf16[256,512]{1,0:T(8,128)(2,1)}, u32[]{:S(2)}) %copy-start.2) | copy-done | bytes 262168
  4.0 1.9 %collective-permute-start.10 = (bf16[2,256,512]{2,1,0:T(8,128)(2,1)S(1)}, bf16[2,256,512]{2,1,0:T(8,128)(2,1)S(1)}, u32[]{:S(2)}, u32[]{:S(2)}) collective-permute-start(bf16[2,256,512]{2,1,0:T(8,128)(2,1)S(1)} %shard_map.75), channel_id=1, source_target_pairs={{0,8},{1,17},{2,10},{3,19},{4,12},{5,21},{6,14},{7,23},{8,0},{9,25... | collective-permute-start | bytes 1572872 | tf_op jit(solution)/shard_map/ppermute | solution.py:314
  5.9 2.5 %collective-permute-start.1 = (bf16[256,512]{1,0:T(8,128)(2,1)S(1)}, bf16[256,512]{1,0:T(8,128)(2,1)S(1)}, u32[]{:S(2)}, u32[]{:S(2)}) collective-permute-start(bf16[256,512]{1,0:T(8,128)(2,1)S(1)} %copy-done.2), channel_id=1, source_target_pairs={{0,24},{8,16},{16,8},{24,0},{1,25},{9,17},{17,9},{25,1},{2,26},{10... | collective-permute-start | bytes 786440 | tf_op jit(solution)/shard_map/ppermute | solution.py:17
  8.3 1.5 %collective-permute-start.7 = (bf16[256,512]{1,0:T(8,128)(2,1)S(1)}, bf16[256,512]{1,0:T(8,128)(2,1)S(1)}, u32[]{:S(2)}, u32[]{:S(2)}) collective-permute-start(bf16[256,512]{1,0:T(8,128)(2,1)S(1)} %copy-done.2), channel_id=1, source_target_pairs={{0,4},{1,3},{2,6},{3,1},{4,0},{5,7},{6,2},{7,5},{8,12},{9,11},{10,... | collective-permute-start | bytes 786440 | tf_op jit(solution)/shard_map/ppermute | solution.py:17
  9.9 0.5 collective-permute-start.4
  10.4 15.4 %collective-permute-done.1 = bf16[256,512]{1,0:T(8,128)(2,1)S(1)} collective-permute-done((bf16[256,512]{1,0:T(8,128)(2,1)S(1)}, bf16[256,512]{1,0:T(8,128)(2,1)S(1)}, u32[]{:S(2)}, u32[]{:S(2)}) %collective-permute-start.1) | collective-permute-done | bytes 262176 | tf_op jit(solution)/shard_map/ppermute | solution.py:17
  25.9 0.6 collective-permute-start.9
  26.5 1.5 %collective-permute-start.11 = (bf16[2,256,512]{2,1,0:T(8,128)(2,1)S(1)}, bf16[2,256,512]{2,1,0:T(8,128)(2,1)S(1)}, u32[]{:S(2)}, u32[]{:S(2)}) collective-permute-start(bf16[2,256,512]{2,1,0:T(8,128)(2,1)S(1)} %collective-permute-done.10.refs_6_), channel_id=1, source_target_pairs={{0,2},{1,5},{2,0},{3,7},{4,6},{5,1},{6,4},{7,3},{8,10},{9,13},{10,... | collective-permute-start | bytes 1572872 | tf_op jit(solution)/shard_map/ppermute | solution.py:17
  28.0 1.2 %shard_map.65 = (f32[16,384,128]{2,1,0:T(8,128)S(1)}, bf16[32,2048]{1,0:T(8,128)(2,1)S(1)}, f32[16,32,128]{2,1,0:T(8,128)S(1)}) custom-call(bf16[1,384,2048]{2,1,0:T(8,128)(2,1)S(1)} %copy-done, bf16[1,384,2048]{2,1,0:T(8,128)(2,1)S(1)} %copy-done.1, bf16[31,2048]{1,0:T(8,128)(2,1)S(1)} %copy-done.6, bf16[16,128]{1,0:T(8,128)(2,1)S(1)} %shard_map.64.refs_3_), custom_call_target="tpu_custom_call" | custom-call | flops 31457280 | tf_op jit(solution)/shard_map/pallas_call | solution.py:248
  29.2 5.2 %collective-permute-start = (bf16[32,2048]{1,0:T(8,128)(2,1)S(1)}, bf16[32,2048]{1,0:T(8,128)(2,1)S(1)}, u32[]{:S(2)}, u32[]{:S(2)}) collective-permute-start(bf16[32,2048]{1,0:T(8,128)(2,1)S(1)} %get-tuple-element.10), channel_id=1, source_target_pairs={{0,8},{8,16},{16,24},{24,0},{1,9},{9,17},{17,25},{25,1},{2,10},{10... | collective-permute-start | bytes 393224 | tf_op jit(solution)/shard_map/ppermute | solution.py:283
  34.4 1.5 %collective-permute-start.18 = (bf16[256,512]{1,0:T(8,128)(2,1)S(1)}, bf16[256,512]{1,0:T(8,128)(2,1)S(1)}, u32[]{:S(2)}, u32[]{:S(2)}) collective-permute-start(bf16[256,512]{1,0:T(8,128)(2,1)S(1)} %collective-permute-done.1), channel_id=1, source_target_pairs={{0,2},{1,5},{2,0},{3,7},{4,6},{5,1},{6,4},{7,3},{8,10},{9,13},{10,... | collective-permute-start | bytes 786440 | tf_op jit(solution)/shard_map/ppermute | solution.py:17
  35.9 1.4 %collective-permute-done.refs_4_ = bf16[32,2048]{1,0:T(8,128)(2,1)S(1)} collective-permute-done((bf16[32,2048]{1,0:T(8,128)(2,1)S(1)}, bf16[32,2048]{1,0:T(8,128)(2,1)S(1)}, u32[]{:S(2)}, u32[]{:S(2)}) %collective-permute-start) | collective-permute-done | bytes 131104 | tf_op jit(solution)/shard_map/ppermute | solution.py:283
  37.3 3.8 %collective-permute-start.5 = (bf16[256,512]{1,0:T(8,128)(2,1)S(1)}, bf16[256,512]{1,0:T(8,128)(2,1)S(1)}, u32[]{:S(2)}, u32[]{:S(2)}) collective-permute-start(bf16[256,512]{1,0:T(8,128)(2,1)S(1)} %collective-permute-done.4.refs_2_), channel_id=1, source_target_pairs={{0,24},{8,16},{16,8},{24,0},{1,25},{9,17},{17,9},{25,1},{2,26},{10... | collective-permute-start | bytes 786440 | tf_op jit(solution)/shard_map/ppermute | solution.py:17
  41.1 1.5 %collective-permute-start.12 = (bf16[2,256,512]{2,1,0:T(8,128)(2,1)S(1)}, bf16[2,256,512]{2,1,0:T(8,128)(2,1)S(1)}, u32[]{:S(2)}, u32[]{:S(2)}) collective-permute-start(bf16[2,256,512]{2,1,0:T(8,128)(2,1)S(1)} %collective-permute-done.10.refs_6_), channel_id=1, source_target_pairs={{0,4},{1,3},{2,6},{3,1},{4,0},{5,7},{6,2},{7,5},{8,12},{9,11},{10,... | collective-permute-start | bytes 1572872 | tf_op jit(solution)/shard_map/ppermute | solution.py:17
  42.7 0.5 collective-permute-start.13
  43.2 1.5 %collective-permute-start.19 = (bf16[256,512]{1,0:T(8,128)(2,1)S(1)}, bf16[256,512]{1,0:T(8,128)(2,1)S(1)}, u32[]{:S(2)}, u32[]{:S(2)}) collective-permute-start(bf16[256,512]{1,0:T(8,128)(2,1)S(1)} %collective-permute-done.1), channel_id=1, source_target_pairs={{0,4},{1,3},{2,6},{3,1},{4,0},{5,7},{6,2},{7,5},{8,12},{9,11},{10,... | collective-permute-start | bytes 786440 | tf_op jit(solution)/shard_map/ppermute | solution.py:17
  44.7 2.4 %collective-permute-done.5 = bf16[256,512]{1,0:T(8,128)(2,1)S(1)} collective-permute-done((bf16[256,512]{1,0:T(8,128)(2,1)S(1)}, bf16[256,512]{1,0:T(8,128)(2,1)S(1)}, u32[]{:S(2)}, u32[]{:S(2)}) %collective-permute-start.5) | collective-permute-done | bytes 262176 | tf_op jit(solution)/shard_map/ppermute | solution.py:17
  47.2 11.6 %collective-permute-done.19.refs_1_ = bf16[256,512]{1,0:T(8,128)(2,1)S(1)} collective-permute-done((bf16[256,512]{1,0:T(8,128)(2,1)S(1)}, bf16[256,512]{1,0:T(8,128)(2,1)S(1)}, u32[]{:S(2)}, u32[]{:S(2)}) %collective-permute-start.19) | collective-permute-done | bytes 262176 | tf_op jit(solution)/shard_map/ppermute | solution.py:17
  58.8 0.5 collective-permute-start.15
  60.0 2.0 %shard_map.67.refs_1_.refs_5_ = bf16[8,64,256]{2,1,0:T(8,128)(2,1)S(1)} custom-call(f32[16,384,128]{2,1,0:T(8,128)S(1)} %get-tuple-element.8.refs_0_, f32[16,32,128]{2,1,0:T(8,128)S(1)} %get-tuple-element.9.refs_1_, f32[16,1,128]{2,1,0:T(1,128)S(1)} %bitcast.20, f32[16,1,128]{2,1,0:T(1,128)S(1)} %bitcast.26), custom_call_target="tpu_custom_call" | custom-call | flops 8126464 | tf_op jit(solution)/shard_map/pallas_call | solution.py:248
  61.9 2.0 %shard_map.68.refs_2_.refs_6_ = bf16[8,64,256]{2,1,0:T(8,128)(2,1)S(1)} custom-call(f32[16,384,128]{2,1,0:T(8,128)S(1)} %get-tuple-element.8.refs_0_, f32[16,32,128]{2,1,0:T(8,128)S(1)} %get-tuple-element.9.refs_1_, f32[16,1,128]{2,1,0:T(1,128)S(1)} %bitcast.21, f32[16,1,128]{2,1,0:T(1,128)S(1)} %bitcast.27), custom_call_target="tpu_custom_call" | custom-call | flops 8126464 | tf_op jit(solution)/shard_map/pallas_call | solution.py:248
  63.9 2.0 %shard_map.69.refs_3_.refs_7_ = bf16[8,64,256]{2,1,0:T(8,128)(2,1)S(1)} custom-call(f32[16,384,128]{2,1,0:T(8,128)S(1)} %get-tuple-element.8.refs_0_, f32[16,32,128]{2,1,0:T(8,128)S(1)} %get-tuple-element.9.refs_1_, f32[16,1,128]{2,1,0:T(1,128)S(1)} %bitcast.22, f32[16,1,128]{2,1,0:T(1,128)S(1)} %bitcast.28), custom_call_target="tpu_custom_call" | custom-call | flops 8126464 | tf_op jit(solution)/shard_map/pallas_call | solution.py:248
  65.9 2.0 %shard_map.70.refs_4_.refs_8_ = bf16[8,64,256]{2,1,0:T(8,128)(2,1)S(1)} custom-call(f32[16,384,128]{2,1,0:T(8,128)S(1)} %get-tuple-element.8.refs_0_, f32[16,32,128]{2,1,0:T(8,128)S(1)} %get-tuple-element.9.refs_1_, f32[16,1,128]{2,1,0:T(1,128)S(1)} %bitcast.23, f32[16,1,128]{2,1,0:T(1,128)S(1)} %bitcast.29), custom_call_target="tpu_custom_call" | custom-call | flops 8126464 | tf_op jit(solution)/shard_map/pallas_call | solution.py:248
  67.9 2.0 %shard_map.71.refs_5_.refs_9_ = bf16[8,64,256]{2,1,0:T(8,128)(2,1)S(1)} custom-call(f32[16,384,128]{2,1,0:T(8,128)S(1)} %get-tuple-element.8.refs_0_, f32[16,32,128]{2,1,0:T(8,128)S(1)} %get-tuple-element.9.refs_1_, f32[16,1,128]{2,1,0:T(1,128)S(1)} %bitcast.24, f32[16,1,128]{2,1,0:T(1,128)S(1)} %bitcast.30), custom_call_target="tpu_custom_call" | custom-call | flops 8126464 | tf_op jit(solution)/shard_map/pallas_call | solution.py:248
  69.8 2.1 %shard_map.66.refs_0_.refs_4_ = bf16[8,64,256]{2,1,0:T(8,128)(2,1)S(1)} custom-call(f32[16,384,128]{2,1,0:T(8,128)S(1)} %get-tuple-element.8.refs_0_, f32[16,32,128]{2,1,0:T(8,128)S(1)} %get-tuple-element.9.refs_1_, f32[16,1,128]{2,1,0:T(1,128)S(1)} %bitcast.25, f32[16,1,128]{2,1,0:T(1,128)S(1)} %bitcast.31, bf16[32,2048]{1,0:T(8,128)(2,1)S(1)} %collective-permute-done.refs_4_), custom_call_target="tpu_custom_call" | custom-call | flops 8126464 | tf_op jit(solution)/shard_map/pallas_call | solution.py:248
  72.0 0.6 shard_map.72.refs_0_
  72.9 1.0 %shard_map.74.refs_1_ = bf16[384,512]{1,0:T(8,128)(2,1)S(1)} custom-call(bf16[8,64,256]{2,1,0:T(8,128)(2,1)S(1)} %shard_map.66.refs_0_.refs_4_, bf16[8,64,256]{2,1,0:T(8,128)(2,1)S(1)} %shard_map.67.refs_1_.refs_5_, bf16[8,64,256]{2,1,0:T(8,128)(2,1)S(1)} %shard_map.68.refs_2_.refs_6_, bf16[8,64,256]{2,1,0:T(8,128)(2,1)S(1)} %shard_map.69.refs_3_.refs_7_, ...), custom_call_target="tpu_custom_call" | custom-call | flops 805306368 | tf_op jit(solution)/shard_map/pallas_call | solution.py:248
  73.9 1.0 %shard_map.76.refs_2_ = bf16[384,512]{1,0:T(8,128)(2,1)S(1)} custom-call(bf16[8,64,256]{2,1,0:T(8,128)(2,1)S(1)} %shard_map.66.refs_0_.refs_4_, bf16[8,64,256]{2,1,0:T(8,128)(2,1)S(1)} %shard_map.67.refs_1_.refs_5_, bf16[8,64,256]{2,1,0:T(8,128)(2,1)S(1)} %shard_map.68.refs_2_.refs_6_, bf16[8,64,256]{2,1,0:T(8,128)(2,1)S(1)} %shard_map.69.refs_3_.refs_7_, ...), custom_call_target="tpu_custom_call" | custom-call | flops 805306368 | tf_op jit(solution)/shard_map/pallas_call | solution.py:248
  74.9 1.0 %shard_map.77.refs_3_ = bf16[384,512]{1,0:T(8,128)(2,1)S(1)} custom-call(bf16[8,64,256]{2,1,0:T(8,128)(2,1)S(1)} %shard_map.66.refs_0_.refs_4_, bf16[8,64,256]{2,1,0:T(8,128)(2,1)S(1)} %shard_map.67.refs_1_.refs_5_, bf16[8,64,256]{2,1,0:T(8,128)(2,1)S(1)} %shard_map.68.refs_2_.refs_6_, bf16[8,64,256]{2,1,0:T(8,128)(2,1)S(1)} %shard_map.69.refs_3_.refs_7_, ...), custom_call_target="tpu_custom_call" | custom-call | flops 805306368 | tf_op jit(solution)/shard_map/pallas_call | solution.py:248
  75.9 1.5 %shard_map.79 = bf16[1,384,2048]{2,1,0:T(8,128)(2,1)} custom-call(f32[384,512]{1,0:T(8,128)S(1)} %shard_map.72.refs_0_, bf16[384,512]{1,0:T(8,128)(2,1)S(1)} %shard_map.74.refs_1_, bf16[384,512]{1,0:T(8,128)(2,1)S(1)} %shard_map.76.refs_2_, bf16[384,512]{1,0:T(8,128)(2,1)S(1)} %shard_map.77.refs_3_, bf16[8,64,256]{2,1,0:T(8,128)(2,1)S(1)} %shard_map.66.refs_0_.refs_4_, ...), custom_call_target="tpu_custom_call" | custom-call | flops 402653184 | tf_op jit(solution)/shard_map/pallas_call | solution.py:248
  (40 shorter events, 1.2 us)
Async XLA Ops:
  0.0 3.0 %collective-permute-start.8 = (bf16[256,512]{1,0:T(8,128)(2,1)}, bf16[256,512]{1,0:T(8,128)(2,1)S(1)}, u32[]{:S(2)}, u32[]{:S(2)}) collective-permute-start(bf16[256,512]{1,0:T(8,128)(2,1)} %refs_0_.3), channel_id=1, source_target_pairs={{0,1},{1,0},{2,3},{3,2},{4,5},{5,4},{6,7},{7,6},{8,9},{9,8},{10,11... | collective-permute-start | bytes 786440 | tf_op jit(solution)/shard_map/ppermute | solution.py:17
  0.5 9.4 %collective-permute-start.3 = (bf16[256,512]{1,0:T(8,128)(2,1)}, bf16[256,512]{1,0:T(8,128)(2,1)S(1)}, u32[]{:S(2)}, u32[]{:S(2)}) collective-permute-start(bf16[256,512]{1,0:T(8,128)(2,1)} %refs_0_.3), channel_id=1, source_target_pairs={{0,2},{1,5},{2,0},{3,7},{4,6},{5,1},{6,4},{7,3},{8,10},{9,13},{10,... | collective-permute-start | bytes 786440 | tf_op jit(solution)/shard_map/ppermute | solution.py:17
  3.0 1.0 %copy-start.2 = (bf16[256,512]{1,0:T(8,128)(2,1)S(1)}, bf16[256,512]{1,0:T(8,128)(2,1)}, u32[]{:S(2)}) copy-start(bf16[256,512]{1,0:T(8,128)(2,1)} %refs_0_.3) | copy-start | bytes 786436
  4.0 22.5 %collective-permute-start.10 = (bf16[2,256,512]{2,1,0:T(8,128)(2,1)S(1)}, bf16[2,256,512]{2,1,0:T(8,128)(2,1)S(1)}, u32[]{:S(2)}, u32[]{:S(2)}) collective-permute-start(bf16[2,256,512]{2,1,0:T(8,128)(2,1)S(1)} %shard_map.75), channel_id=1, source_target_pairs={{0,8},{1,17},{2,10},{3,19},{4,12},{5,21},{6,14},{7,23},{8,0},{9,25... | collective-permute-start | bytes 1572872 | tf_op jit(solution)/shard_map/ppermute | solution.py:314
  5.9 19.9 %collective-permute-start.1 = (bf16[256,512]{1,0:T(8,128)(2,1)S(1)}, bf16[256,512]{1,0:T(8,128)(2,1)S(1)}, u32[]{:S(2)}, u32[]{:S(2)}) collective-permute-start(bf16[256,512]{1,0:T(8,128)(2,1)S(1)} %copy-done.2), channel_id=1, source_target_pairs={{0,24},{8,16},{16,8},{24,0},{1,25},{9,17},{17,9},{25,1},{2,26},{10... | collective-permute-start | bytes 786440 | tf_op jit(solution)/shard_map/ppermute | solution.py:17
  8.3 17.5 %collective-permute-start.7 = (bf16[256,512]{1,0:T(8,128)(2,1)S(1)}, bf16[256,512]{1,0:T(8,128)(2,1)S(1)}, u32[]{:S(2)}, u32[]{:S(2)}) collective-permute-start(bf16[256,512]{1,0:T(8,128)(2,1)S(1)} %copy-done.2), channel_id=1, source_target_pairs={{0,4},{1,3},{2,6},{3,1},{4,0},{5,7},{6,2},{7,5},{8,12},{9,11},{10,... | collective-permute-start | bytes 786440 | tf_op jit(solution)/shard_map/ppermute | solution.py:17
  9.9 16.0 %collective-permute-start.4 = (bf16[256,512]{1,0:T(8,128)(2,1)S(1)}, bf16[256,512]{1,0:T(8,128)(2,1)S(1)}, u32[]{:S(2)}, u32[]{:S(2)}) collective-permute-start(bf16[256,512]{1,0:T(8,128)(2,1)S(1)} %collective-permute-done.3.refs_0_), channel_id=1, source_target_pairs={{0,4},{1,3},{2,6},{3,1},{4,0},{5,7},{6,2},{7,5},{8,12},{9,11},{10,... | collective-permute-start | bytes 786440 | tf_op jit(solution)/shard_map/ppermute | solution.py:17
  25.8 15.4 %collective-permute-start.2 = (bf16[256,512]{1,0:T(8,128)(2,1)S(1)}, bf16[256,512]{1,0:T(8,128)(2,1)S(1)}, u32[]{:S(2)}, u32[]{:S(2)}) collective-permute-start(bf16[256,512]{1,0:T(8,128)(2,1)S(1)} %collective-permute-done.1), channel_id=1, source_target_pairs={{0,1},{1,0},{2,3},{3,2},{4,5},{5,4},{6,7},{7,6},{8,9},{9,8},{10,11... | collective-permute-start | bytes 786440 | tf_op jit(solution)/shard_map/ppermute | solution.py:17
  25.9 2.1 %copy-start = (bf16[1,384,2048]{2,1,0:T(8,128)(2,1)S(1)}, bf16[1,384,2048]{2,1,0:T(8,128)(2,1)}, u32[]{:S(2)}) copy-start(bf16[1,384,2048]{2,1,0:T(8,128)(2,1)} %refs_0_.2) | copy-start | bytes 4718596
  25.9 2.1 %copy-start.1 = (bf16[1,384,2048]{2,1,0:T(8,128)(2,1)S(1)}, bf16[1,384,2048]{2,1,0:T(8,128)(2,1)}, u32[]{:S(2)}) copy-start(bf16[1,384,2048]{2,1,0:T(8,128)(2,1)} %refs_1_.1) | copy-start | bytes 4718596
  25.9 2.1 %copy-start.6 = (bf16[31,2048]{1,0:T(8,128)(2,1)S(1)}, bf16[31,2048]{1,0:T(8,128)(2,1)}, u32[]{:S(2)}) copy-start(bf16[31,2048]{1,0:T(8,128)(2,1)} %refs_2_.1) | copy-start | bytes 380932
  25.9 33.9 %collective-permute-start.9 = (bf16[3,256,512]{2,1,0:T(8,128)(2,1)S(1)}, bf16[3,256,512]{2,1,0:T(8,128)(2,1)S(1)}, u32[]{:S(2)}, u32[]{:S(2)}) collective-permute-start(bf16[3,256,512]{2,1,0:T(8,128)(2,1)S(1)} %shard_map.73), channel_id=1, source_target_pairs={{0,1},{1,0},{2,3},{3,2},{4,5},{5,4},{6,7},{7,6},{8,9},{9,8},{10,11... | collective-permute-start | bytes 2359304 | tf_op jit(solution)/shard_map/ppermute | solution.py:17
  26.5 16.2 %collective-permute-start.11 = (bf16[2,256,512]{2,1,0:T(8,128)(2,1)S(1)}, bf16[2,256,512]{2,1,0:T(8,128)(2,1)S(1)}, u32[]{:S(2)}, u32[]{:S(2)}) collective-permute-start(bf16[2,256,512]{2,1,0:T(8,128)(2,1)S(1)} %collective-permute-done.10.refs_6_), channel_id=1, source_target_pairs={{0,2},{1,5},{2,0},{3,7},{4,6},{5,1},{6,4},{7,3},{8,10},{9,13},{10,... | collective-permute-start | bytes 1572872 | tf_op jit(solution)/shard_map/ppermute | solution.py:17
  28.0 32.0 %copy-start.4 = (f32[2048]{0:T(1024)S(1)}, f32[2048]{0:T(1024)}, u32[]{:S(2)}) copy-start(f32[2048]{0:T(1024)} %param.9) | copy-start | bytes 24580
  28.0 32.0 %copy-start.5 = (f32[2048]{0:T(1024)S(1)}, f32[2048]{0:T(1024)}, u32[]{:S(2)}) copy-start(f32[2048]{0:T(1024)} %param.10) | copy-start | bytes 24580
  29.2 8.2 %collective-permute-start = (bf16[32,2048]{1,0:T(8,128)(2,1)S(1)}, bf16[32,2048]{1,0:T(8,128)(2,1)S(1)}, u32[]{:S(2)}, u32[]{:S(2)}) collective-permute-start(bf16[32,2048]{1,0:T(8,128)(2,1)S(1)} %get-tuple-element.10), channel_id=1, source_target_pairs={{0,8},{8,16},{16,24},{24,0},{1,9},{9,17},{17,25},{25,1},{2,10},{10... | collective-permute-start | bytes 393224 | tf_op jit(solution)/shard_map/ppermute | solution.py:283
  34.4 8.8 %collective-permute-start.18 = (bf16[256,512]{1,0:T(8,128)(2,1)S(1)}, bf16[256,512]{1,0:T(8,128)(2,1)S(1)}, u32[]{:S(2)}, u32[]{:S(2)}) collective-permute-start(bf16[256,512]{1,0:T(8,128)(2,1)S(1)} %collective-permute-done.1), channel_id=1, source_target_pairs={{0,2},{1,5},{2,0},{3,7},{4,6},{5,1},{6,4},{7,3},{8,10},{9,13},{10,... | collective-permute-start | bytes 786440 | tf_op jit(solution)/shard_map/ppermute | solution.py:17
  37.3 9.8 %collective-permute-start.5 = (bf16[256,512]{1,0:T(8,128)(2,1)S(1)}, bf16[256,512]{1,0:T(8,128)(2,1)S(1)}, u32[]{:S(2)}, u32[]{:S(2)}) collective-permute-start(bf16[256,512]{1,0:T(8,128)(2,1)S(1)} %collective-permute-done.4.refs_2_), channel_id=1, source_target_pairs={{0,24},{8,16},{16,8},{24,0},{1,25},{9,17},{17,9},{25,1},{2,26},{10... | collective-permute-start | bytes 786440 | tf_op jit(solution)/shard_map/ppermute | solution.py:17
  41.1 18.1 %collective-permute-start.12 = (bf16[2,256,512]{2,1,0:T(8,128)(2,1)S(1)}, bf16[2,256,512]{2,1,0:T(8,128)(2,1)S(1)}, u32[]{:S(2)}, u32[]{:S(2)}) collective-permute-start(bf16[2,256,512]{2,1,0:T(8,128)(2,1)S(1)} %collective-permute-done.10.refs_6_), channel_id=1, source_target_pairs={{0,4},{1,3},{2,6},{3,1},{4,0},{5,7},{6,2},{7,5},{8,12},{9,11},{10,... | collective-permute-start | bytes 1572872 | tf_op jit(solution)/shard_map/ppermute | solution.py:17
  42.7 16.7 %collective-permute-start.13 = (bf16[2,256,512]{2,1,0:T(8,128)(2,1)S(1)}, bf16[2,256,512]{2,1,0:T(8,128)(2,1)S(1)}, u32[]{:S(2)}, u32[]{:S(2)}) collective-permute-start(bf16[2,256,512]{2,1,0:T(8,128)(2,1)S(1)} %collective-permute-done.11.refs_7_), channel_id=1, source_target_pairs={{0,4},{1,3},{2,6},{3,1},{4,0},{5,7},{6,2},{7,5},{8,12},{9,11},{10,... | collective-permute-start | bytes 1572872 | tf_op jit(solution)/shard_map/ppermute | solution.py:17
  43.2 15.6 %collective-permute-start.19 = (bf16[256,512]{1,0:T(8,128)(2,1)S(1)}, bf16[256,512]{1,0:T(8,128)(2,1)S(1)}, u32[]{:S(2)}, u32[]{:S(2)}) collective-permute-start(bf16[256,512]{1,0:T(8,128)(2,1)S(1)} %collective-permute-done.1), channel_id=1, source_target_pairs={{0,4},{1,3},{2,6},{3,1},{4,0},{5,7},{6,2},{7,5},{8,12},{9,11},{10,... | collective-permute-start | bytes 786440 | tf_op jit(solution)/shard_map/ppermute | solution.py:17
  47.2 11.6 %collective-permute-start.6 = (bf16[256,512]{1,0:T(8,128)(2,1)S(1)}, bf16[256,512]{1,0:T(8,128)(2,1)S(1)}, u32[]{:S(2)}, u32[]{:S(2)}) collective-permute-start(bf16[256,512]{1,0:T(8,128)(2,1)S(1)} %collective-permute-done.5), channel_id=1, source_target_pairs={{0,1},{1,0},{2,3},{3,2},{4,5},{5,4},{6,7},{7,6},{8,9},{9,8},{10,11... | collective-permute-start | bytes 786440 | tf_op jit(solution)/shard_map/ppermute | solution.py:17
  58.8 16.1 %collective-permute-start.14 = (bf16[2,256,512]{2,1,0:T(8,128)(2,1)S(1)}, bf16[2,256,512]{2,1,0:T(8,128)(2,1)S(1)}, u32[]{:S(2)}, u32[]{:S(2)}) collective-permute-start(bf16[2,256,512]{2,1,0:T(8,128)(2,1)S(1)} %collective-permute-done.10.refs_6_), channel_id=1, source_target_pairs={{0,1},{1,0},{2,3},{3,2},{4,5},{5,4},{6,7},{7,6},{8,9},{9,8},{10,11... | collective-permute-start | bytes 1572872 | tf_op jit(solution)/shard_map/ppermute | solution.py:17
  58.8 16.1 %collective-permute-start.15 = (bf16[2,256,512]{2,1,0:T(8,128)(2,1)S(1)}, bf16[2,256,512]{2,1,0:T(8,128)(2,1)S(1)}, u32[]{:S(2)}, u32[]{:S(2)}) collective-permute-start(bf16[2,256,512]{2,1,0:T(8,128)(2,1)S(1)} %collective-permute-done.11.refs_7_), channel_id=1, source_target_pairs={{0,1},{1,0},{2,3},{3,2},{4,5},{5,4},{6,7},{7,6},{8,9},{9,8},{10,11... | collective-permute-start | bytes 1572872 | tf_op jit(solution)/shard_map/ppermute | solution.py:17
  59.3 15.6 %collective-permute-start.16 = (bf16[2,256,512]{2,1,0:T(8,128)(2,1)S(1)}, bf16[2,256,512]{2,1,0:T(8,128)(2,1)S(1)}, u32[]{:S(2)}, u32[]{:S(2)}) collective-permute-start(bf16[2,256,512]{2,1,0:T(8,128)(2,1)S(1)} %collective-permute-done.12.refs_8_), channel_id=1, source_target_pairs={{0,1},{1,0},{2,3},{3,2},{4,5},{5,4},{6,7},{7,6},{8,9},{9,8},{10,11... | collective-permute-start | bytes 1572872 | tf_op jit(solution)/shard_map/ppermute | solution.py:17
  59.4 15.5 %collective-permute-start.17 = (bf16[2,256,512]{2,1,0:T(8,128)(2,1)S(1)}, bf16[2,256,512]{2,1,0:T(8,128)(2,1)S(1)}, u32[]{:S(2)}, u32[]{:S(2)}) collective-permute-start(bf16[2,256,512]{2,1,0:T(8,128)(2,1)S(1)} %collective-permute-done.13.refs_9_), channel_id=1, source_target_pairs={{0,1},{1,0},{2,3},{3,2},{4,5},{5,4},{6,7},{7,6},{8,9},{9,8},{10,11... | collective-permute-start | bytes 1572872 | tf_op jit(solution)/shard_map/ppermute | solution.py:17
  59.8 16.0 %collective-permute-start.20 = (bf16[2,256,512]{2,1,0:T(8,128)(2,1)S(1)}, bf16[2,256,512]{2,1,0:T(8,128)(2,1)S(1)}, u32[]{:S(2)}, u32[]{:S(2)}) collective-permute-start(bf16[2,256,512]{2,1,0:T(8,128)(2,1)S(1)} %shard_map.78), channel_id=1, source_target_pairs={{0,1},{1,0},{2,3},{3,2},{4,5},{5,4},{6,7},{7,6},{8,9},{9,8},{10,11... | collective-permute-start | bytes 1572872 | tf_op jit(solution)/shard_map/ppermute | solution.py:17
  72.0 1.0 %copy-start.3 = (bf16[256,512]{1,0:T(8,128)(2,1)S(1)}, bf16[256,512]{1,0:T(8,128)(2,1)}, u32[]{:S(2)}) copy-start(bf16[256,512]{1,0:T(8,128)(2,1)} %refs_0_.3) | copy-start | bytes 786436

commit v4 on v3

--- a/solution.py
+++ b/solution.py
@@ -217,21 +217,36 @@
     refs[-1][...] = projected(refs[:chunks], refs[chunks:-1], slots).astype(refs[-1].dtype)
 
 
+def put(source, out_ref, rows, step, sem):
+    width = source.shape[1]
+    column = pl.ds(pl.multiple_of((lax.axis_index("sp") ^ step) * width, width), width)
+    copy = pltpu.make_async_copy(source.at[rows], out_ref.at[0, rows, column], sem)
+    copy.start()
+    return copy
+
+
+def middle_kernel(chunks, slots, count, step_of, *refs):
+    (done, acts, weights) = (refs[0], refs[1 : 1 + chunks], refs[1 + chunks : 1 + chunks + count])
+    (block_ref, out_ref, sem) = refs[-3:]
+    step = step_of(lax.axis_index("dp") % 2)
+    copy = put(done, out_ref, pl.ds(0, done.shape[0]), step, sem.at[0])
+    block_ref[...] = projected(acts, weights, slots).astype(block_ref.dtype)
+    copy.wait()
+
+
 def last_kernel(chunks, slots, *refs):
-    (begun, done) = (refs[0], refs[1:4])
-    (acts, weights) = (refs[4 : 4 + chunks], refs[4 + chunks : -3])
+    (begun, third) = refs[:2]
+    (acts, weights) = (refs[2 : 2 + chunks], refs[2 + chunks : -4])
     (out_ref, buf, sem) = refs[-3:]
-    width = buf.shape[1]
-    (here, parity) = (lax.axis_index("sp"), lax.axis_index("dp") % 2)
-    copies = []
-    for index, step in enumerate((0, 1 + parity, 2 - parity, 3)):
-        if index == len(done):
-            buf[...] = (begun[...] + projected(acts, weights, slots)).astype(buf.dtype)
-        column = pl.ds(pl.multiple_of((here ^ step) * width, width), width)
-        source = buf if index == len(done) else done[index]
-        copy = pltpu.make_async_copy(source, out_ref.at[0, :, column], sem.at[index])
-        copy.start()
-        copies.append(copy)
+    rows = acts[0].shape[1]
+    copies = [put(third, out_ref, pl.ds(0, third.shape[0]), 2 - lax.axis_index("dp") % 2, sem.at[2])]
+    first = 0
+    for half, count in enumerate((chunks - chunks // 2, chunks // 2)):
+        span = pl.ds(first * rows, count * rows)
+        total = begun[span] + projected(acts[first : first + count], weights, slots)
+        buf[span] = total.astype(buf.dtype)
+        copies.append(put(buf, out_ref, span, 3, sem.at[half]))
+        first += count
     for copy in copies:
         copy.wait()
 
@@ -243,13 +258,14 @@
 HBM = pl.BlockSpec(memory_space=pltpu.HBM)
 
 
-def kernel_call(body, operands, outs, scratch=(), out_spec=VMEM, flops=0, mib=8, hbm=0):
+def kernel_call(body, operands, outs, scratch=(), out_spec=VMEM, flops=0, mib=8, aliases=None):
     outs = [jax.ShapeDtypeStruct(out, jnp.bfloat16) if isinstance(out, tuple) else out for out in outs]
     results = pl.pallas_call(
         body,
         out_shape=outs,
-        in_specs=[HBM] * hbm + [VMEM] * (len(operands) - hbm),
-        out_specs=[out_spec] * len(outs),
+        in_specs=[ANY if index in (aliases or {}) else VMEM for index in range(len(operands))],
+        out_specs=list(out_spec) if isinstance(out_spec, tuple) else [out_spec] * len(outs),
+        input_output_aliases=aliases or {},
         scratch_shapes=list(scratch),
         compiler_params=pltpu.CompilerParams(vmem_limit_bytes=mib << 20),
         cost_estimate=pl.CostEstimate(flops=flops, bytes_accessed=0, transcendentals=0),
@@ -263,7 +279,7 @@
     layers = lax.axis_size("sp")
     depth, width = out_weight.shape
     pad = -(-(tap_count - 1) // 32) * 32
-    rows = next(count for count in (64, 64, 32) if tok_rows % count == 0)
+    rows = next(count for count in (128, 64, 32) if tok_rows % count == 0)
     chunks = tok_rows // rows
     groups = channels // LANES
 
@@ -355,20 +371,42 @@
             (piece, first, second, forwarded, partner, swapped_0),
             ((0,), (1,), (2,), (3,), (4,), (5, 6, 7)),
         ),
-        project(pairs, ((0, 4), (1, 6), (2, 5), (3, 7))),
-        project(pairs_other, ((4, 0), (5, 2), (6, 1), (7, 3))),
     ]
+    whole = jax.ShapeDtypeStruct((1, tok_rows, layers * width), jnp.bfloat16)
+
+    def middle(weights, slots, step_of, block, out):
+        operands = [block] + acts + list(weights) + ([] if out is None else [out])
+        return kernel_call(
+            functools.partial(middle_kernel, chunks, slots, len(weights), step_of),
+            operands,
+            [(tok_rows, width), whole],
+            (pltpu.SemaphoreType.DMA((1,)),),
+            out_spec=(VMEM, ANY),
+            flops=16 * tok_rows * depth * width,
+            aliases=None if out is None else {len(operands) - 1: 1},
+        )
+
+    block, out = middle(pairs, ((0, 4), (1, 6), (2, 5), (3, 7)), lambda parity: 0, done[0], None)
+    third, out = middle(
+        pairs_other, ((4, 0), (5, 2), (6, 1), (7, 3)), lambda parity: 1 + parity, block, out
+    )
     (piece, first, second, forwarded, partner) = singles[1]
     last = named(forwarded, "dp", 1, 1)
-    begun = project((piece, partner, forwarded, last), ((0,), (4,), (3,), (7,)), jnp.float32)
     swapped_3 = both((first, second))
+    begun = project(
+        (piece, partner, forwarded, last, first, second),
+        ((0,), (4,), (3,), (7,), (1,), (2,)),
+        jnp.float32,
+    )
+    operands = [begun, third] + acts + [swapped_3, out]
     return kernel_call(
-        functools.partial(last_kernel, chunks, ((1,), (2,), (5, 6))),
-        [begun] + done + acts + [first[None], second[None], swapped_3],
-        [(1, tok_rows, layers * width)],
-        (pltpu.VMEM((tok_rows, width), jnp.bfloat16), pltpu.SemaphoreType.DMA((layers,))),
+        functools.partial(last_kernel, chunks, ((5, 6),)),
+        operands,
+        [whole],
+        (pltpu.VMEM((tok_rows, width), jnp.bfloat16), pltpu.SemaphoreType.DMA((3,))),
         out_spec=ANY,
-        flops=8 * tok_rows * depth * width,
+        flops=4 * tok_rows * depth * width,
+        aliases={len(operands) - 1: 0},
     )
 
 

time: 77.6 us -> 74.9 us (0.965)
  starting transfers between devices: 26.6 us -> 24.3 us
  local copies, waits for them, and re-layouts: 1.38 us -> 2.33 us
  waiting for transfers between devices: 31 us -> 30.2 us
    ppermute x19, starting transfers between devices: 19.5 us -> 17.5 us  [swapped(): lax.ppermute(value, axis, [(index, index ^ mask_of(index)) for index in r...]
    ppermute x19, waiting for transfers between devices: 29.5 us -> 27.6 us  [swapped(): lax.ppermute(value, axis, [(index, index ^ mask_of(index)) for index in r...]
    ppermute x1, waiting for transfers between devices: 1.44 us -> 2.66 us  [square_plane(): lax.ppermute(tail, 'sp', [(source, (source + 1) % layers) for source in r...]
    unnamed x14, local copies, waits for them, and re-layouts: 1.38 us -> 2.33 us
    pallas_call x16 -> x13, Pallas kernels: 18.2 us -> 17.6 us  [kernel_call(): pl.pallas_call(body, out_shape=outs, in_specs=[ANY if index in (aliases o...]
  transfers between devices with their start and end apart: 21 -> 21, of which waited for: 4 -> 6; matrix products, arithmetic and copies ran while one was open for 0% -> 0% of each run, Pallas kernels for 22% -> 22%
where the time goes in v4:
time: 74.9 us; the launch traced here: 74.7 us
  waiting for transfers between devices  30.2 us (40%)
  starting transfers between devices  24.3 us (32%)
  Pallas kernels  17.6 us (23%)
  local copies, waits for them, and re-layouts  2.33 us (3%)
    ppermute x19, waiting for transfers between devices, swapped(): lax.ppermute(value, axis, [(index, index ^ mask_of(index)) for index in r...  27.6 us
    pallas_call x13, Pallas kernels, kernel_call(): pl.pallas_call(body, out_shape=outs, in_specs=[ANY if index in (aliases o...  17.6 us
    ppermute x19, starting transfers between devices, swapped(): lax.ppermute(value, axis, [(index, index ^ mask_of(index)) for index in r...  17.5 us
    ppermute x1, starting transfers between devices, square_plane(): lax.ppermute(tail, 'sp', [(source, (source + 1) % layers) for source in r...  4.98 us
    ppermute x1, waiting for transfers between devices, square_plane(): lax.ppermute(tail, 'sp', [(source, (source + 1) % layers) for source in r...  2.66 us
    unnamed x14, local copies, waits for them, and re-layouts  2.33 us
    ppermute x1, starting transfers between devices, square_plane(): arrived = lax.ppermute(chip, ('sp', 'dp'), route)  1.86 us
  transfers between devices with their start and end apart: 21, of which 6 were waited for; matrix products, arithmetic and copies ran while one was open for 0% of the time, Pallas kernels for 22%

profile of v4, /device:TPU:0, one launch (start us, length us, event | category | flops | bytes accessed | tf_op | source)
XLA Modules:
  0.0 74.7 jit_solution(57849749902037089)
XLA Ops:
  0.0 0.5 collective-permute-start.10
  0.5 2.5 %collective-permute-start.3 = (bf16[256,512]{1,0:T(8,128)(2,1)}, bf16[256,512]{1,0:T(8,128)(2,1)S(1)}, u32[]{:S(2)}, u32[]{:S(2)}) collective-permute-start(bf16[256,512]{1,0:T(8,128)(2,1)} %refs_0_.3), channel_id=1, source_target_pairs={{0,2},{1,5},{2,0},{3,7},{4,6},{5,1},{6,4},{7,3},{8,10},{9,13},{10,... | collective-permute-start | bytes 786440 | tf_op jit(solution)/shard_map/ppermute | solution.py:17
  3.0 1.0 %copy-done.2 = bf16[256,512]{1,0:T(8,128)(2,1)S(1)} copy-done((bf16[256,512]{1,0:T(8,128)(2,1)S(1)}, bf16[256,512]{1,0:T(8,128)(2,1)}, u32[]{:S(2)}) %copy-start.2) | copy-done | bytes 262168
  4.0 1.9 %collective-permute-start.12 = (bf16[2,256,512]{2,1,0:T(8,128)(2,1)S(1)}, bf16[2,256,512]{2,1,0:T(8,128)(2,1)S(1)}, u32[]{:S(2)}, u32[]{:S(2)}) collective-permute-start(bf16[2,256,512]{2,1,0:T(8,128)(2,1)S(1)} %shard_map.72), channel_id=1, source_target_pairs={{0,8},{1,17},{2,10},{3,19},{4,12},{5,21},{6,14},{7,23},{8,0},{9,25... | collective-permute-start | bytes 1572872 | tf_op jit(solution)/shard_map/ppermute | solution.py:330
  5.9 2.5 %collective-permute-start.1 = (bf16[256,512]{1,0:T(8,128)(2,1)S(1)}, bf16[256,512]{1,0:T(8,128)(2,1)S(1)}, u32[]{:S(2)}, u32[]{:S(2)}) collective-permute-start(bf16[256,512]{1,0:T(8,128)(2,1)S(1)} %copy-done.2), channel_id=1, source_target_pairs={{0,24},{8,16},{16,8},{24,0},{1,25},{9,17},{17,9},{25,1},{2,26},{10... | collective-permute-start | bytes 786440 | tf_op jit(solution)/shard_map/ppermute | solution.py:17
  8.3 1.5 %collective-permute-start.9 = (bf16[256,512]{1,0:T(8,128)(2,1)S(1)}, bf16[256,512]{1,0:T(8,128)(2,1)S(1)}, u32[]{:S(2)}, u32[]{:S(2)}) collective-permute-start(bf16[256,512]{1,0:T(8,128)(2,1)S(1)} %copy-done.2), channel_id=1, source_target_pairs={{0,4},{1,3},{2,6},{3,1},{4,0},{5,7},{6,2},{7,5},{8,12},{9,11},{10,... | collective-permute-start | bytes 786440 | tf_op jit(solution)/shard_map/ppermute | solution.py:17
  9.9 0.5 collective-permute-start.4
  10.4 15.4 %collective-permute-done.1 = bf16[256,512]{1,0:T(8,128)(2,1)S(1)} collective-permute-done((bf16[256,512]{1,0:T(8,128)(2,1)S(1)}, bf16[256,512]{1,0:T(8,128)(2,1)S(1)}, u32[]{:S(2)}, u32[]{:S(2)}) %collective-permute-start.1) | collective-permute-done | bytes 262176 | tf_op jit(solution)/shard_map/ppermute | solution.py:17
  25.8 1.5 %collective-permute-start.7 = (bf16[256,512]{1,0:T(8,128)(2,1)S(1)}, bf16[256,512]{1,0:T(8,128)(2,1)S(1)}, u32[]{:S(2)}, u32[]{:S(2)}) collective-permute-start(bf16[256,512]{1,0:T(8,128)(2,1)S(1)} %collective-permute-done.1), channel_id=1, source_target_pairs={{0,2},{1,5},{2,0},{3,7},{4,6},{5,1},{6,4},{7,3},{8,10},{9,13},{10,... | collective-permute-start | bytes 786440 | tf_op jit(solution)/shard_map/ppermute | solution.py:17
  27.5 0.6 collective-permute-start.13
  28.1 0.7 copy-done
  29.2 1.1 %shard_map.65 = (f32[16,384,128]{2,1,0:T(8,128)S(1)}, bf16[32,2048]{1,0:T(8,128)(2,1)S(1)}, f32[16,32,128]{2,1,0:T(8,128)S(1)}) custom-call(bf16[1,384,2048]{2,1,0:T(8,128)(2,1)S(1)} %copy-done, bf16[1,384,2048]{2,1,0:T(8,128)(2,1)S(1)} %copy-done.1, bf16[31,2048]{1,0:T(8,128)(2,1)S(1)} %copy-done.4, bf16[16,128]{1,0:T(8,128)(2,1)S(1)} %shard_map.64.refs_3_), custom_call_target="tpu_custom_call" | custom-call | flops 31457280 | tf_op jit(solution)/shard_map/pallas_call | solution.py:263
  30.4 5.0 %collective-permute-start = (bf16[32,2048]{1,0:T(8,128)(2,1)S(1)}, bf16[32,2048]{1,0:T(8,128)(2,1)S(1)}, u32[]{:S(2)}, u32[]{:S(2)}) collective-permute-start(bf16[32,2048]{1,0:T(8,128)(2,1)S(1)} %get-tuple-element.14), channel_id=1, source_target_pairs={{0,8},{8,16},{16,24},{24,0},{1,9},{9,17},{17,25},{25,1},{2,10},{10... | collective-permute-start | bytes 393224 | tf_op jit(solution)/shard_map/ppermute | solution.py:299
  35.4 0.5 collective-permute-start.8
  35.9 2.7 %collective-permute-done.refs_4_ = bf16[32,2048]{1,0:T(8,128)(2,1)S(1)} collective-permute-done((bf16[32,2048]{1,0:T(8,128)(2,1)S(1)}, bf16[32,2048]{1,0:T(8,128)(2,1)S(1)}, u32[]{:S(2)}, u32[]{:S(2)}) %collective-permute-start) | collective-permute-done | bytes 131104 | tf_op jit(solution)/shard_map/ppermute | solution.py:299
  38.5 4.1 %collective-permute-start.5 = (bf16[256,512]{1,0:T(8,128)(2,1)S(1)}, bf16[256,512]{1,0:T(8,128)(2,1)S(1)}, u32[]{:S(2)}, u32[]{:S(2)}) collective-permute-start(bf16[256,512]{1,0:T(8,128)(2,1)S(1)} %collective-permute-done.4.refs_2_), channel_id=1, source_target_pairs={{0,24},{8,16},{16,8},{24,0},{1,25},{9,17},{17,9},{25,1},{2,26},{10... | collective-permute-start | bytes 786440 | tf_op jit(solution)/shard_map/ppermute | solution.py:17
  42.7 0.5 collective-permute-start.14
  43.2 1.5 %collective-permute-start.15 = (bf16[2,256,512]{2,1,0:T(8,128)(2,1)S(1)}, bf16[2,256,512]{2,1,0:T(8,128)(2,1)S(1)}, u32[]{:S(2)}, u32[]{:S(2)}) collective-permute-start(bf16[2,256,512]{2,1,0:T(8,128)(2,1)S(1)} %collective-permute-done.13.refs_5_), channel_id=1, source_target_pairs={{0,4},{1,3},{2,6},{3,1},{4,0},{5,7},{6,2},{7,5},{8,12},{9,11},{10,... | collective-permute-start | bytes 1572872 | tf_op jit(solution)/shard_map/ppermute | solution.py:17
  44.7 4.2 %collective-permute-done.5 = bf16[256,512]{1,0:T(8,128)(2,1)S(1)} collective-permute-done((bf16[256,512]{1,0:T(8,128)(2,1)S(1)}, bf16[256,512]{1,0:T(8,128)(2,1)S(1)}, u32[]{:S(2)}, u32[]{:S(2)}) %collective-permute-start.5) | collective-permute-done | bytes 262176 | tf_op jit(solution)/shard_map/ppermute | solution.py:17
  48.9 0.5 collective-permute-start.16
  49.4 1.0 %collective-permute-done.6 = bf16[256,512]{1,0:T(8,128)(2,1)S(1)} collective-permute-done((bf16[256,512]{1,0:T(8,128)(2,1)S(1)}, bf16[256,512]{1,0:T(8,128)(2,1)S(1)}, u32[]{:S(2)}, u32[]{:S(2)}) %collective-permute-start.6) | collective-permute-done | bytes 262176 | tf_op jit(solution)/shard_map/ppermute | solution.py:17
  50.6 1.3 %collective-permute-done.14.refs_6_ = bf16[2,256,512]{2,1,0:T(8,128)(2,1)S(1)} collective-permute-done((bf16[2,256,512]{2,1,0:T(8,128)(2,1)S(1)}, bf16[2,256,512]{2,1,0:T(8,128)(2,1)S(1)}, u32[]{:S(2)}, u32[]{:S(2)}) %collective-permute-start.14) | collective-permute-done | bytes 524320 | tf_op jit(solution)/shard_map/ppermute | solution.py:17
  51.9 5.6 %collective-permute-done.15.refs_7_ = bf16[2,256,512]{2,1,0:T(8,128)(2,1)S(1)} collective-permute-done((bf16[2,256,512]{2,1,0:T(8,128)(2,1)S(1)}, bf16[2,256,512]{2,1,0:T(8,128)(2,1)S(1)}, u32[]{:S(2)}, u32[]{:S(2)}) %collective-permute-start.15) | collective-permute-done | bytes 524320 | tf_op jit(solution)/shard_map/ppermute | solution.py:17
  57.5 0.6 collective-permute-start.20
  58.1 3.4 %shard_map.68.refs_2_.refs_3_.refs_4_ = bf16[8,128,256]{2,1,0:T(8,128)(2,1)S(1)} custom-call(f32[16,384,128]{2,1,0:T(8,128)S(1)} %get-tuple-element.12.refs_0_, f32[16,32,128]{2,1,0:T(8,128)S(1)} %get-tuple-element.13.refs_1_, f32[16,1,128]{2,1,0:T(1,128)S(1)} %bitcast.24, f32[16,1,128]{2,1,0:T(1,128)S(1)} %bitcast.27), custom_call_target="tpu_custom_call" | custom-call | flops 16252928 | tf_op jit(solution)/shard_map/pallas_call | solution.py:263
  61.5 3.4 %shard_map.67.refs_1_.refs_2_.refs_3_ = bf16[8,128,256]{2,1,0:T(8,128)(2,1)S(1)} custom-call(f32[16,384,128]{2,1,0:T(8,128)S(1)} %get-tuple-element.12.refs_0_, f32[16,32,128]{2,1,0:T(8,128)S(1)} %get-tuple-element.13.refs_1_, f32[16,1,128]{2,1,0:T(1,128)S(1)} %bitcast.25, f32[16,1,128]{2,1,0:T(1,128)S(1)} %bitcast.28), custom_call_target="tpu_custom_call" | custom-call | flops 16252928 | tf_op jit(solution)/shard_map/pallas_call | solution.py:263
  65.0 3.6 %shard_map.66.refs_0_.refs_1_.refs_2_ = bf16[8,128,256]{2,1,0:T(8,128)(2,1)S(1)} custom-call(f32[16,384,128]{2,1,0:T(8,128)S(1)} %get-tuple-element.12.refs_0_, f32[16,32,128]{2,1,0:T(8,128)S(1)} %get-tuple-element.13.refs_1_, f32[16,1,128]{2,1,0:T(1,128)S(1)} %bitcast.26, f32[16,1,128]{2,1,0:T(1,128)S(1)} %bitcast.29, ...), custom_call_target="tpu_custom_call" | custom-call | flops 16252928 | tf_op jit(solution)/shard_map/pallas_call | solution.py:263
  68.6 0.8 %shard_map.69.refs_0_ = f32[384,512]{1,0:T(8,128)S(1)} custom-call(bf16[8,128,256]{2,1,0:T(8,128)(2,1)S(1)} %shard_map.66.refs_0_.refs_1_.refs_2_, bf16[8,128,256]{2,1,0:T(8,128)(2,1)S(1)} %shard_map.67.refs_1_.refs_2_.refs_3_, bf16[8,128,256]{2,1,0:T(8,128)(2,1)S(1)} %shard_map.68.refs_2_.refs_3_.refs_4_, bf16[1,256,512]{2,1,0:T(8,128)(2,1)S(1)} %bitcast.20, ...), custom_call_target="tpu_custom_call" | custom-call | flops 603979776 | tf_op jit(solution)/shard_map/pallas_call | solution.py:263
  69.6 1.0 %shard_map.71.refs_0_ = bf16[384,512]{1,0:T(8,128)(2,1)S(1)} custom-call(bf16[8,128,256]{2,1,0:T(8,128)(2,1)S(1)} %shard_map.66.refs_0_.refs_1_.refs_2_, bf16[8,128,256]{2,1,0:T(8,128)(2,1)S(1)} %shard_map.67.refs_1_.refs_2_.refs_3_, bf16[8,128,256]{2,1,0:T(8,128)(2,1)S(1)} %shard_map.68.refs_2_.refs_3_.refs_4_, bf16[1,256,512]{2,1,0:T(8,128)(2,1)S(1)} %bitcast.13, ...), custom_call_target="tpu_custom_call" | custom-call | flops 805306368 | tf_op jit(solution)/shard_map/pallas_call | solution.py:263
  70.5 1.5 %shard_map.73 = (bf16[384,512]{1,0:T(8,128)(2,1)S(1)}, bf16[1,384,2048]{2,1,0:T(8,128)(2,1)}) custom-call(bf16[384,512]{1,0:T(8,128)(2,1)S(1)} %shard_map.71.refs_0_, bf16[8,128,256]{2,1,0:T(8,128)(2,1)S(1)} %shard_map.66.refs_0_.refs_1_.refs_2_, bf16[8,128,256]{2,1,0:T(8,128)(2,1)S(1)} %shard_map.67.refs_1_.refs_2_.refs_3_, ...), custom_call_target="tpu_custom_call" | custom-call | flops 805306368 | tf_op jit(solution)/shard_map/pallas_call | solution.py:263
  72.1 1.5 %shard_map.74 = (bf16[384,512]{1,0:T(8,128)(2,1)S(1)}, bf16[1,384,2048]{2,1,0:T(8,128)(2,1)}) custom-call(bf16[384,512]{1,0:T(8,128)(2,1)S(1)} %get-tuple-element.15.refs_0_, bf16[8,128,256]{2,1,0:T(8,128)(2,1)S(1)} %shard_map.66.refs_0_.refs_1_.refs_2_, bf16[8,128,256]{2,1,0:T(8,128)(2,1)S(1)} %shard_map.67.refs_1_.refs_2_.refs_3_, ...), custom_call_target="tpu_custom_call", output_to_operand_aliasing={{1}: (8, {})} | custom-call | flops 805306368 | tf_op jit(solution)/shard_map/pallas_call | solution.py:263
  73.6 1.1 %shard_map.76 = bf16[1,384,2048]{2,1,0:T(8,128)(2,1)} custom-call(f32[384,512]{1,0:T(8,128)S(1)} %shard_map.69.refs_0_, bf16[384,512]{1,0:T(8,128)(2,1)S(1)} %get-tuple-element.17.refs_1_, bf16[8,128,256]{2,1,0:T(8,128)(2,1)S(1)} %shard_map.66.refs_0_.refs_1_.refs_2_, ...), custom_call_target="tpu_custom_call", output_to_operand_aliasing={{}: (6, {})} | custom-call | flops 201326592 | tf_op jit(solution)/shard_map/pallas_call | solution.py:263
  (37 shorter events, 1.0 us)
Async XLA Ops:
  0.0 3.0 %collective-permute-start.10 = (bf16[256,512]{1,0:T(8,128)(2,1)}, bf16[256,512]{1,0:T(8,128)(2,1)S(1)}, u32[]{:S(2)}, u32[]{:S(2)}) collective-permute-start(bf16[256,512]{1,0:T(8,128)(2,1)} %refs_0_.3), channel_id=1, source_target_pairs={{0,1},{1,0},{2,3},{3,2},{4,5},{5,4},{6,7},{7,6},{8,9},{9,8},{10,11... | collective-permute-start | bytes 786440 | tf_op jit(solution)/shard_map/ppermute | solution.py:17
  0.5 9.4 %collective-permute-start.3 = (bf16[256,512]{1,0:T(8,128)(2,1)}, bf16[256,512]{1,0:T(8,128)(2,1)S(1)}, u32[]{:S(2)}, u32[]{:S(2)}) collective-permute-start(bf16[256,512]{1,0:T(8,128)(2,1)} %refs_0_.3), channel_id=1, source_target_pairs={{0,2},{1,5},{2,0},{3,7},{4,6},{5,1},{6,4},{7,3},{8,10},{9,13},{10,... | collective-permute-start | bytes 786440 | tf_op jit(solution)/shard_map/ppermute | solution.py:17
  3.0 1.0 %copy-start.2 = (bf16[256,512]{1,0:T(8,128)(2,1)S(1)}, bf16[256,512]{1,0:T(8,128)(2,1)}, u32[]{:S(2)}) copy-start(bf16[256,512]{1,0:T(8,128)(2,1)} %refs_0_.3) | copy-start | bytes 786436
  4.0 23.5 %collective-permute-start.12 = (bf16[2,256,512]{2,1,0:T(8,128)(2,1)S(1)}, bf16[2,256,512]{2,1,0:T(8,128)(2,1)S(1)}, u32[]{:S(2)}, u32[]{:S(2)}) collective-permute-start(bf16[2,256,512]{2,1,0:T(8,128)(2,1)S(1)} %shard_map.72), channel_id=1, source_target_pairs={{0,8},{1,17},{2,10},{3,19},{4,12},{5,21},{6,14},{7,23},{8,0},{9,25... | collective-permute-start | bytes 1572872 | tf_op jit(solution)/shard_map/ppermute | solution.py:330
  5.9 19.9 %collective-permute-start.1 = (bf16[256,512]{1,0:T(8,128)(2,1)S(1)}, bf16[256,512]{1,0:T(8,128)(2,1)S(1)}, u32[]{:S(2)}, u32[]{:S(2)}) collective-permute-start(bf16[256,512]{1,0:T(8,128)(2,1)S(1)} %copy-done.2), channel_id=1, source_target_pairs={{0,24},{8,16},{16,8},{24,0},{1,25},{9,17},{17,9},{25,1},{2,26},{10... | collective-permute-start | bytes 786440 | tf_op jit(solution)/shard_map/ppermute | solution.py:17
  8.3 19.0 %collective-permute-start.9 = (bf16[256,512]{1,0:T(8,128)(2,1)S(1)}, bf16[256,512]{1,0:T(8,128)(2,1)S(1)}, u32[]{:S(2)}, u32[]{:S(2)}) collective-permute-start(bf16[256,512]{1,0:T(8,128)(2,1)S(1)} %copy-done.2), channel_id=1, source_target_pairs={{0,4},{1,3},{2,6},{3,1},{4,0},{5,7},{6,2},{7,5},{8,12},{9,11},{10,... | collective-permute-start | bytes 786440 | tf_op jit(solution)/shard_map/ppermute | solution.py:17
  9.9 17.4 %collective-permute-start.4 = (bf16[256,512]{1,0:T(8,128)(2,1)S(1)}, bf16[256,512]{1,0:T(8,128)(2,1)S(1)}, u32[]{:S(2)}, u32[]{:S(2)}) collective-permute-start(bf16[256,512]{1,0:T(8,128)(2,1)S(1)} %collective-permute-done.3.refs_0_), channel_id=1, source_target_pairs={{0,4},{1,3},{2,6},{3,1},{4,0},{5,7},{6,2},{7,5},{8,12},{9,11},{10,... | collective-permute-start | bytes 786440 | tf_op jit(solution)/shard_map/ppermute | solution.py:17
  25.8 16.9 %collective-permute-start.7 = (bf16[256,512]{1,0:T(8,128)(2,1)S(1)}, bf16[256,512]{1,0:T(8,128)(2,1)S(1)}, u32[]{:S(2)}, u32[]{:S(2)}) collective-permute-start(bf16[256,512]{1,0:T(8,128)(2,1)S(1)} %collective-permute-done.1), channel_id=1, source_target_pairs={{0,2},{1,5},{2,0},{3,7},{4,6},{5,1},{6,4},{7,3},{8,10},{9,13},{10,... | collective-permute-start | bytes 786440 | tf_op jit(solution)/shard_map/ppermute | solution.py:17
  27.4 1.4 %copy-start = (bf16[1,384,2048]{2,1,0:T(8,128)(2,1)S(1)}, bf16[1,384,2048]{2,1,0:T(8,128)(2,1)}, u32[]{:S(2)}) copy-start(bf16[1,384,2048]{2,1,0:T(8,128)(2,1)} %refs_0_.2) | copy-start | bytes 4718596
  27.4 1.9 %copy-start.1 = (bf16[1,384,2048]{2,1,0:T(8,128)(2,1)S(1)}, bf16[1,384,2048]{2,1,0:T(8,128)(2,1)}, u32[]{:S(2)}) copy-start(bf16[1,384,2048]{2,1,0:T(8,128)(2,1)} %refs_1_.1) | copy-start | bytes 4718596
  27.4 1.9 %copy-start.4 = (bf16[31,2048]{1,0:T(8,128)(2,1)S(1)}, bf16[31,2048]{1,0:T(8,128)(2,1)}, u32[]{:S(2)}) copy-start(bf16[31,2048]{1,0:T(8,128)(2,1)} %refs_2_.1) | copy-start | bytes 380932
  27.4 30.1 %collective-permute-start.11 = (bf16[3,256,512]{2,1,0:T(8,128)(2,1)S(1)}, bf16[3,256,512]{2,1,0:T(8,128)(2,1)S(1)}, u32[]{:S(2)}, u32[]{:S(2)}) collective-permute-start(bf16[3,256,512]{2,1,0:T(8,128)(2,1)S(1)} %shard_map.70), channel_id=1, source_target_pairs={{0,1},{1,0},{2,3},{3,2},{4,5},{5,4},{6,7},{7,6},{8,9},{9,8},{10,11... | collective-permute-start | bytes 2359304 | tf_op jit(solution)/shard_map/ppermute | solution.py:17
  27.5 15.7 %collective-permute-start.13 = (bf16[2,256,512]{2,1,0:T(8,128)(2,1)S(1)}, bf16[2,256,512]{2,1,0:T(8,128)(2,1)S(1)}, u32[]{:S(2)}, u32[]{:S(2)}) collective-permute-start(bf16[2,256,512]{2,1,0:T(8,128)(2,1)S(1)} %collective-permute-done.12.refs_4_), channel_id=1, source_target_pairs={{0,2},{1,5},{2,0},{3,7},{4,6},{5,1},{6,4},{7,3},{8,10},{9,13},{10,... | collective-permute-start | bytes 1572872 | tf_op jit(solution)/shard_map/ppermute | solution.py:17
  29.2 28.9 %copy-start.5 = (f32[2048]{0:T(1024)S(1)}, f32[2048]{0:T(1024)}, u32[]{:S(2)}) copy-start(f32[2048]{0:T(1024)} %param.9) | copy-start | bytes 24580
  29.2 28.9 %copy-start.6 = (f32[2048]{0:T(1024)S(1)}, f32[2048]{0:T(1024)}, u32[]{:S(2)}) copy-start(f32[2048]{0:T(1024)} %param.10) | copy-start | bytes 24580
  30.4 8.1 %collective-permute-start = (bf16[32,2048]{1,0:T(8,128)(2,1)S(1)}, bf16[32,2048]{1,0:T(8,128)(2,1)S(1)}, u32[]{:S(2)}, u32[]{:S(2)}) collective-permute-start(bf16[32,2048]{1,0:T(8,128)(2,1)S(1)} %get-tuple-element.14), channel_id=1, source_target_pairs={{0,8},{8,16},{16,24},{24,0},{1,9},{9,17},{17,25},{25,1},{2,10},{10... | collective-permute-start | bytes 393224 | tf_op jit(solution)/shard_map/ppermute | solution.py:299
  35.4 9.3 %collective-permute-start.8 = (bf16[256,512]{1,0:T(8,128)(2,1)S(1)}, bf16[256,512]{1,0:T(8,128)(2,1)S(1)}, u32[]{:S(2)}, u32[]{:S(2)}) collective-permute-start(bf16[256,512]{1,0:T(8,128)(2,1)S(1)} %collective-permute-done.1), channel_id=1, source_target_pairs={{0,4},{1,3},{2,6},{3,1},{4,0},{5,7},{6,2},{7,5},{8,12},{9,11},{10,... | collective-permute-start | bytes 786440 | tf_op jit(solution)/shard_map/ppermute | solution.py:17
  38.5 10.4 %collective-permute-start.5 = (bf16[256,512]{1,0:T(8,128)(2,1)S(1)}, bf16[256,512]{1,0:T(8,128)(2,1)S(1)}, u32[]{:S(2)}, u32[]{:S(2)}) collective-permute-start(bf16[256,512]{1,0:T(8,128)(2,1)S(1)} %collective-permute-done.4.refs_2_), channel_id=1, source_target_pairs={{0,24},{8,16},{16,8},{24,0},{1,25},{9,17},{17,9},{25,1},{2,26},{10... | collective-permute-start | bytes 786440 | tf_op jit(solution)/shard_map/ppermute | solution.py:17
  42.7 9.2 %collective-permute-start.14 = (bf16[2,256,512]{2,1,0:T(8,128)(2,1)S(1)}, bf16[2,256,512]{2,1,0:T(8,128)(2,1)S(1)}, u32[]{:S(2)}, u32[]{:S(2)}) collective-permute-start(bf16[2,256,512]{2,1,0:T(8,128)(2,1)S(1)} %collective-permute-done.12.refs_4_), channel_id=1, source_target_pairs={{0,4},{1,3},{2,6},{3,1},{4,0},{5,7},{6,2},{7,5},{8,12},{9,11},{10,... | collective-permute-start | bytes 1572872 | tf_op jit(solution)/shard_map/ppermute | solution.py:17
  43.2 14.3 %collective-permute-start.15 = (bf16[2,256,512]{2,1,0:T(8,128)(2,1)S(1)}, bf16[2,256,512]{2,1,0:T(8,128)(2,1)S(1)}, u32[]{:S(2)}, u32[]{:S(2)}) collective-permute-start(bf16[2,256,512]{2,1,0:T(8,128)(2,1)S(1)} %collective-permute-done.13.refs_5_), channel_id=1, source_target_pairs={{0,4},{1,3},{2,6},{3,1},{4,0},{5,7},{6,2},{7,5},{8,12},{9,11},{10,... | collective-permute-start | bytes 1572872 | tf_op jit(solution)/shard_map/ppermute | solution.py:17
  44.7 4.2 %collective-permute-start.2 = (bf16[256,512]{1,0:T(8,128)(2,1)S(1)}, bf16[256,512]{1,0:T(8,128)(2,1)S(1)}, u32[]{:S(2)}, u32[]{:S(2)}) collective-permute-start(bf16[256,512]{1,0:T(8,128)(2,1)S(1)} %collective-permute-done.1), channel_id=1, source_target_pairs={{0,1},{1,0},{2,3},{3,2},{4,5},{5,4},{6,7},{7,6},{8,9},{9,8},{10,11... | collective-permute-start | bytes 786440 | tf_op jit(solution)/shard_map/ppermute | solution.py:17
  48.9 1.5 %collective-permute-start.6 = (bf16[256,512]{1,0:T(8,128)(2,1)S(1)}, bf16[256,512]{1,0:T(8,128)(2,1)S(1)}, u32[]{:S(2)}, u32[]{:S(2)}) collective-permute-start(bf16[256,512]{1,0:T(8,128)(2,1)S(1)} %collective-permute-done.5), channel_id=1, source_target_pairs={{0,1},{1,0},{2,3},{3,2},{4,5},{5,4},{6,7},{7,6},{8,9},{9,8},{10,11... | collective-permute-start | bytes 786440 | tf_op jit(solution)/shard_map/ppermute | solution.py:17
  48.9 23.1 %collective-permute-start.16 = (bf16[2,256,512]{2,1,0:T(8,128)(2,1)S(1)}, bf16[2,256,512]{2,1,0:T(8,128)(2,1)S(1)}, u32[]{:S(2)}, u32[]{:S(2)}) collective-permute-start(bf16[2,256,512]{2,1,0:T(8,128)(2,1)S(1)} %collective-permute-done.12.refs_4_), channel_id=1, source_target_pairs={{0,1},{1,0},{2,3},{3,2},{4,5},{5,4},{6,7},{7,6},{8,9},{9,8},{10,11... | collective-permute-start | bytes 1572872 | tf_op jit(solution)/shard_map/ppermute | solution.py:17
  50.4 21.6 %collective-permute-start.17 = (bf16[2,256,512]{2,1,0:T(8,128)(2,1)S(1)}, bf16[2,256,512]{2,1,0:T(8,128)(2,1)S(1)}, u32[]{:S(2)}, u32[]{:S(2)}) collective-permute-start(bf16[2,256,512]{2,1,0:T(8,128)(2,1)S(1)} %collective-permute-done.13.refs_5_), channel_id=1, source_target_pairs={{0,1},{1,0},{2,3},{3,2},{4,5},{5,4},{6,7},{7,6},{8,9},{9,8},{10,11... | collective-permute-start | bytes 1572872 | tf_op jit(solution)/shard_map/ppermute | solution.py:17
  51.9 20.2 %collective-permute-start.18 = (bf16[2,256,512]{2,1,0:T(8,128)(2,1)S(1)}, bf16[2,256,512]{2,1,0:T(8,128)(2,1)S(1)}, u32[]{:S(2)}, u32[]{:S(2)}) collective-permute-start(bf16[2,256,512]{2,1,0:T(8,128)(2,1)S(1)} %collective-permute-done.14.refs_6_), channel_id=1, source_target_pairs={{0,1},{1,0},{2,3},{3,2},{4,5},{5,4},{6,7},{7,6},{8,9},{9,8},{10,11... | collective-permute-start | bytes 1572872 | tf_op jit(solution)/shard_map/ppermute | solution.py:17
  57.5 14.6 %collective-permute-start.19 = (bf16[2,256,512]{2,1,0:T(8,128)(2,1)S(1)}, bf16[2,256,512]{2,1,0:T(8,128)(2,1)S(1)}, u32[]{:S(2)}, u32[]{:S(2)}) collective-permute-start(bf16[2,256,512]{2,1,0:T(8,128)(2,1)S(1)} %collective-permute-done.15.refs_7_), channel_id=1, source_target_pairs={{0,1},{1,0},{2,3},{3,2},{4,5},{5,4},{6,7},{7,6},{8,9},{9,8},{10,11... | collective-permute-start | bytes 1572872 | tf_op jit(solution)/shard_map/ppermute | solution.py:17
  57.5 16.0 %collective-permute-start.20 = (bf16[2,256,512]{2,1,0:T(8,128)(2,1)S(1)}, bf16[2,256,512]{2,1,0:T(8,128)(2,1)S(1)}, u32[]{:S(2)}, u32[]{:S(2)}) collective-permute-start(bf16[2,256,512]{2,1,0:T(8,128)(2,1)S(1)} %shard_map.75), channel_id=1, source_target_pairs={{0,1},{1,0},{2,3},{3,2},{4,5},{5,4},{6,7},{7,6},{8,9},{9,8},{10,11... | collective-permute-start | bytes 1572872 | tf_op jit(solution)/shard_map/ppermute | solution.py:17
  68.6 1.0 %copy-start.3 = (bf16[256,512]{1,0:T(8,128)(2,1)S(1)}, bf16[256,512]{1,0:T(8,128)(2,1)}, u32[]{:S(2)}) copy-start(bf16[256,512]{1,0:T(8,128)(2,1)} %refs_0_.3) | copy-start | bytes 786436

commit v5 on v4

--- a/solution.py
+++ b/solution.py
@@ -235,11 +235,15 @@
 
 
 def last_kernel(chunks, slots, *refs):
-    (begun, third) = refs[:2]
-    (acts, weights) = (refs[2 : 2 + chunks], refs[2 + chunks : -4])
+    (begun, second, third) = refs[:3]
+    (acts, weights) = (refs[3 : 3 + chunks], refs[3 + chunks : -4])
     (out_ref, buf, sem) = refs[-3:]
     rows = acts[0].shape[1]
-    copies = [put(third, out_ref, pl.ds(0, third.shape[0]), 2 - lax.axis_index("dp") % 2, sem.at[2])]
+    parity = lax.axis_index("dp") % 2
+    copies = [
+        put(block, out_ref, pl.ds(0, block.shape[0]), step, sem.at[index])
+        for index, (block, step) in enumerate(((second, 1 + parity), (third, 2 - parity)), 2)
+    ]
     first = 0
     for half, count in enumerate((chunks - chunks // 2, chunks // 2)):
         span = pl.ds(first * rows, count * rows)
@@ -387,9 +391,7 @@
         )
 
     block, out = middle(pairs, ((0, 4), (1, 6), (2, 5), (3, 7)), lambda parity: 0, done[0], None)
-    third, out = middle(
-        pairs_other, ((4, 0), (5, 2), (6, 1), (7, 3)), lambda parity: 1 + parity, block, out
-    )
+    third = project(pairs_other, ((4, 0), (5, 2), (6, 1), (7, 3)))
     (piece, first, second, forwarded, partner) = singles[1]
     last = named(forwarded, "dp", 1, 1)
     swapped_3 = both((first, second))
@@ -398,12 +400,12 @@
         ((0,), (4,), (3,), (7,), (1,), (2,)),
         jnp.float32,
     )
-    operands = [begun, third] + acts + [swapped_3, out]
+    operands = [begun, block, third] + acts + [swapped_3, out]
     return kernel_call(
         functools.partial(last_kernel, chunks, ((5, 6),)),
         operands,
         [whole],
-        (pltpu.VMEM((tok_rows, width), jnp.bfloat16), pltpu.SemaphoreType.DMA((3,))),
+        (pltpu.VMEM((tok_rows, width), jnp.bfloat16), pltpu.SemaphoreType.DMA((4,))),
         out_spec=ANY,
         flops=4 * tok_rows * depth * width,
         aliases={len(operands) - 1: 0},

time: 74.9 us -> 76.4 us (1.020)
  starting transfers between devices: 24.3 us -> 26.6 us
  local copies, waits for them, and re-layouts: 2.33 us -> 1.18 us
  waiting for transfers between devices: 30.2 us -> 31 us
    ppermute x19, starting transfers between devices: 17.5 us -> 19.5 us  [swapped(): lax.ppermute(value, axis, [(index, index ^ mask_of(index)) for index in r...]
    ppermute x19, waiting for transfers between devices: 27.6 us -> 29.5 us  [swapped(): lax.ppermute(value, axis, [(index, index ^ mask_of(index)) for index in r...]
    ppermute x1, waiting for transfers between devices: 2.66 us -> 1.44 us  [square_plane(): lax.ppermute(tail, 'sp', [(source, (source + 1) % layers) for source in r...]
    unnamed x14, local copies, waits for them, and re-layouts: 2.33 us -> 1.18 us
  transfers between devices with their start and end apart: 21 -> 21, of which waited for: 6 -> 4; matrix products, arithmetic and copies ran while one was open for 0% -> 0% of each run, Pallas kernels for 22% -> 21%
where the time goes in v5:
time: 76.4 us; the launch traced here: 76.2 us
  waiting for transfers between devices  31 us (41%)
  starting transfers between devices  26.6 us (35%)
  Pallas kernels  17.2 us (23%)
  local copies, waits for them, and re-layouts  1.18 us (2%)
    ppermute x19, waiting for transfers between devices, swapped(): lax.ppermute(value, axis, [(index, index ^ mask_of(index)) for index in r...  29.5 us
    ppermute x19, starting transfers between devices, swapped(): lax.ppermute(value, axis, [(index, index ^ mask_of(index)) for index in r...  19.5 us
    pallas_call x13, Pallas kernels, kernel_call(): pl.pallas_call(body, out_shape=outs, in_specs=[ANY if index in (aliases o...  17.2 us
    ppermute x1, starting transfers between devices, square_plane(): lax.ppermute(tail, 'sp', [(source, (source + 1) % layers) for source in r...  5.22 us
    ppermute x1, starting transfers between devices, square_plane(): arrived = lax.ppermute(chip, ('sp', 'dp'), route)  1.86 us
  transfers between devices with their start and end apart: 21, of which 4 were waited for; matrix products, arithmetic and copies ran while one was open for 0% of the time, Pallas kernels for 21%

profile of v5, /device:TPU:0, one launch (start us, length us, event | category | flops | bytes accessed | tf_op | source)
XLA Modules:
  0.0 76.2 jit_solution(4459213414923148092)
XLA Ops:
  0.0 0.5 collective-permute-start.10
  0.5 2.5 %collective-permute-start.3 = (bf16[256,512]{1,0:T(8,128)(2,1)}, bf16[256,512]{1,0:T(8,128)(2,1)S(1)}, u32[]{:S(2)}, u32[]{:S(2)}) collective-permute-start(bf16[256,512]{1,0:T(8,128)(2,1)} %refs_0_.3), channel_id=1, source_target_pairs={{0,2},{1,5},{2,0},{3,7},{4,6},{5,1},{6,4},{7,3},{8,10},{9,13},{10,... | collective-permute-start | bytes 786440 | tf_op jit(solution)/shard_map/ppermute | solution.py:17
  3.0 1.0 %copy-done.2 = bf16[256,512]{1,0:T(8,128)(2,1)S(1)} copy-done((bf16[256,512]{1,0:T(8,128)(2,1)S(1)}, bf16[256,512]{1,0:T(8,128)(2,1)}, u32[]{:S(2)}) %copy-start.2) | copy-done | bytes 262168
  4.0 1.9 %collective-permute-start.12 = (bf16[2,256,512]{2,1,0:T(8,128)(2,1)S(1)}, bf16[2,256,512]{2,1,0:T(8,128)(2,1)S(1)}, u32[]{:S(2)}, u32[]{:S(2)}) collective-permute-start(bf16[2,256,512]{2,1,0:T(8,128)(2,1)S(1)} %shard_map.72), channel_id=1, source_target_pairs={{0,8},{1,17},{2,10},{3,19},{4,12},{5,21},{6,14},{7,23},{8,0},{9,25... | collective-permute-start | bytes 1572872 | tf_op jit(solution)/shard_map/ppermute | solution.py:334
  5.9 2.5 %collective-permute-start.1 = (bf16[256,512]{1,0:T(8,128)(2,1)S(1)}, bf16[256,512]{1,0:T(8,128)(2,1)S(1)}, u32[]{:S(2)}, u32[]{:S(2)}) collective-permute-start(bf16[256,512]{1,0:T(8,128)(2,1)S(1)} %copy-done.2), channel_id=1, source_target_pairs={{0,24},{8,16},{16,8},{24,0},{1,25},{9,17},{17,9},{25,1},{2,26},{10... | collective-permute-start | bytes 786440 | tf_op jit(solution)/shard_map/ppermute | solution.py:17
  8.3 1.5 %collective-permute-start.9 = (bf16[256,512]{1,0:T(8,128)(2,1)S(1)}, bf16[256,512]{1,0:T(8,128)(2,1)S(1)}, u32[]{:S(2)}, u32[]{:S(2)}) collective-permute-start(bf16[256,512]{1,0:T(8,128)(2,1)S(1)} %copy-done.2), channel_id=1, source_target_pairs={{0,4},{1,3},{2,6},{3,1},{4,0},{5,7},{6,2},{7,5},{8,12},{9,11},{10,... | collective-permute-start | bytes 786440 | tf_op jit(solution)/shard_map/ppermute | solution.py:17
  9.9 0.5 collective-permute-start.4
  10.4 15.4 %collective-permute-done.1 = bf16[256,512]{1,0:T(8,128)(2,1)S(1)} collective-permute-done((bf16[256,512]{1,0:T(8,128)(2,1)S(1)}, bf16[256,512]{1,0:T(8,128)(2,1)S(1)}, u32[]{:S(2)}, u32[]{:S(2)}) %collective-permute-start.1) | collective-permute-done | bytes 262176 | tf_op jit(solution)/shard_map/ppermute | solution.py:17
  25.9 0.6 collective-permute-start.11
  26.5 1.5 %collective-permute-start.13 = (bf16[2,256,512]{2,1,0:T(8,128)(2,1)S(1)}, bf16[2,256,512]{2,1,0:T(8,128)(2,1)S(1)}, u32[]{:S(2)}, u32[]{:S(2)}) collective-permute-start(bf16[2,256,512]{2,1,0:T(8,128)(2,1)S(1)} %collective-permute-done.12.refs_4_), channel_id=1, source_target_pairs={{0,2},{1,5},{2,0},{3,7},{4,6},{5,1},{6,4},{7,3},{8,10},{9,13},{10,... | collective-permute-start | bytes 1572872 | tf_op jit(solution)/shard_map/ppermute | solution.py:17
  28.0 1.2 %shard_map.65 = (f32[16,384,128]{2,1,0:T(8,128)S(1)}, bf16[32,2048]{1,0:T(8,128)(2,1)S(1)}, f32[16,32,128]{2,1,0:T(8,128)S(1)}) custom-call(bf16[1,384,2048]{2,1,0:T(8,128)(2,1)S(1)} %copy-done, bf16[1,384,2048]{2,1,0:T(8,128)(2,1)S(1)} %copy-done.1, bf16[31,2048]{1,0:T(8,128)(2,1)S(1)} %copy-done.4, bf16[16,128]{1,0:T(8,128)(2,1)S(1)} %shard_map.64.refs_3_), custom_call_target="tpu_custom_call" | custom-call | flops 31457280 | tf_op jit(solution)/shard_map/pallas_call | solution.py:267
  29.2 5.2 %collective-permute-start = (bf16[32,2048]{1,0:T(8,128)(2,1)S(1)}, bf16[32,2048]{1,0:T(8,128)(2,1)S(1)}, u32[]{:S(2)}, u32[]{:S(2)}) collective-permute-start(bf16[32,2048]{1,0:T(8,128)(2,1)S(1)} %get-tuple-element.12), channel_id=1, source_target_pairs={{0,8},{8,16},{16,24},{24,0},{1,9},{9,17},{17,25},{25,1},{2,10},{10... | collective-permute-start | bytes 393224 | tf_op jit(solution)/shard_map/ppermute | solution.py:303
  34.4 1.5 %collective-permute-start.7 = (bf16[256,512]{1,0:T(8,128)(2,1)S(1)}, bf16[256,512]{1,0:T(8,128)(2,1)S(1)}, u32[]{:S(2)}, u32[]{:S(2)}) collective-permute-start(bf16[256,512]{1,0:T(8,128)(2,1)S(1)} %collective-permute-done.1), channel_id=1, source_target_pairs={{0,2},{1,5},{2,0},{3,7},{4,6},{5,1},{6,4},{7,3},{8,10},{9,13},{10,... | collective-permute-start | bytes 786440 | tf_op jit(solution)/shard_map/ppermute | solution.py:17
  35.9 1.4 %collective-permute-done.refs_4_ = bf16[32,2048]{1,0:T(8,128)(2,1)S(1)} collective-permute-done((bf16[32,2048]{1,0:T(8,128)(2,1)S(1)}, bf16[32,2048]{1,0:T(8,128)(2,1)S(1)}, u32[]{:S(2)}, u32[]{:S(2)}) %collective-permute-start) | collective-permute-done | bytes 131104 | tf_op jit(solution)/shard_map/ppermute | solution.py:303
  37.3 3.8 %collective-permute-start.5 = (bf16[256,512]{1,0:T(8,128)(2,1)S(1)}, bf16[256,512]{1,0:T(8,128)(2,1)S(1)}, u32[]{:S(2)}, u32[]{:S(2)}) collective-permute-start(bf16[256,512]{1,0:T(8,128)(2,1)S(1)} %collective-permute-done.4.refs_2_), channel_id=1, source_target_pairs={{0,24},{8,16},{16,8},{24,0},{1,25},{9,17},{17,9},{25,1},{2,26},{10... | collective-permute-start | bytes 786440 | tf_op jit(solution)/shard_map/ppermute | solution.py:17
  41.1 1.5 %collective-permute-start.14 = (bf16[2,256,512]{2,1,0:T(8,128)(2,1)S(1)}, bf16[2,256,512]{2,1,0:T(8,128)(2,1)S(1)}, u32[]{:S(2)}, u32[]{:S(2)}) collective-permute-start(bf16[2,256,512]{2,1,0:T(8,128)(2,1)S(1)} %collective-permute-done.12.refs_4_), channel_id=1, source_target_pairs={{0,4},{1,3},{2,6},{3,1},{4,0},{5,7},{6,2},{7,5},{8,12},{9,11},{10,... | collective-permute-start | bytes 1572872 | tf_op jit(solution)/shard_map/ppermute | solution.py:17
  42.7 0.5 collective-permute-start.15
  43.2 1.5 %collective-permute-start.8 = (bf16[256,512]{1,0:T(8,128)(2,1)S(1)}, bf16[256,512]{1,0:T(8,128)(2,1)S(1)}, u32[]{:S(2)}, u32[]{:S(2)}) collective-permute-start(bf16[256,512]{1,0:T(8,128)(2,1)S(1)} %collective-permute-done.1), channel_id=1, source_target_pairs={{0,4},{1,3},{2,6},{3,1},{4,0},{5,7},{6,2},{7,5},{8,12},{9,11},{10,... | collective-permute-start | bytes 786440 | tf_op jit(solution)/shard_map/ppermute | solution.py:17
  44.7 2.4 %collective-permute-done.5 = bf16[256,512]{1,0:T(8,128)(2,1)S(1)} collective-permute-done((bf16[256,512]{1,0:T(8,128)(2,1)S(1)}, bf16[256,512]{1,0:T(8,128)(2,1)S(1)}, u32[]{:S(2)}, u32[]{:S(2)}) %collective-permute-start.5) | collective-permute-done | bytes 262176 | tf_op jit(solution)/shard_map/ppermute | solution.py:17
  47.2 11.6 %collective-permute-done.8.refs_1_ = bf16[256,512]{1,0:T(8,128)(2,1)S(1)} collective-permute-done((bf16[256,512]{1,0:T(8,128)(2,1)S(1)}, bf16[256,512]{1,0:T(8,128)(2,1)S(1)}, u32[]{:S(2)}, u32[]{:S(2)}) %collective-permute-start.8) | collective-permute-done | bytes 262176 | tf_op jit(solution)/shard_map/ppermute | solution.py:17
  58.8 0.5 collective-permute-start.17
  59.4 0.4 collective-permute-start.19
  59.8 0.1 collective-permute-start.20
  60.0 3.4 %shard_map.67.refs_1_.refs_2_.refs_4_ = bf16[8,128,256]{2,1,0:T(8,128)(2,1)S(1)} custom-call(f32[16,384,128]{2,1,0:T(8,128)S(1)} %get-tuple-element.10.refs_0_, f32[16,32,128]{2,1,0:T(8,128)S(1)} %get-tuple-element.11.refs_1_, f32[16,1,128]{2,1,0:T(1,128)S(1)} %bitcast.24, f32[16,1,128]{2,1,0:T(1,128)S(1)} %bitcast.27), custom_call_target="tpu_custom_call" | custom-call | flops 16252928 | tf_op jit(solution)/shard_map/pallas_call | solution.py:267
  63.4 3.4 %shard_map.68.refs_2_.refs_3_.refs_5_ = bf16[8,128,256]{2,1,0:T(8,128)(2,1)S(1)} custom-call(f32[16,384,128]{2,1,0:T(8,128)S(1)} %get-tuple-element.10.refs_0_, f32[16,32,128]{2,1,0:T(8,128)S(1)} %get-tuple-element.11.refs_1_, f32[16,1,128]{2,1,0:T(1,128)S(1)} %bitcast.25, f32[16,1,128]{2,1,0:T(1,128)S(1)} %bitcast.28), custom_call_target="tpu_custom_call" | custom-call | flops 16252928 | tf_op jit(solution)/shard_map/pallas_call | solution.py:267
  66.8 3.6 %shard_map.66.refs_0_.refs_1_.refs_3_ = bf16[8,128,256]{2,1,0:T(8,128)(2,1)S(1)} custom-call(f32[16,384,128]{2,1,0:T(8,128)S(1)} %get-tuple-element.10.refs_0_, f32[16,32,128]{2,1,0:T(8,128)S(1)} %get-tuple-element.11.refs_1_, f32[16,1,128]{2,1,0:T(1,128)S(1)} %bitcast.26, f32[16,1,128]{2,1,0:T(1,128)S(1)} %bitcast.29, ...), custom_call_target="tpu_custom_call" | custom-call | flops 16252928 | tf_op jit(solution)/shard_map/pallas_call | solution.py:267
  70.5 0.8 %shard_map.69.refs_0_ = f32[384,512]{1,0:T(8,128)S(1)} custom-call(bf16[8,128,256]{2,1,0:T(8,128)(2,1)S(1)} %shard_map.66.refs_0_.refs_1_.refs_3_, bf16[8,128,256]{2,1,0:T(8,128)(2,1)S(1)} %shard_map.67.refs_1_.refs_2_.refs_4_, bf16[8,128,256]{2,1,0:T(8,128)(2,1)S(1)} %shard_map.68.refs_2_.refs_3_.refs_5_, bf16[1,256,512]{2,1,0:T(8,128)(2,1)S(1)} %bitcast.20, ...), custom_call_target="tpu_custom_call" | custom-call | flops 603979776 | tf_op jit(solution)/shard_map/pallas_call | solution.py:267
  71.3 0.2 copy-done.3
  71.4 1.0 %shard_map.71.refs_0_ = bf16[384,512]{1,0:T(8,128)(2,1)S(1)} custom-call(bf16[8,128,256]{2,1,0:T(8,128)(2,1)S(1)} %shard_map.66.refs_0_.refs_1_.refs_3_, bf16[8,128,256]{2,1,0:T(8,128)(2,1)S(1)} %shard_map.67.refs_1_.refs_2_.refs_4_, bf16[8,128,256]{2,1,0:T(8,128)(2,1)S(1)} %shard_map.68.refs_2_.refs_3_.refs_5_, bf16[1,256,512]{2,1,0:T(8,128)(2,1)S(1)} %bitcast.13, ...), custom_call_target="tpu_custom_call" | custom-call | flops 805306368 | tf_op jit(solution)/shard_map/pallas_call | solution.py:267
  72.4 1.5 %shard_map.73 = (bf16[384,512]{1,0:T(8,128)(2,1)S(1)}, bf16[1,384,2048]{2,1,0:T(8,128)(2,1)}) custom-call(bf16[384,512]{1,0:T(8,128)(2,1)S(1)} %shard_map.71.refs_0_, bf16[8,128,256]{2,1,0:T(8,128)(2,1)S(1)} %shard_map.66.refs_0_.refs_1_.refs_3_, bf16[8,128,256]{2,1,0:T(8,128)(2,1)S(1)} %shard_map.67.refs_1_.refs_2_.refs_4_, ...), custom_call_target="tpu_custom_call" | custom-call | flops 805306368 | tf_op jit(solution)/shard_map/pallas_call | solution.py:267
  73.9 1.0 %shard_map.74.refs_2_ = bf16[384,512]{1,0:T(8,128)(2,1)S(1)} custom-call(bf16[8,128,256]{2,1,0:T(8,128)(2,1)S(1)} %shard_map.66.refs_0_.refs_1_.refs_3_, bf16[8,128,256]{2,1,0:T(8,128)(2,1)S(1)} %shard_map.67.refs_1_.refs_2_.refs_4_, bf16[8,128,256]{2,1,0:T(8,128)(2,1)S(1)} %shard_map.68.refs_2_.refs_3_.refs_5_, ...), custom_call_target="tpu_custom_call" | custom-call | flops 805306368 | tf_op jit(solution)/shard_map/pallas_call | solution.py:267
  74.9 1.3 %shard_map.76 = bf16[1,384,2048]{2,1,0:T(8,128)(2,1)} custom-call(f32[384,512]{1,0:T(8,128)S(1)} %shard_map.69.refs_0_, bf16[384,512]{1,0:T(8,128)(2,1)S(1)} %get-tuple-element.13.refs_1_, bf16[384,512]{1,0:T(8,128)(2,1)S(1)} %shard_map.74.refs_2_, bf16[8,128,256]{2,1,0:T(8,128)(2,1)S(1)} %shard_map.66.refs_0_.refs_1_.refs_3_, ...), custom_call_target="tpu_custom_call", output_to_operand_aliasing={{}: (7, {})} | custom-call | flops 201326592 | tf_op jit(solution)/shard_map/pallas_call | solution.py:267
  (37 shorter events, 0.3 us)
Async XLA Ops:
  0.0 3.0 %collective-permute-start.10 = (bf16[256,512]{1,0:T(8,128)(2,1)}, bf16[256,512]{1,0:T(8,128)(2,1)S(1)}, u32[]{:S(2)}, u32[]{:S(2)}) collective-permute-start(bf16[256,512]{1,0:T(8,128)(2,1)} %refs_0_.3), channel_id=1, source_target_pairs={{0,1},{1,0},{2,3},{3,2},{4,5},{5,4},{6,7},{7,6},{8,9},{9,8},{10,11... | collective-permute-start | bytes 786440 | tf_op jit(solution)/shard_map/ppermute | solution.py:17
  0.5 9.4 %collective-permute-start.3 = (bf16[256,512]{1,0:T(8,128)(2,1)}, bf16[256,512]{1,0:T(8,128)(2,1)S(1)}, u32[]{:S(2)}, u32[]{:S(2)}) collective-permute-start(bf16[256,512]{1,0:T(8,128)(2,1)} %refs_0_.3), channel_id=1, source_target_pairs={{0,2},{1,5},{2,0},{3,7},{4,6},{5,1},{6,4},{7,3},{8,10},{9,13},{10,... | collective-permute-start | bytes 786440 | tf_op jit(solution)/shard_map/ppermute | solution.py:17
  3.0 1.0 %copy-start.2 = (bf16[256,512]{1,0:T(8,128)(2,1)S(1)}, bf16[256,512]{1,0:T(8,128)(2,1)}, u32[]{:S(2)}) copy-start(bf16[256,512]{1,0:T(8,128)(2,1)} %refs_0_.3) | copy-start | bytes 786436
  4.0 22.5 %collective-permute-start.12 = (bf16[2,256,512]{2,1,0:T(8,128)(2,1)S(1)}, bf16[2,256,512]{2,1,0:T(8,128)(2,1)S(1)}, u32[]{:S(2)}, u32[]{:S(2)}) collective-permute-start(bf16[2,256,512]{2,1,0:T(8,128)(2,1)S(1)} %shard_map.72), channel_id=1, source_target_pairs={{0,8},{1,17},{2,10},{3,19},{4,12},{5,21},{6,14},{7,23},{8,0},{9,25... | collective-permute-start | bytes 1572872 | tf_op jit(solution)/shard_map/ppermute | solution.py:334
  5.9 19.9 %collective-permute-start.1 = (bf16[256,512]{1,0:T(8,128)(2,1)S(1)}, bf16[256,512]{1,0:T(8,128)(2,1)S(1)}, u32[]{:S(2)}, u32[]{:S(2)}) collective-permute-start(bf16[256,512]{1,0:T(8,128)(2,1)S(1)} %copy-done.2), channel_id=1, source_target_pairs={{0,24},{8,16},{16,8},{24,0},{1,25},{9,17},{17,9},{25,1},{2,26},{10... | collective-permute-start | bytes 786440 | tf_op jit(solution)/shard_map/ppermute | solution.py:17
  8.3 17.5 %collective-permute-start.9 = (bf16[256,512]{1,0:T(8,128)(2,1)S(1)}, bf16[256,512]{1,0:T(8,128)(2,1)S(1)}, u32[]{:S(2)}, u32[]{:S(2)}) collective-permute-start(bf16[256,512]{1,0:T(8,128)(2,1)S(1)} %copy-done.2), channel_id=1, source_target_pairs={{0,4},{1,3},{2,6},{3,1},{4,0},{5,7},{6,2},{7,5},{8,12},{9,11},{10,... | collective-permute-start | bytes 786440 | tf_op jit(solution)/shard_map/ppermute | solution.py:17
  9.9 16.0 %collective-permute-start.4 = (bf16[256,512]{1,0:T(8,128)(2,1)S(1)}, bf16[256,512]{1,0:T(8,128)(2,1)S(1)}, u32[]{:S(2)}, u32[]{:S(2)}) collective-permute-start(bf16[256,512]{1,0:T(8,128)(2,1)S(1)} %collective-permute-done.3.refs_0_), channel_id=1, source_target_pairs={{0,4},{1,3},{2,6},{3,1},{4,0},{5,7},{6,2},{7,5},{8,12},{9,11},{10,... | collective-permute-start | bytes 786440 | tf_op jit(solution)/shard_map/ppermute | solution.py:17
  25.8 15.4 %collective-permute-start.2 = (bf16[256,512]{1,0:T(8,128)(2,1)S(1)}, bf16[256,512]{1,0:T(8,128)(2,1)S(1)}, u32[]{:S(2)}, u32[]{:S(2)}) collective-permute-start(bf16[256,512]{1,0:T(8,128)(2,1)S(1)} %collective-permute-done.1), channel_id=1, source_target_pairs={{0,1},{1,0},{2,3},{3,2},{4,5},{5,4},{6,7},{7,6},{8,9},{9,8},{10,11... | collective-permute-start | bytes 786440 | tf_op jit(solution)/shard_map/ppermute | solution.py:17
  25.9 2.1 %copy-start = (bf16[1,384,2048]{2,1,0:T(8,128)(2,1)S(1)}, bf16[1,384,2048]{2,1,0:T(8,128)(2,1)}, u32[]{:S(2)}) copy-start(bf16[1,384,2048]{2,1,0:T(8,128)(2,1)} %refs_0_.2) | copy-start | bytes 4718596
  25.9 2.1 %copy-start.1 = (bf16[1,384,2048]{2,1,0:T(8,128)(2,1)S(1)}, bf16[1,384,2048]{2,1,0:T(8,128)(2,1)}, u32[]{:S(2)}) copy-start(bf16[1,384,2048]{2,1,0:T(8,128)(2,1)} %refs_1_.1) | copy-start | bytes 4718596
  25.9 2.1 %copy-start.4 = (bf16[31,2048]{1,0:T(8,128)(2,1)S(1)}, bf16[31,2048]{1,0:T(8,128)(2,1)}, u32[]{:S(2)}) copy-start(bf16[31,2048]{1,0:T(8,128)(2,1)} %refs_2_.1) | copy-start | bytes 380932
  25.9 33.9 %collective-permute-start.11 = (bf16[3,256,512]{2,1,0:T(8,128)(2,1)S(1)}, bf16[3,256,512]{2,1,0:T(8,128)(2,1)S(1)}, u32[]{:S(2)}, u32[]{:S(2)}) collective-permute-start(bf16[3,256,512]{2,1,0:T(8,128)(2,1)S(1)} %shard_map.70), channel_id=1, source_target_pairs={{0,1},{1,0},{2,3},{3,2},{4,5},{5,4},{6,7},{7,6},{8,9},{9,8},{10,11... | collective-permute-start | bytes 2359304 | tf_op jit(solution)/shard_map/ppermute | solution.py:17
  26.5 16.2 %collective-permute-start.13 = (bf16[2,256,512]{2,1,0:T(8,128)(2,1)S(1)}, bf16[2,256,512]{2,1,0:T(8,128)(2,1)S(1)}, u32[]{:S(2)}, u32[]{:S(2)}) collective-permute-start(bf16[2,256,512]{2,1,0:T(8,128)(2,1)S(1)} %collective-permute-done.12.refs_4_), channel_id=1, source_target_pairs={{0,2},{1,5},{2,0},{3,7},{4,6},{5,1},{6,4},{7,3},{8,10},{9,13},{10,... | collective-permute-start | bytes 1572872 | tf_op jit(solution)/shard_map/ppermute | solution.py:17
  28.0 32.0 %copy-start.5 = (f32[2048]{0:T(1024)S(1)}, f32[2048]{0:T(1024)}, u32[]{:S(2)}) copy-start(f32[2048]{0:T(1024)} %param.9) | copy-start | bytes 24580
  28.0 32.0 %copy-start.6 = (f32[2048]{0:T(1024)S(1)}, f32[2048]{0:T(1024)}, u32[]{:S(2)}) copy-start(f32[2048]{0:T(1024)} %param.10) | copy-start | bytes 24580
  29.2 8.2 %collective-permute-start = (bf16[32,2048]{1,0:T(8,128)(2,1)S(1)}, bf16[32,2048]{1,0:T(8,128)(2,1)S(1)}, u32[]{:S(2)}, u32[]{:S(2)}) collective-permute-start(bf16[32,2048]{1,0:T(8,128)(2,1)S(1)} %get-tuple-element.12), channel_id=1, source_target_pairs={{0,8},{8,16},{16,24},{24,0},{1,9},{9,17},{17,25},{25,1},{2,10},{10... | collective-permute-start | bytes 393224 | tf_op jit(solution)/shard_map/ppermute | solution.py:303
  34.4 8.8 %collective-permute-start.7 = (bf16[256,512]{1,0:T(8,128)(2,1)S(1)}, bf16[256,512]{1,0:T(8,128)(2,1)S(1)}, u32[]{:S(2)}, u32[]{:S(2)}) collective-permute-start(bf16[256,512]{1,0:T(8,128)(2,1)S(1)} %collective-permute-done.1), channel_id=1, source_target_pairs={{0,2},{1,5},{2,0},{3,7},{4,6},{5,1},{6,4},{7,3},{8,10},{9,13},{10,... | collective-permute-start | bytes 786440 | tf_op jit(solution)/shard_map/ppermute | solution.py:17
  37.3 9.8 %collective-permute-start.5 = (bf16[256,512]{1,0:T(8,128)(2,1)S(1)}, bf16[256,512]{1,0:T(8,128)(2,1)S(1)}, u32[]{:S(2)}, u32[]{:S(2)}) collective-permute-start(bf16[256,512]{1,0:T(8,128)(2,1)S(1)} %collective-permute-done.4.refs_2_), channel_id=1, source_target_pairs={{0,24},{8,16},{16,8},{24,0},{1,25},{9,17},{17,9},{25,1},{2,26},{10... | collective-permute-start | bytes 786440 | tf_op jit(solution)/shard_map/ppermute | solution.py:17
  41.1 18.1 %collective-permute-start.14 = (bf16[2,256,512]{2,1,0:T(8,128)(2,1)S(1)}, bf16[2,256,512]{2,1,0:T(8,128)(2,1)S(1)}, u32[]{:S(2)}, u32[]{:S(2)}) collective-permute-start(bf16[2,256,512]{2,1,0:T(8,128)(2,1)S(1)} %collective-permute-done.12.refs_4_), channel_id=1, source_target_pairs={{0,4},{1,3},{2,6},{3,1},{4,0},{5,7},{6,2},{7,5},{8,12},{9,11},{10,... | collective-permute-start | bytes 1572872 | tf_op jit(solution)/shard_map/ppermute | solution.py:17
  42.7 16.7 %collective-permute-start.15 = (bf16[2,256,512]{2,1,0:T(8,128)(2,1)S(1)}, bf16[2,256,512]{2,1,0:T(8,128)(2,1)S(1)}, u32[]{:S(2)}, u32[]{:S(2)}) collective-permute-start(bf16[2,256,512]{2,1,0:T(8,128)(2,1)S(1)} %collective-permute-done.13.refs_5_), channel_id=1, source_target_pairs={{0,4},{1,3},{2,6},{3,1},{4,0},{5,7},{6,2},{7,5},{8,12},{9,11},{10,... | collective-permute-start | bytes 1572872 | tf_op jit(solution)/shard_map/ppermute | solution.py:17
  43.2 15.6 %collective-permute-start.8 = (bf16[256,512]{1,0:T(8,128)(2,1)S(1)}, bf16[256,512]{1,0:T(8,128)(2,1)S(1)}, u32[]{:S(2)}, u32[]{:S(2)}) collective-permute-start(bf16[256,512]{1,0:T(8,128)(2,1)S(1)} %collective-permute-done.1), channel_id=1, source_target_pairs={{0,4},{1,3},{2,6},{3,1},{4,0},{5,7},{6,2},{7,5},{8,12},{9,11},{10,... | collective-permute-start | bytes 786440 | tf_op jit(solution)/shard_map/ppermute | solution.py:17
  47.2 11.6 %collective-permute-start.6 = (bf16[256,512]{1,0:T(8,128)(2,1)S(1)}, bf16[256,512]{1,0:T(8,128)(2,1)S(1)}, u32[]{:S(2)}, u32[]{:S(2)}) collective-permute-start(bf16[256,512]{1,0:T(8,128)(2,1)S(1)} %collective-permute-done.5), channel_id=1, source_target_pairs={{0,1},{1,0},{2,3},{3,2},{4,5},{5,4},{6,7},{7,6},{8,9},{9,8},{10,11... | collective-permute-start | bytes 786440 | tf_op jit(solution)/shard_map/ppermute | solution.py:17
  58.8 15.1 %collective-permute-start.16 = (bf16[2,256,512]{2,1,0:T(8,128)(2,1)S(1)}, bf16[2,256,512]{2,1,0:T(8,128)(2,1)S(1)}, u32[]{:S(2)}, u32[]{:S(2)}) collective-permute-start(bf16[2,256,512]{2,1,0:T(8,128)(2,1)S(1)} %collective-permute-done.12.refs_4_), channel_id=1, source_target_pairs={{0,1},{1,0},{2,3},{3,2},{4,5},{5,4},{6,7},{7,6},{8,9},{9,8},{10,11... | collective-permute-start | bytes 1572872 | tf_op jit(solution)/shard_map/ppermute | solution.py:17
  58.8 15.1 %collective-permute-start.17 = (bf16[2,256,512]{2,1,0:T(8,128)(2,1)S(1)}, bf16[2,256,512]{2,1,0:T(8,128)(2,1)S(1)}, u32[]{:S(2)}, u32[]{:S(2)}) collective-permute-start(bf16[2,256,512]{2,1,0:T(8,128)(2,1)S(1)} %collective-permute-done.13.refs_5_), channel_id=1, source_target_pairs={{0,1},{1,0},{2,3},{3,2},{4,5},{5,4},{6,7},{7,6},{8,9},{9,8},{10,11... | collective-permute-start | bytes 1572872 | tf_op jit(solution)/shard_map/ppermute | solution.py:17
  59.3 14.6 %collective-permute-start.18 = (bf16[2,256,512]{2,1,0:T(8,128)(2,1)S(1)}, bf16[2,256,512]{2,1,0:T(8,128)(2,1)S(1)}, u32[]{:S(2)}, u32[]{:S(2)}) collective-permute-start(bf16[2,256,512]{2,1,0:T(8,128)(2,1)S(1)} %collective-permute-done.14.refs_6_), channel_id=1, source_target_pairs={{0,1},{1,0},{2,3},{3,2},{4,5},{5,4},{6,7},{7,6},{8,9},{9,8},{10,11... | collective-permute-start | bytes 1572872 | tf_op jit(solution)/shard_map/ppermute | solution.py:17
  59.4 14.6 %collective-permute-start.19 = (bf16[2,256,512]{2,1,0:T(8,128)(2,1)S(1)}, bf16[2,256,512]{2,1,0:T(8,128)(2,1)S(1)}, u32[]{:S(2)}, u32[]{:S(2)}) collective-permute-start(bf16[2,256,512]{2,1,0:T(8,128)(2,1)S(1)} %collective-permute-done.15.refs_7_), channel_id=1, source_target_pairs={{0,1},{1,0},{2,3},{3,2},{4,5},{5,4},{6,7},{7,6},{8,9},{9,8},{10,11... | collective-permute-start | bytes 1572872 | tf_op jit(solution)/shard_map/ppermute | solution.py:17
  59.8 15.1 %collective-permute-start.20 = (bf16[2,256,512]{2,1,0:T(8,128)(2,1)S(1)}, bf16[2,256,512]{2,1,0:T(8,128)(2,1)S(1)}, u32[]{:S(2)}, u32[]{:S(2)}) collective-permute-start(bf16[2,256,512]{2,1,0:T(8,128)(2,1)S(1)} %shard_map.75), channel_id=1, source_target_pairs={{0,1},{1,0},{2,3},{3,2},{4,5},{5,4},{6,7},{7,6},{8,9},{9,8},{10,11... | collective-permute-start | bytes 1572872 | tf_op jit(solution)/shard_map/ppermute | solution.py:17
  70.5 1.0 %copy-start.3 = (bf16[256,512]{1,0:T(8,128)(2,1)S(1)}, bf16[256,512]{1,0:T(8,128)(2,1)}, u32[]{:S(2)}) copy-start(bf16[256,512]{1,0:T(8,128)(2,1)} %refs_0_.3) | copy-start | bytes 786436
